TPU v7x, 256 devices: a whole 4x4x8 slice. The times are simulated.
256 devices in a mesh: sp: 64 (over z, x, core), tp: 4 (over y).
Axes of the slice: x: 4, y: 4, z: 8, core: 2. Of those that a mesh axis runs over, the one named last changes fastest.
Arguments:
- layer_input: bfloat16 [8192, 2048], P('sp', 'tp'), may hold values from -6 to 6
- cotangent: bfloat16 [8192, 2048], P('sp', 'tp'), may hold values from -16 to 16
- routes: int32 [8192, 2], P('sp'), may hold values from 0 to 63, all different within a row; in each aligned block of 128 rows (0 to 127, 128 to 255, ...) at most 6 rows name the same one
- route_weight: float32 [8192, 2], P('sp'), may hold values from 0.1 to 0.6
- gate_weight: bfloat16 [64, 2048, 1024], P('sp', None, 'tp'), may hold values from -0.125 to 0.125
- up_weight: bfloat16 [64, 2048, 1024], P('sp', None, 'tp'), may hold values from -0.125 to 0.125
- down_weight: bfloat16 [64, 1024, 2048], P('sp', 'tp'), may hold values from -0.1875 to 0.1875
- heads_value: bfloat16 [8192, 2048], P('sp', 'tp'), may hold values from -6 to 6
- output_gate: bfloat16 [8192, 2048], P('sp', 'tp'), may hold values from -8 to 8
- mixer_saved: bfloat16 [8192, 2048], P('sp', 'tp'), may hold values from -6 to 6
- proj_weight: bfloat16 [2048, 2048], P(None, 'tp'), may hold values from -0.125 to 0.125
- state_write: bfloat16 [8192, 512], P('sp', 'tp'), may hold values from -0.5 to 0.5
- state_read: bfloat16 [8192, 512], P('sp', 'tp'), may hold values from -0.5 to 0.5
- decay_rate: float32 [8192, 32], P('sp', 'tp'), may hold values from 0 to 1.1, as said below
Outputs:
- gate_grad: bfloat16 [64, 2048, 1024], P('sp', None, 'tp')
- up_grad: bfloat16 [64, 2048, 1024], P('sp', None, 'tp')
- down_grad: bfloat16 [64, 1024, 2048], P('sp', 'tp')
- proj_grad: float32 [2048, 2048], P('sp', 'tp')
- value_grad: bfloat16 [8192, 2048], P('sp', 'tp')
- write_gradient: bfloat16 [8192, 512], P('sp', 'tp')
- read_gradient: bfloat16 [8192, 512], P('sp', 'tp')
- outgate_grad: bfloat16 [8192, 2048], P('sp', 'tp')
Inputs may be any that keep to these rules, and one draw needn't show every extreme that they name: `routes`: each row names 2 different experts; within the rows of one aligned block of 128 tokens no expert is named by more than 6 rows, a bound that some block reaches. `decay_rate`: positive log-decays.
All inputs are finite; a program needn't handle non-finite values.
Results may differ from a plain program's by a relative error of at most 0.017.
Values may be sent and summed in bfloat16 or wider, within the bound.
No kernel may reach another device: no remote copies, remote signals or barrier semaphores. Data moves between devices by JAX's collectives and lax.ppermute only.
A program may use at most 128 MiB of HBM per device.

v0:
```python
import jax
import jax.numpy as jnp
from jax import lax
from jax.experimental import pallas as pl
from jax.experimental.pallas import tpu as pltpu
from jax.sharding import Mesh
from jax.sharding import PartitionSpec as P


HEAD_DIM = 64
STATE = 128
SP = ("sp_0", "sp_1", "sp_2")
CHIPS = ("sp_0", "sp_1")
CORE = "sp_2"
TP = "tp"

f32 = jnp.float32
bf16 = jnp.bfloat16


def dot(a, b, ca=1, cb=0):
    return lax.dot_general(a, b, (((ca,), (cb,)), ((), ())), preferred_element_type=f32)


def swap(x):
    return lax.ppermute(x, CORE, [(0, 1), (1, 0)])


def ring(x, shift, axis=TP):
    n = lax.axis_size(axis)
    return lax.ppermute(x, axis, [(i, (i + shift) % n) for i in range(n)])


def ring_reduce(parts, axis):
    own, right, far, left = parts
    opposite = ring(far, 2, axis)
    low = ring(right, 1, axis)
    up = ring(left, -1, axis)
    return own.astype(f32) + low.astype(f32) + up.astype(f32) + opposite.astype(f32)


def exchange(x):
    return lax.all_to_all(x, CHIPS, split_axis=0, concat_axis=0, tiled=True)


def silu_parts(value):
    sigma = jax.nn.sigmoid(value)
    return (value * sigma, sigma * (1.0 + value * (1.0 - sigma)))


def scan_kernel(msg_ref, out_ref, work_ref):
    chunks, height, _ = out_ref.shape
    work_ref[...] = msg_ref[...].astype(f32)
    fades = [
        jnp.exp(-(work_ref[k, height : height + 1, :] + work_ref[k, height + 1 : height + 2, :]))
        for k in range(chunks)
    ]
    states = [jnp.zeros((8, 128), f32)] * (height // 8)
    for i in range(chunks):
        for s in range(height // 8):
            k = i if s % 2 == 0 else chunks - 1 - i
            rows = slice(s * 8, s * 8 + 8)
            own = work_ref[k, rows, :]
            work_ref[k, rows, :] = states[s]
            states[s] = states[s] * fades[k] + own
    out_ref[...] = work_ref[:, :height, :].astype(bf16)


def scan_chunks(msg):
    chunks, height, lanes = msg.shape
    return pl.pallas_call(
        scan_kernel,
        out_shape=jax.ShapeDtypeStruct((chunks, height - 8, lanes), bf16),
        scratch_shapes=[pltpu.VMEM(msg.shape, f32)],
    )(msg)


def tail_kernel(
    core_ref,
    back_ref,
    write_ref,
    value_start_ref,
    value_end_ref,
    delta_start_ref,
    delta_end_ref,
    fade_start_ref,
    fade_end_ref,
    base_ref,
    mine_ref,
    send_ref,
    work_ref,
):
    blocks = value_start_ref.shape[1] // 128
    steps = back_ref.shape[0] // blocks
    half = blocks * 128
    write = write_ref[...]
    write_sum = base_ref[:, half : half + STATE]
    read_sum = base_ref[:, half + STATE :]
    for q in range(blocks):
        states = back_ref[q * steps : (q + 1) * steps].astype(f32)
        read_low, read_high, write_low, write_high = (
            states[:, 8 * i : 8 * i + 8, :].reshape(STATE, 128).astype(bf16) for i in range(4)
        )
        lanes = slice(q * 128, (q + 1) * 128)
        work_ref[:, lanes] = (
            base_ref[:, lanes]
            + dot(write, read_low) * fade_start_ref[:, lanes]
            + dot(write, read_high) * fade_end_ref[:, lanes]
        )
        write_sum = write_sum + dot(value_start_ref[:, lanes], read_low, 1, 1)
        write_sum = write_sum + dot(value_end_ref[:, lanes], read_high, 1, 1)
        read_sum = read_sum + dot(delta_start_ref[:, lanes], write_low, 1, 1)
        read_sum = read_sum + dot(delta_end_ref[:, lanes], write_high, 1, 1)
    work_ref[:, half : half + STATE] = write_sum
    work_ref[:, half + STATE :] = read_sum
    tokens = mine_ref.shape[0]
    mine_ref[...] = work_ref[pl.ds(pl.multiple_of(core_ref[0] * tokens, tokens), tokens), :]
    send_ref[...] = work_ref[
        pl.ds(pl.multiple_of((1 - core_ref[0]) * tokens, tokens), tokens), :
    ].astype(bf16)


def tail(core, back, write, value_start, value_end, delta_start, delta_end, fades, base):
    rows, width = base.shape
    vmem = pl.BlockSpec(memory_space=pltpu.VMEM)
    return pl.pallas_call(
        tail_kernel,
        in_specs=[pl.BlockSpec(memory_space=pltpu.SMEM)] + [vmem] * 9,
        out_shape=(
            jax.ShapeDtypeStruct((rows // 2, width), f32),
            jax.ShapeDtypeStruct((rows // 2, width), bf16),
        ),
        scratch_shapes=[pltpu.VMEM((rows, width), f32)],
    )(core.reshape(1), back, write, value_start, value_end, delta_start, delta_end, *fades, base)


def to_message(low, high):
    def cut(a):
        n, w = a.shape
        return a.astype(bf16).reshape(n // 8, 8, w // 128, 128).transpose(2, 0, 1, 3)

    both = jnp.stack([cut(low), cut(high)], axis=2)
    return both.reshape(-1, 16, 128)


def on_device(
    layer_input,
    cotangent,
    routes,
    route_weight,
    gate_weight,
    up_weight,
    down_weight,
    heads_value,
    output_gate,
    mixer_saved,
    proj_weight,
    state_write,
    state_read,
    decay_rate,
):
    core = lax.axis_index(CORE)
    tp = lax.axis_index(TP)
    first = core == 0
    tokens, width = layer_input.shape
    chips = lax.axis_size(CHIPS)
    experts = 2 * chips
    cap = max(2, 3 * tokens * routes.shape[1] // (2 * experts))
    rows = 2 * cap
    n_tp = lax.axis_size(TP)
    heads = decay_rate.shape[1]
    half_heads = heads // 2
    half = heads_value.shape[1] // 2

    def ordered(mine, other, axis=0):
        return jnp.concatenate(
            [jnp.where(first, mine, other), jnp.where(first, other, mine)], axis=axis
        )

    def halves(a):
        left, right = a[:, : a.shape[1] // 2], a[:, a.shape[1] // 2 :]
        return jnp.where(first, left, right), jnp.where(first, right, left)

    small = jnp.concatenate([routes.astype(f32), route_weight, decay_rate], axis=1)
    small_other = swap(small)
    input_other = swap(layer_input)
    cotangent_other = swap(cotangent)

    routes_row = jnp.concatenate([routes.T, small_other[:, 0:2].T.astype(jnp.int32)], axis=1)
    weight_row = jnp.concatenate([route_weight.T, small_other[:, 2:4].T], axis=1)
    count = 2 * tokens
    token_row = lax.broadcasted_iota(jnp.int32, (1, count), 1)
    source_row = (token_row >= tokens).astype(jnp.int32)
    expert_col = lax.broadcasted_iota(jnp.int32, (experts, count), 0)
    named = [expert_col == routes_row[k : k + 1] for k in range(2)]
    named_any = (named[0] | named[1]).astype(bf16)
    earlier = lax.broadcasted_iota(jnp.int32, (count, count), 0)
    later = lax.broadcasted_iota(jnp.int32, (count, count), 1)
    before_mask = ((earlier < later) & ((earlier < tokens) == (later < tokens))).astype(bf16)
    before = dot(named_any, before_mask)
    place = []
    for k in range(2):
        rank = jnp.sum(jnp.where(named[k], before, 0.0), axis=0, keepdims=True).astype(jnp.int32)
        expert = routes_row[k : k + 1]
        here = (expert & 1) == core
        place.append(
            (jnp.where(here, expert >> 1, -1), source_row * cap + rank)
        )
    out_col = lax.broadcasted_iota(jnp.int32, (chips * 2 * rows, 2 * count), 0)
    pick = None
    scale = None
    for k in range(2):
        chip, inner = place[k]
        spot = jnp.where(chip < 0, -1, chip * (2 * rows) + inner)
        spots = jnp.concatenate([spot, jnp.where(spot < 0, -1, spot + rows)], axis=1)
        factor = jnp.concatenate([jnp.ones_like(weight_row[k : k + 1]), weight_row[k : k + 1]], axis=1)
        hit = out_col == spots
        part = jnp.where(hit, factor, 0.0)
        pick = hit if pick is None else pick | hit
        scale = part if scale is None else scale + part
    scale = jnp.sum(scale, axis=1, keepdims=True)
    stacked = jnp.concatenate([layer_input, input_other, cotangent, cotangent_other], axis=0)
    sent = (dot(pick.astype(bf16), stacked) * scale).astype(bf16)
    later_inputs = (gate_weight, up_weight, down_weight, heads_value, output_gate, mixer_saved)
    later_inputs += (proj_weight, state_write, state_read, decay_rate, small_other)
    sent, later_inputs = lax.optimization_barrier((sent, later_inputs))
    gate_weight, up_weight, down_weight, heads_value, output_gate, mixer_saved = later_inputs[:6]
    proj_weight, state_write, state_read, decay_rate, small_other = later_inputs[6:]

    back_col = lax.broadcasted_iota(jnp.int32, (chips * rows, count), 0)
    back = None
    for k in range(2):
        chip, inner = place[k]
        hit = back_col == jnp.where(chip < 0, -1, chip * rows + inner)
        back = hit if back is None else back | hit
    back = back.astype(bf16)

    active_gate, slope_gate = silu_parts(output_gate.astype(f32))
    saved = mixer_saved.astype(f32)
    gated = (saved * active_gate).astype(bf16)
    value_mine, value_send = halves(heads_value)
    gated_mine, gated_send = halves(gated)
    side = jnp.concatenate([value_send, gated_send, state_write, state_read], axis=1)
    side_other = swap(side)
    value = ordered(value_mine, side_other[:, :half])
    gated_all = jnp.concatenate([gated_mine, side_other[:, half : 2 * half]], axis=0)
    write = ordered(state_write, side_other[:, 2 * half : 2 * half + STATE])
    read = ordered(state_read, side_other[:, 2 * half + STATE :])
    rates = ordered(halves(decay_rate)[0], halves(small_other[:, 4:])[0])
    cumul = jnp.cumsum(rates, axis=0)
    spread = (
        lax.broadcasted_iota(jnp.int32, (half_heads, half), 1) // HEAD_DIM
        == lax.broadcasted_iota(jnp.int32, (half_heads, half), 0)
    ).astype(f32)
    cumul_wide = jnp.dot(cumul, spread, precision=lax.Precision.HIGHEST)
    total_wide = cumul_wide[-1:]
    fade_end = jnp.exp(cumul_wide - total_wide)
    fade_start = jnp.exp(-cumul_wide)
    value_f = value.astype(f32)
    value_end = (value_f * fade_end).astype(bf16)
    value_start = (value_f * fade_start).astype(bf16)
    write_states = to_message(dot(write, value_end, 0, 0), dot(write, value_start, 0, 0))
    total_high = lax.reduce_precision(total_wide, 8, 7)
    total_rows = jnp.concatenate(
        [total_high, total_wide - total_high, jnp.zeros((6, half), f32)], axis=0
    ).astype(bf16)
    total_rows = jnp.broadcast_to(
        total_rows.reshape(8, half // 128, 1, 128).transpose(1, 2, 0, 3),
        (half // 128, STATE // 8, 8, 128),
    ).reshape(-1, 8, 128)
    quarter = width

    def rolled(a):
        parts = a.reshape(n_tp, quarter, a.shape[1])
        return [
            lax.dynamic_index_in_dim(parts, (tp + i) & (n_tp - 1), 0, keepdims=False)
            for i in range(n_tp)
        ]

    def unrolled(parts):
        stack = jnp.stack(parts)
        return [
            lax.dynamic_index_in_dim(stack, (k + n_tp - tp) & (n_tp - 1), 0, keepdims=False)
            for k in range(n_tp)
        ]

    gate_up = [
        jnp.concatenate(pair, axis=1) for pair in zip(rolled(gate_weight[0]), rolled(up_weight[0]))
    ]
    down = [
        lax.dynamic_slice_in_dim(down_weight[0], ((tp + i) & (n_tp - 1)) * quarter, quarter, 1)
        for i in range(n_tp)
    ]
    proj = rolled(proj_weight)
    hid = gate_weight.shape[2]
    slots = chips * rows

    out_row = lax.broadcasted_iota(jnp.int32, (2 * slots, 2 * slots), 0)
    in_row = lax.broadcasted_iota(jnp.int32, (2 * slots, 2 * slots), 1)
    kind = (out_row >= slots).astype(jnp.int32)
    slot = out_row - kind * slots
    sort_rows = (slot + slot // rows * rows + kind * rows == in_row).astype(bf16)
    sort_rows, sent = lax.optimization_barrier((sort_rows, sent))
    received = exchange(sent.reshape(chips, 2 * rows, width)).reshape(2 * slots, width)
    sorted_rows = dot(sort_rows, received).astype(bf16)
    from_low = ring(sorted_rows, 1)
    from_up = ring(sorted_rows, -1)
    input_far = ring(from_low[:slots], 1)
    cotangent_far = ring(from_up[slots:], -1)
    input_parts = [sorted_rows[:slots], from_up[:slots], input_far, from_low[:slots]]
    cotangent_parts = [sorted_rows[slots:], from_up[slots:], cotangent_far, from_low[slots:]]
    order = (0, 1, 3, 2)
    pre = sum(dot(input_parts[i], gate_up[i]) for i in order)
    hidden_grad = sum(dot(cotangent_parts[i], down[i], 1, 1) for i in order)
    pre_gate, pre_up = pre[:, :hid], pre[:, hid:]
    active, slope = silu_parts(pre_gate)
    hidden = (active * pre_up).astype(bf16)
    deltas = jnp.concatenate(
        [(hidden_grad * pre_up * slope).astype(bf16), (hidden_grad * active).astype(bf16)], axis=1
    )
    ready = (write, read, value, gated_all, cumul, fade_end, fade_start, value_end, value_start)
    ready += (write_states, total_rows)
    deltas, ready = lax.optimization_barrier((deltas, ready))
    write, read, value, gated_all, cumul, fade_end, fade_start, value_end, value_start = ready[:9]
    write_states, total_rows = ready[9:]
    partial = [dot(deltas, gate_up[i], 1, 1).astype(bf16) for i in range(n_tp)]
    returned = ring_reduce(partial, TP).astype(bf16)
    returned, deltas, hidden = lax.optimization_barrier((returned, deltas, hidden))
    arrived = exchange(returned.reshape(chips, rows, width)).reshape(slots, width)

    both_grad = unrolled([dot(input_parts[i], deltas, 0, 0).astype(bf16) for i in range(n_tp)])
    gate_grad = jnp.concatenate([a[:, :hid] for a in both_grad], axis=0)[None]
    up_grad = jnp.concatenate([a[:, hid:] for a in both_grad], axis=0)[None]
    down_grad = jnp.concatenate(
        unrolled([dot(hidden, cotangent_parts[i], 0, 0).astype(bf16) for i in range(n_tp)]), axis=1
    )[None]

    summed = dot(back, arrived, 0, 0)
    summed_other = swap(summed[tokens:].astype(bf16)).astype(f32)
    layer_grad = (cotangent.astype(f32) + summed[:tokens] + summed_other).astype(bf16)
    grads = [layer_grad, ring(layer_grad, -1), ring(layer_grad, 2), ring(layer_grad, 1)]
    out_delta = sum(dot(grads[i], proj[i]) for i in (0, 1, 3, 2)).astype(bf16).astype(f32)
    outgate_grad = (out_delta * saved * slope_gate).astype(bf16)
    mixer_delta = (out_delta * active_gate).astype(bf16)
    delta_mine, delta_send = halves(mixer_delta)
    delta = ordered(delta_mine, swap(delta_send))
    delta_f = delta.astype(f32)
    delta_end = (delta_f * fade_end).astype(bf16)
    delta_start = (delta_f * fade_start).astype(bf16)
    read_states = to_message(dot(read, delta_end, 0, 0), dot(read, delta_start, 0, 0))
    states_got = exchange(jnp.concatenate([read_states, write_states, total_rows], axis=1))

    grad_mine = jnp.concatenate(grads, axis=1)
    grad_all = jnp.concatenate([grad_mine, swap(grad_mine)], axis=0)
    proj_part = dot(grad_all, gated_all, 0, 0).astype(bf16)
    deep, wide = lax.axis_size(SP[0]), lax.axis_size(SP[1])
    block = proj_part.shape[0] // chips
    across = lax.axis_index(SP[1])
    proj_part = jnp.stack(unrolled([
        proj_part[i * quarter : (i + 1) * quarter].reshape(deep // n_tp, wide, block, half)
        for i in range(n_tp)
    ]))
    proj_sum = ring_reduce(
        [
            lax.dynamic_index_in_dim(
                proj_part, (across + i) & (wide - 1), 2, keepdims=False
            ).reshape(deep, block, half)
            for i in range(wide)
        ],
        SP[1],
    )
    scanned = scan_chunks(states_got)
    states_back = exchange(scanned)
    depth = lax.axis_index(SP[0])
    gap = deep // 2
    while gap:
        upper = (depth & gap) != 0
        below, above = proj_sum[:gap], proj_sum[gap:]
        away = jnp.where(upper, below, above).astype(bf16)
        got = lax.ppermute(away, SP[0], [(i, i ^ gap) for i in range(deep)])
        proj_sum = jnp.where(upper, above, below) + got.astype(f32)
        gap //= 2
    proj_sum = proj_sum[0]
    top, bottom = proj_sum[: block // 2], proj_sum[block // 2 :]
    proj_mine = jnp.where(first, top, bottom)
    proj_grad = ordered(proj_mine, swap(jnp.where(first, bottom, top)), axis=1)

    cumul_row = cumul.T
    common = dot(read, write, 1, 1)
    score = None
    value_parts = []
    for h in range(half_heads):
        mix = jnp.exp(-jnp.abs(cumul[:, h : h + 1] - cumul_row[h : h + 1]))
        lanes = slice(h * HEAD_DIM, (h + 1) * HEAD_DIM)
        match = dot(delta[:, lanes], value[:, lanes], 1, 1) * mix
        score = match if score is None else score + match
        value_parts.append(dot((mix * common).astype(bf16), delta[:, lanes], 0, 0))
    score = score.astype(bf16)
    base = jnp.concatenate(value_parts + [dot(score, read, 0, 0), dot(score, write)], axis=1)
    outs_mine, outs_send = tail(
        core,
        states_back,
        write,
        value_start,
        value_end,
        delta_start,
        delta_end,
        (fade_start, fade_end),
        base,
    )
    outs_got = swap(outs_send)
    value_out = ordered(outs_mine[:, :half].astype(bf16), outs_got[:, :half], axis=1)
    sums = (outs_mine[:, half:] + outs_got[:, half:].astype(f32)).astype(bf16)
    return (
        gate_grad,
        up_grad,
        down_grad,
        proj_grad,
        value_out,
        sums[:, :STATE],
        sums[:, STATE:],
        outgate_grad,
    )


def solution(mesh):
    split = Mesh(mesh.devices.reshape(8, 4, 2, mesh.shape["tp"]), SP + (TP,))
    placed = (
        P(SP, TP),
        P(SP, TP),
        P(SP, None),
        P(SP, None),
        P(SP, None, TP),
        P(SP, None, TP),
        P(SP, TP, None),
        P(SP, TP),
        P(SP, TP),
        P(SP, TP),
        P(None, TP),
        P(SP, TP),
        P(SP, TP),
        P(SP, TP),
    )

    return jax.shard_map(
        on_device,
        mesh=split,
        in_specs=placed,
        out_specs=(
            P(SP, None, TP),
            P(SP, None, TP),
            P(SP, TP, None),
            P(SP, TP),
            P(SP, TP),
            P(SP, TP),
            P(SP, TP),
            P(SP, TP),
        ),
        check_vma=False,
    )
```

profile of v0, /device:TPU:4, one launch (start us, length us, event | category | flops | bytes accessed | tf_op | source)
XLA Modules:
  0.0 230.4 jit_solution(17282540462488674429)
XLA Ops:
  8.4 2.5 %multiply_convert_fusion = bf16[768,512]{1,0:T(8,128)(2,1)} fusion(f32[768]{0:T(1024)S(1)} %add_reduce_fusion, s32[512]{0:T(512)S(1)} %bitcast.247, s32[512]{0:T(512)S(1)} %bitcast.245, bf16[128,512]{1,0:T(8,128)(2,1)} %collective-permute-done.2, bf16[128,512]{1,0:T(8,128)(2,1)} %param.15, bf16[128,512]{1,0:T(8,128)(2,1)S(1)} %collective-permute-done.1, ...), kind=kOutput, calls=%fused_computation.4 | convolution fusion | flops 406716416 | bytes 1317888 | tf_op jit(solution)/shard_map/dot_general | solution.py:22
  10.9 1.2 reduce-window.6
  14.2 1.1 fusion.75
  16.7 1.5 pad_maximum_fusion.22
  18.6 11.6 %all-to-all-start = ((bf16[32,24,512]{2,1,0:T(8,128)(2,1)}), bf16[32,24,512]{2,1,0:T(8,128)(2,1)}, u32[]{:S(2)}, u32[]{:S(2)}) async-start(bf16[32,24,512]{2,1,0:T(8,128)(2,1)} %bitcast.227), calls=%async_computation | async-start | bytes 1572864 | tf_op jit(solution)/shard_map/all_to_all | solution.py:43
  30.4 2.3 dynamic-slice_bitcast_fusion.11
  33.7 1.4 broadcast_select_fusion.13
  35.1 1.5 broadcast_select_fusion.8
  39.9 13.2 %all-to-all-done = bf16[32,24,512]{2,1,0:T(8,128)(2,1)} async-done(((bf16[32,24,512]{2,1,0:T(8,128)(2,1)}), bf16[32,24,512]{2,1,0:T(8,128)(2,1)}, u32[]{:S(2)}, u32[]{:S(2)}) %all-to-all-start) | async-done | bytes 786464 | tf_op jit(solution)/shard_map/all_to_all | solution.py:43
  53.1 2.0 convolution_convert_fusion.1
  55.1 3.1 %collective-permute-start.3 = (bf16[768,512]{1,0:T(8,128)(2,1)S(1)}, bf16[768,512]{1,0:T(8,128)(2,1)S(1)}, u32[]{:S(2)}, u32[]{:S(2)}) collective-permute-start(bf16[768,512]{1,0:T(8,128)(2,1)S(1)} %convolution_convert_fusion.1), channel_id=1, source_target_pairs={{0,3},{1,0},{2,1},{3,2},{4,7},{5,4},{6,5},{7,6},{8,11},{9,8},{10,9... | collective-permute-start | bytes 2359304 | tf_op jit(solution)/shard_map/ppermute | solution.py:31
  60.4 16.6 %collective-permute-done.4 = bf16[768,512]{1,0:T(8,128)(2,1)S(1)} collective-permute-done((bf16[768,512]{1,0:T(8,128)(2,1)S(1)}, bf16[768,512]{1,0:T(8,128)(2,1)S(1)}, u32[]{:S(2)}, u32[]{:S(2)}) %collective-permute-start.4) | collective-permute-done | bytes 786464 | tf_op jit(solution)/shard_map/ppermute | solution.py:31
  77.2 3.5 %collective-permute-start.5 = (bf16[384,512]{1,0:T(8,128)(2,1)S(1)}, bf16[384,512]{1,0:T(8,128)(2,1)S(1)}, u32[]{:S(2)}, u32[]{:S(2)}) collective-permute-start(bf16[384,512]{1,0:T(8,128)(2,1)S(1)} %slice.323), channel_id=1, source_target_pairs={{0,3},{1,0},{2,1},{3,2},{4,7},{5,4},{6,5},{7,6},{8,11},{9,8},{10,9... | collective-permute-start | bytes 1179656 | tf_op jit(solution)/shard_map/ppermute | solution.py:31
  81.5 4.7 %collective-permute-done.5 = bf16[384,512]{1,0:T(8,128)(2,1)S(1)} collective-permute-done((bf16[384,512]{1,0:T(8,128)(2,1)S(1)}, bf16[384,512]{1,0:T(8,128)(2,1)S(1)}, u32[]{:S(2)}, u32[]{:S(2)}) %collective-permute-start.5) | collective-permute-done | bytes 393248 | tf_op jit(solution)/shard_map/ppermute | solution.py:31
  90.9 3.7 %collective-permute-start.9 = (bf16[384,512]{1,0:T(8,128)(2,1)S(1)}, bf16[384,512]{1,0:T(8,128)(2,1)S(1)}, u32[]{:S(2)}, u32[]{:S(2)}) collective-permute-start(bf16[384,512]{1,0:T(8,128)(2,1)S(1)} %convolution_convert_fusion.7), channel_id=1, source_target_pairs={{0,3},{1,0},{2,1},{3,2},{4,7},{5,4},{6,5},{7,6},{8,11},{9,8},{10,9... | collective-permute-start | bytes 1179656 | tf_op jit(solution)/shard_map/ppermute | solution.py:31
  94.6 1.4 collective-permute-start.10
  98.0 6.1 %collective-permute-done.8 = bf16[384,512]{1,0:T(8,128)(2,1)S(1)} collective-permute-done((bf16[384,512]{1,0:T(8,128)(2,1)S(1)}, bf16[384,512]{1,0:T(8,128)(2,1)S(1)}, u32[]{:S(2)}, u32[]{:S(2)}) %collective-permute-start.8) | collective-permute-done | bytes 393248 | tf_op jit(solution)/shard_map/ppermute | solution.py:31
  104.1 3.6 %collective-permute-done.9 = bf16[384,512]{1,0:T(8,128)(2,1)S(1)} collective-permute-done((bf16[384,512]{1,0:T(8,128)(2,1)S(1)}, bf16[384,512]{1,0:T(8,128)(2,1)S(1)}, u32[]{:S(2)}, u32[]{:S(2)}) %collective-permute-start.9) | collective-permute-done | bytes 393248 | tf_op jit(solution)/shard_map/ppermute | solution.py:31
  107.7 1.8 collective-permute-done.10
  109.6 1.2 add_convert_fusion
  110.8 1.9 reshape.177
  112.7 8.0 %all-to-all-start.1 = ((bf16[32,12,512]{2,1,0:T(8,128)(2,1)}), bf16[32,12,512]{2,1,0:T(8,128)(2,1)}, u32[]{:S(2)}, u32[]{:S(2)}) async-start(bf16[32,12,512]{2,1,0:T(8,128)(2,1)} %reshape.177), calls=%async_computation.1 | async-start | bytes 1048576 | tf_op jit(solution)/shard_map/all_to_all | solution.py:43
  120.7 1.3 fusion.13
  122.1 1.6 fusion.8
  129.9 1.1 maximum_bitcast_fusion.2
  131.0 3.2 %all-to-all-done.1 = bf16[32,12,512]{2,1,0:T(8,128)(2,1)} async-done(((bf16[32,12,512]{2,1,0:T(8,128)(2,1)}), bf16[32,12,512]{2,1,0:T(8,128)(2,1)}, u32[]{:S(2)}, u32[]{:S(2)}) %all-to-all-start.1) | async-done | bytes 393248 | tf_op jit(solution)/shard_map/all_to_all | solution.py:43
  134.2 1.1 reshape.178
  135.9 2.1 maximum_bitcast_fusion.1
  139.3 1.9 collective-permute-start.14
  141.2 1.6 collective-permute-start.12
  142.8 3.3 %collective-permute-done.13 = bf16[128,512]{1,0:T(8,128)(2,1)S(1)} collective-permute-done((bf16[128,512]{1,0:T(8,128)(2,1)S(1)}, bf16[128,512]{1,0:T(8,128)(2,1)S(1)}, u32[]{:S(2)}, u32[]{:S(2)}) %collective-permute-start.13) | collective-permute-done | bytes 131104 | tf_op jit(solution)/shard_map/ppermute | solution.py:31
  146.3 2.1 collective-permute-done.14
  155.9 1.2 collective-permute-start.16
  158.0 3.0 %collective-permute-start.18 = (bf16[8,64,256]{2,1,0:T(8,128)(2,1)S(1)}, bf16[8,64,256]{2,1,0:T(8,128)(2,1)S(1)}, u32[]{:S(2)}, u32[]{:S(2)}) collective-permute-start(bf16[8,64,256]{2,1,0:T(8,128)(2,1)S(1)} %bitcast.230), channel_id=1, source_target_pairs={{0,16},{8,24},{16,0},{24,8},{1,17},{9,25},{17,1},{25,9},{2,18},{10... | collective-permute-start | bytes 786440 | tf_op jit(solution)/shard_map/ppermute | solution.py:31
  161.5 3.5 %collective-permute-done.16 = bf16[8,64,256]{2,1,0:T(8,128)(2,1)S(1)} collective-permute-done((bf16[8,64,256]{2,1,0:T(8,128)(2,1)S(1)}, bf16[8,64,256]{2,1,0:T(8,128)(2,1)S(1)}, u32[]{:S(2)}, u32[]{:S(2)}) %collective-permute-start.16) | collective-permute-done | bytes 262176 | tf_op jit(solution)/shard_map/ppermute | solution.py:31
  165.0 1.3 collective-permute-done.17
  166.3 3.7 %collective-permute-done.18 = bf16[8,64,256]{2,1,0:T(8,128)(2,1)S(1)} collective-permute-done((bf16[8,64,256]{2,1,0:T(8,128)(2,1)S(1)}, bf16[8,64,256]{2,1,0:T(8,128)(2,1)S(1)}, u32[]{:S(2)}, u32[]{:S(2)}) %collective-permute-start.18) | collective-permute-done | bytes 262176 | tf_op jit(solution)/shard_map/ppermute | solution.py:31
  170.2 2.3 collective-permute-start.19
  172.8 8.6 %collective-permute-done.19 = bf16[4,64,256]{2,1,0:T(8,128)(2,1)S(1)} collective-permute-done((bf16[4,64,256]{2,1,0:T(8,128)(2,1)S(1)}, bf16[4,64,256]{2,1,0:T(8,128)(2,1)S(1)}, u32[]{:S(2)}, u32[]{:S(2)}) %collective-permute-start.19) | collective-permute-done | bytes 131104 | tf_op jit(solution)/shard_map/ppermute | solution.py:380
  181.4 2.0 collective-permute-start.20
  184.2 8.2 %all-to-all-start.2 = ((bf16[32,40,128]{2,1,0:T(8,128)(2,1)}), bf16[32,40,128]{2,1,0:T(8,128)(2,1)S(1)}, u32[]{:S(2)}, u32[]{:S(2)}) async-start(bf16[32,40,128]{2,1,0:T(8,128)(2,1)} %pad_maximum_fusion.20), calls=%async_computation.2 | async-start | bytes 655360 | tf_op jit(solution)/shard_map/all_to_all | solution.py:43
  192.5 1.6 collective-permute-start.21
  194.2 10.0 %all-to-all-done.2.msg_ref = bf16[32,40,128]{2,1,0:T(8,128)(2,1)S(1)} async-done(((bf16[32,40,128]{2,1,0:T(8,128)(2,1)}), bf16[32,40,128]{2,1,0:T(8,128)(2,1)S(1)}, u32[]{:S(2)}, u32[]{:S(2)}) %all-to-all-start.2) | async-done | bytes 327712 | tf_op jit(solution)/shard_map/all_to_all | solution.py:43
  205.0 1.8 shard_map.197
  206.8 5.7 %all-to-all-start.3 = ((bf16[32,32,128]{2,1,0:T(8,128)(2,1)}), bf16[32,32,128]{2,1,0:T(8,128)(2,1)S(1)}, u32[]{:S(2)}, u32[]{:S(2)}) async-start(bf16[32,32,128]{2,1,0:T(8,128)(2,1)} %shard_map.197), calls=%async_computation.3 | async-start | bytes 524288 | tf_op jit(solution)/shard_map/all_to_all | solution.py:43
  212.9 1.9 concatenate.132.base_ref
  214.8 7.6 %all-to-all-done.3.back_ref = bf16[32,32,128]{2,1,0:T(8,128)(2,1)S(1)} async-done(((bf16[32,32,128]{2,1,0:T(8,128)(2,1)}), bf16[32,32,128]{2,1,0:T(8,128)(2,1)S(1)}, u32[]{:S(2)}, u32[]{:S(2)}) %all-to-all-start.3) | async-done | bytes 262176 | tf_op jit(solution)/shard_map/all_to_all | solution.py:43
  223.1 2.6 %shard_map.198 = (f32[128,512]{1,0:T(8,128)}, bf16[128,512]{1,0:T(8,128)(2,1)}) custom-call(s32[1]{0:T(128)} %bitcast.75.core_ref, bf16[32,32,128]{2,1,0:T(8,128)(2,1)} %copy-done.26, bf16[256,128]{1,0:T(8,128)(2,1)} %pad_maximum_fusion.28.write_ref, bf16[256,256]{1,0:T(8,128)(2,1)} %copy-done.14, bf16[256,256]{1,0:T(8,128)(2,1)} %copy-done.13, ...), custom_call_target="tpu_custom_call" | custom-call | tf_op jit(solution)/shard_map/pallas_call | solution.py:126
  (273 shorter events, 50.3 us)
Async XLA Ops:
  0.6 145.4 %copy-start = (bf16[2048,512]{1,0:T(8,128)(2,1)S(1)}, bf16[2048,512]{1,0:T(8,128)(2,1)}, u32[]{:S(2)}) copy-start(bf16[2048,512]{1,0:T(8,128)(2,1)} %param.24) | copy-start | bytes 6291460
  2.2 2.8 %collective-permute-start = (f32[128,12]{0,1:T(8,128)S(1)}, f32[128,12]{0,1:T(8,128)S(1)}, u32[]{:S(2)}, u32[]{:S(2)}) collective-permute-start(f32[128,12]{0,1:T(8,128)S(1)} %pad_maximum_fusion.31), channel_id=1, source_target_pairs={{0,4},{4,0},{1,5},{5,1},{2,6},{6,2},{3,7},{7,3},{8,12},{12,8},{9,1... | collective-permute-start | bytes 18440 | tf_op jit(solution)/shard_map/ppermute | solution.py:26
  2.3 6.1 %collective-permute-start.1 = (bf16[128,512]{1,0:T(8,128)(2,1)}, bf16[128,512]{1,0:T(8,128)(2,1)S(1)}, u32[]{:S(2)}, u32[]{:S(2)}) collective-permute-start(bf16[128,512]{1,0:T(8,128)(2,1)} %param.14), channel_id=1, source_target_pairs={{0,4},{4,0},{1,5},{5,1},{2,6},{6,2},{3,7},{7,3},{8,12},{12,8},{9,1... | collective-permute-start | bytes 393224 | tf_op jit(solution)/shard_map/ppermute | solution.py:26
  2.8 5.6 %collective-permute-start.2 = (bf16[128,512]{1,0:T(8,128)(2,1)}, bf16[128,512]{1,0:T(8,128)(2,1)}, u32[]{:S(2)}, u32[]{:S(2)}) collective-permute-start(bf16[128,512]{1,0:T(8,128)(2,1)} %param.15), channel_id=1, source_target_pairs={{0,4},{4,0},{1,5},{5,1},{2,6},{6,2},{3,7},{7,3},{8,12},{12,8},{9,1... | collective-permute-start | bytes 393224 | tf_op jit(solution)/shard_map/ppermute | solution.py:26
  18.2 15.5 %collective-permute-start.7 = (bf16[128,768]{1,0:T(8,128)(2,1)}, bf16[128,768]{1,0:T(8,128)(2,1)}, u32[]{:S(2)}, u32[]{:S(2)}) collective-permute-start(bf16[128,768]{1,0:T(8,128)(2,1)} %pad_maximum_fusion.22), channel_id=1, source_target_pairs={{0,4},{4,0},{1,5},{5,1},{2,6},{6,2},{3,7},{7,3},{8,12},{12,8},{9,1... | collective-permute-start | bytes 589832 | tf_op jit(solution)/shard_map/ppermute | solution.py:26
  18.6 34.4 %all-to-all-start = ((bf16[32,24,512]{2,1,0:T(8,128)(2,1)}), bf16[32,24,512]{2,1,0:T(8,128)(2,1)}, u32[]{:S(2)}, u32[]{:S(2)}) async-start(bf16[32,24,512]{2,1,0:T(8,128)(2,1)} %bitcast.227), calls=%async_computation | async-start | bytes 1572864 | tf_op jit(solution)/shard_map/all_to_all | solution.py:43
  39.9 19.0 %copy-start.37 = (bf16[128,256]{1,0:T(8,128)(2,1)S(1)}, bf16[128,256]{1,0:T(8,128)(2,1)}, u32[]{:S(2)}) copy-start(bf16[128,256]{1,0:T(8,128)(2,1)} %get-tuple-element.139) | copy-start | bytes 196612
  39.9 19.0 %copy-start.38 = (bf16[128,256]{1,0:T(8,128)(2,1)S(1)}, bf16[128,256]{1,0:T(8,128)(2,1)}, u32[]{:S(2)}) copy-start(bf16[128,256]{1,0:T(8,128)(2,1)} %get-tuple-element.134) | copy-start | bytes 196612
  53.0 6.8 %copy-start.22 = (bf16[512,256]{1,0:T(8,128)(2,1)S(1)}, bf16[512,256]{1,0:T(8,128)(2,1)}, u32[]{:S(2)}) copy-start(bf16[512,256]{1,0:T(8,128)(2,1)} %get-tuple-element.103) | copy-start | bytes 786436
  53.1 6.8 %copy-start.23 = (bf16[512,256]{1,0:T(8,128)(2,1)S(1)}, bf16[512,256]{1,0:T(8,128)(2,1)}, u32[]{:S(2)}) copy-start(bf16[512,256]{1,0:T(8,128)(2,1)} %get-tuple-element.107) | copy-start | bytes 786436
  55.1 22.0 %copy-start.3 = (bf16[768,512]{1,0:T(8,128)(2,1)}, bf16[768,512]{1,0:T(8,128)(2,1)S(1)}, u32[]{:S(2)}) copy-start(bf16[768,512]{1,0:T(8,128)(2,1)S(1)} %convolution_convert_fusion.1) | copy-start | bytes 2359300
  55.1 22.1 %collective-permute-start.3 = (bf16[768,512]{1,0:T(8,128)(2,1)S(1)}, bf16[768,512]{1,0:T(8,128)(2,1)S(1)}, u32[]{:S(2)}, u32[]{:S(2)}) collective-permute-start(bf16[768,512]{1,0:T(8,128)(2,1)S(1)} %convolution_convert_fusion.1), channel_id=1, source_target_pairs={{0,3},{1,0},{2,1},{3,2},{4,7},{5,4},{6,5},{7,6},{8,11},{9,8},{10,9... | collective-permute-start | bytes 2359304 | tf_op jit(solution)/shard_map/ppermute | solution.py:31
  58.2 18.8 %collective-permute-start.4 = (bf16[768,512]{1,0:T(8,128)(2,1)S(1)}, bf16[768,512]{1,0:T(8,128)(2,1)S(1)}, u32[]{:S(2)}, u32[]{:S(2)}) collective-permute-start(bf16[768,512]{1,0:T(8,128)(2,1)S(1)} %convolution_convert_fusion.1), channel_id=1, source_target_pairs={{0,1},{1,2},{2,3},{3,0},{4,5},{5,6},{6,7},{7,4},{8,9},{9,10},{10,1... | collective-permute-start | bytes 2359304 | tf_op jit(solution)/shard_map/ppermute | solution.py:31
  59.6 21.1 %copy-start.16 = (bf16[512,256]{1,0:T(8,128)(2,1)S(1)}, bf16[512,256]{1,0:T(8,128)(2,1)}, u32[]{:S(2)}) copy-start(bf16[512,256]{1,0:T(8,128)(2,1)} %get-tuple-element.102) | copy-start | bytes 786436
  59.6 21.1 %copy-start.18 = (bf16[512,256]{1,0:T(8,128)(2,1)S(1)}, bf16[512,256]{1,0:T(8,128)(2,1)}, u32[]{:S(2)}) copy-start(bf16[512,256]{1,0:T(8,128)(2,1)} %get-tuple-element.106) | copy-start | bytes 786436
  77.0 11.4 %copy-start.1 = (bf16[768,512]{1,0:T(8,128)(2,1)}, bf16[768,512]{1,0:T(8,128)(2,1)S(1)}, u32[]{:S(2)}) copy-start(bf16[768,512]{1,0:T(8,128)(2,1)S(1)} %collective-permute-done.4) | copy-start | bytes 2359300
  77.1 9.6 %collective-permute-start.6 = (bf16[384,512]{1,0:T(8,128)(2,1)S(1)}, bf16[384,512]{1,0:T(8,128)(2,1)S(1)}, u32[]{:S(2)}, u32[]{:S(2)}) collective-permute-start(bf16[384,512]{1,0:T(8,128)(2,1)S(1)} %slice.326), channel_id=1, source_target_pairs={{0,1},{1,2},{2,3},{3,0},{4,5},{5,6},{6,7},{7,4},{8,9},{9,10},{10,1... | collective-permute-start | bytes 1179656 | tf_op jit(solution)/shard_map/ppermute | solution.py:31
  77.2 9.0 %collective-permute-start.5 = (bf16[384,512]{1,0:T(8,128)(2,1)S(1)}, bf16[384,512]{1,0:T(8,128)(2,1)S(1)}, u32[]{:S(2)}, u32[]{:S(2)}) collective-permute-start(bf16[384,512]{1,0:T(8,128)(2,1)S(1)} %slice.323), channel_id=1, source_target_pairs={{0,3},{1,0},{2,1},{3,2},{4,7},{5,4},{6,5},{7,6},{8,11},{9,8},{10,9... | collective-permute-start | bytes 1179656 | tf_op jit(solution)/shard_map/ppermute | solution.py:31
  80.7 6.8 %copy-start.25 = (bf16[512,256]{1,0:T(8,128)(2,1)S(1)}, bf16[512,256]{1,0:T(8,128)(2,1)}, u32[]{:S(2)}) copy-start(bf16[512,256]{1,0:T(8,128)(2,1)} %get-tuple-element.105) | copy-start | bytes 786436
  81.2 6.8 %copy-start.15 = (bf16[512,256]{1,0:T(8,128)(2,1)S(1)}, bf16[512,256]{1,0:T(8,128)(2,1)}, u32[]{:S(2)}) copy-start(bf16[512,256]{1,0:T(8,128)(2,1)} %get-tuple-element.100) | copy-start | bytes 786436
  90.0 7.1 %copy-start.20 = (bf16[256,128]{1,0:T(8,128)(2,1)S(1)}, bf16[256,128]{1,0:T(8,128)(2,1)}, u32[]{:S(2)}) copy-start(bf16[256,128]{1,0:T(8,128)(2,1)} %pad_maximum_fusion.28.write_ref) | copy-start | bytes 196612
  90.8 13.3 %collective-permute-start.8 = (bf16[384,512]{1,0:T(8,128)(2,1)S(1)}, bf16[384,512]{1,0:T(8,128)(2,1)S(1)}, u32[]{:S(2)}, u32[]{:S(2)}) collective-permute-start(bf16[384,512]{1,0:T(8,128)(2,1)S(1)} %convolution_convert_fusion.8), channel_id=1, source_target_pairs={{0,1},{1,2},{2,3},{3,0},{4,5},{5,6},{6,7},{7,4},{8,9},{9,10},{10,1... | collective-permute-start | bytes 1179656 | tf_op jit(solution)/shard_map/ppermute | solution.py:31
  90.9 16.8 %collective-permute-start.9 = (bf16[384,512]{1,0:T(8,128)(2,1)S(1)}, bf16[384,512]{1,0:T(8,128)(2,1)S(1)}, u32[]{:S(2)}, u32[]{:S(2)}) collective-permute-start(bf16[384,512]{1,0:T(8,128)(2,1)S(1)} %convolution_convert_fusion.7), channel_id=1, source_target_pairs={{0,3},{1,0},{2,1},{3,2},{4,7},{5,4},{6,5},{7,6},{8,11},{9,8},{10,9... | collective-permute-start | bytes 1179656 | tf_op jit(solution)/shard_map/ppermute | solution.py:31
  94.6 15.0 %collective-permute-start.10 = (bf16[384,512]{1,0:T(8,128)(2,1)S(1)}, bf16[384,512]{1,0:T(8,128)(2,1)S(1)}, u32[]{:S(2)}, u32[]{:S(2)}) collective-permute-start(bf16[384,512]{1,0:T(8,128)(2,1)S(1)} %convolution_convert_fusion.6), channel_id=1, source_target_pairs={{0,2},{1,3},{2,0},{3,1},{4,6},{5,7},{6,4},{7,5},{8,10},{9,11},{10,... | collective-permute-start | bytes 1179656 | tf_op jit(solution)/shard_map/ppermute | solution.py:31
  112.7 21.5 %all-to-all-start.1 = ((bf16[32,12,512]{2,1,0:T(8,128)(2,1)}), bf16[32,12,512]{2,1,0:T(8,128)(2,1)}, u32[]{:S(2)}, u32[]{:S(2)}) async-start(bf16[32,12,512]{2,1,0:T(8,128)(2,1)} %reshape.177), calls=%async_computation.1 | async-start | bytes 1048576 | tf_op jit(solution)/shard_map/all_to_all | solution.py:43
  131.0 7.0 %copy-start.39 = (bf16[128,512]{1,0:T(8,128)(2,1)S(1)}, bf16[128,512]{1,0:T(8,128)(2,1)}, u32[]{:S(2)}) copy-start(bf16[128,512]{1,0:T(8,128)(2,1)} %param.15) | copy-start | bytes 393220
  135.8 2.3 collective-permute-start.11
  138.1 8.0 %collective-permute-start.13 = (bf16[128,512]{1,0:T(8,128)(2,1)S(1)}, bf16[128,512]{1,0:T(8,128)(2,1)S(1)}, u32[]{:S(2)}, u32[]{:S(2)}) collective-permute-start(bf16[128,512]{1,0:T(8,128)(2,1)S(1)} %fusion.88), channel_id=1, source_target_pairs={{0,2},{1,3},{2,0},{3,1},{4,6},{5,7},{6,4},{7,5},{8,10},{9,11},{10,... | collective-permute-start | bytes 393224 | tf_op jit(solution)/shard_map/ppermute | solution.py:31
  138.2 10.6 %copy-start.40 = (bf16[128,512]{1,0:T(8,128)(2,1)S(1)}, bf16[128,512]{1,0:T(8,128)(2,1)}, u32[]{:S(2)}) copy-start(bf16[128,512]{1,0:T(8,128)(2,1)} %param.23) | copy-start | bytes 393220
  138.2 10.6 %copy-start.41 = (bf16[128,512]{1,0:T(8,128)(2,1)S(1)}, bf16[128,512]{1,0:T(8,128)(2,1)}, u32[]{:S(2)}) copy-start(bf16[128,512]{1,0:T(8,128)(2,1)} %param.22) | copy-start | bytes 393220
  139.3 9.1 %collective-permute-start.14 = (bf16[128,512]{1,0:T(8,128)(2,1)S(1)}, bf16[128,512]{1,0:T(8,128)(2,1)S(1)}, u32[]{:S(2)}, u32[]{:S(2)}) collective-permute-start(bf16[128,512]{1,0:T(8,128)(2,1)S(1)} %fusion.88), channel_id=1, source_target_pairs={{0,1},{1,2},{2,3},{3,0},{4,5},{5,6},{6,7},{7,4},{8,9},{9,10},{10,1... | collective-permute-start | bytes 393224 | tf_op jit(solution)/shard_map/ppermute | solution.py:31
  141.2 7.4 %collective-permute-start.12 = (bf16[128,512]{1,0:T(8,128)(2,1)S(1)}, bf16[128,512]{1,0:T(8,128)(2,1)S(1)}, u32[]{:S(2)}, u32[]{:S(2)}) collective-permute-start(bf16[128,512]{1,0:T(8,128)(2,1)S(1)} %fusion.88), channel_id=1, source_target_pairs={{0,3},{1,0},{2,1},{3,2},{4,7},{5,4},{6,5},{7,6},{8,11},{9,8},{10,9... | collective-permute-start | bytes 393224 | tf_op jit(solution)/shard_map/ppermute | solution.py:31
  149.9 1.3 collective-permute-start.23
  150.1 4.7 %collective-permute-start.15 = (bf16[128,2048]{1,0:T(8,128)(2,1)S(1)}, bf16[128,2048]{1,0:T(8,128)(2,1)S(1)}, u32[]{:S(2)}, u32[]{:S(2)}) collective-permute-start(bf16[128,2048]{1,0:T(8,128)(2,1)S(1)} %pad_maximum_fusion.8), channel_id=1, source_target_pairs={{0,4},{4,0},{1,5},{5,1},{2,6},{6,2},{3,7},{7,3},{8,12},{12,8},{9,1... | collective-permute-start | bytes 1572872 | tf_op jit(solution)/shard_map/ppermute | solution.py:26
  154.8 17.7 %copy-start.12 = (bf16[256,256]{1,0:T(8,128)(2,1)}, bf16[256,256]{1,0:T(8,128)(2,1)S(1)}, u32[]{:S(2)}) copy-start(bf16[256,256]{1,0:T(8,128)(2,1)S(1)} %get-tuple-element.138.delta_start_ref) | copy-start | bytes 393220
  155.9 9.1 %collective-permute-start.16 = (bf16[8,64,256]{2,1,0:T(8,128)(2,1)S(1)}, bf16[8,64,256]{2,1,0:T(8,128)(2,1)S(1)}, u32[]{:S(2)}, u32[]{:S(2)}) collective-permute-start(bf16[8,64,256]{2,1,0:T(8,128)(2,1)S(1)} %bitcast.232), channel_id=1, source_target_pairs={{0,8},{8,16},{16,24},{24,0},{1,9},{9,17},{17,25},{25,1},{2,10},{10... | collective-permute-start | bytes 786440 | tf_op jit(solution)/shard_map/ppermute | solution.py:31
  157.1 9.2 %collective-permute-start.17 = (bf16[8,64,256]{2,1,0:T(8,128)(2,1)S(1)}, bf16[8,64,256]{2,1,0:T(8,128)(2,1)S(1)}, u32[]{:S(2)}, u32[]{:S(2)}) collective-permute-start(bf16[8,64,256]{2,1,0:T(8,128)(2,1)S(1)} %bitcast.231), channel_id=1, source_target_pairs={{0,24},{8,0},{16,8},{24,16},{1,25},{9,1},{17,9},{25,17},{2,26},{10... | collective-permute-start | bytes 786440 | tf_op jit(solution)/shard_map/ppermute | solution.py:31
  158.0 12.0 %collective-permute-start.18 = (bf16[8,64,256]{2,1,0:T(8,128)(2,1)S(1)}, bf16[8,64,256]{2,1,0:T(8,128)(2,1)S(1)}, u32[]{:S(2)}, u32[]{:S(2)}) collective-permute-start(bf16[8,64,256]{2,1,0:T(8,128)(2,1)S(1)} %bitcast.230), channel_id=1, source_target_pairs={{0,16},{8,24},{16,0},{24,8},{1,17},{9,25},{17,1},{25,9},{2,18},{10... | collective-permute-start | bytes 786440 | tf_op jit(solution)/shard_map/ppermute | solution.py:31
  161.5 22.0 %copy-start.32 = (bf16[2,16,2,8,128]{4,3,2,1,0:T(8,128)(2,1)S(1)}, bf16[2,16,2,8,128]{4,3,2,1,0:T(8,128)(2,1)}, u32[]{:S(2)}) copy-start(bf16[2,16,2,8,128]{4,3,2,1,0:T(8,128)(2,1)} %pad_maximum_fusion.25) | copy-start | bytes 393220
  161.5 21.9 %copy-start.35 = (bf16[2,16,8,128]{3,2,1,0:T(8,128)(2,1)S(1)}, bf16[2,16,8,128]{3,2,1,0:T(8,128)(2,1)}, u32[]{:S(2)}) copy-start(bf16[2,16,8,128]{3,2,1,0:T(8,128)(2,1)} %broadcast_in_dim.70) | copy-start | bytes 196612
  170.1 23.9 %copy-start.21 = (bf16[256,128]{1,0:T(8,128)(2,1)S(1)}, bf16[256,128]{1,0:T(8,128)(2,1)}, u32[]{:S(2)}) copy-start(bf16[256,128]{1,0:T(8,128)(2,1)} %pad_maximum_fusion.28.write_ref) | copy-start | bytes 196612
  170.2 11.1 %collective-permute-start.19 = (bf16[4,64,256]{2,1,0:T(8,128)(2,1)S(1)}, bf16[4,64,256]{2,1,0:T(8,128)(2,1)S(1)}, u32[]{:S(2)}, u32[]{:S(2)}) collective-permute-start(bf16[4,64,256]{2,1,0:T(8,128)(2,1)S(1)} %select_convert_fusion), channel_id=1, source_target_pairs={{0,128},{32,160},{64,192},{96,224},{128,0},{160,32},{192,64},{224,... | collective-permute-start | bytes 393224 | tf_op jit(solution)/shard_map/ppermute | solution.py:380
  181.4 11.0 %collective-permute-start.20 = (bf16[2,64,256]{2,1,0:T(8,128)(2,1)S(1)}, bf16[2,64,256]{2,1,0:T(8,128)(2,1)S(1)}, u32[]{:S(2)}, u32[]{:S(2)}) collective-permute-start(bf16[2,64,256]{2,1,0:T(8,128)(2,1)S(1)} %select_convert_fusion.1), channel_id=1, source_target_pairs={{0,64},{32,96},{64,0},{96,32},{128,192},{160,224},{192,128},{224,1... | collective-permute-start | bytes 196616 | tf_op jit(solution)/shard_map/ppermute | solution.py:380
  184.2 20.0 %all-to-all-start.2 = ((bf16[32,40,128]{2,1,0:T(8,128)(2,1)}), bf16[32,40,128]{2,1,0:T(8,128)(2,1)S(1)}, u32[]{:S(2)}, u32[]{:S(2)}) async-start(bf16[32,40,128]{2,1,0:T(8,128)(2,1)} %pad_maximum_fusion.20), calls=%async_computation.2 | async-start | bytes 655360 | tf_op jit(solution)/shard_map/all_to_all | solution.py:43
  192.5 20.0 %collective-permute-start.21 = (bf16[1,64,256]{2,1,0:T(8,128)(2,1)S(1)}, bf16[1,64,256]{2,1,0:T(8,128)(2,1)S(1)}, u32[]{:S(2)}, u32[]{:S(2)}) collective-permute-start(bf16[1,64,256]{2,1,0:T(8,128)(2,1)S(1)} %select_convert_fusion.2), channel_id=1, source_target_pairs={{0,32},{32,0},{64,96},{96,64},{128,160},{160,128},{192,224},{224,1... | collective-permute-start | bytes 98312 | tf_op jit(solution)/shard_map/ppermute | solution.py:380
  206.8 15.6 %all-to-all-start.3 = ((bf16[32,32,128]{2,1,0:T(8,128)(2,1)}), bf16[32,32,128]{2,1,0:T(8,128)(2,1)S(1)}, u32[]{:S(2)}, u32[]{:S(2)}) async-start(bf16[32,32,128]{2,1,0:T(8,128)(2,1)} %shard_map.197), calls=%async_computation.3 | async-start | bytes 524288 | tf_op jit(solution)/shard_map/all_to_all | solution.py:43
  212.5 13.2 %collective-permute-start.22 = (f32[32,256]{1,0:T(8,128)S(1)}, f32[32,256]{1,0:T(8,128)S(1)}, u32[]{:S(2)}, u32[]{:S(2)}) collective-permute-start(f32[32,256]{1,0:T(8,128)S(1)} %select_bitcast_fusion), channel_id=1, source_target_pairs={{0,4},{4,0},{1,5},{5,1},{2,6},{6,2},{3,7},{7,3},{8,12},{12,8},{9,1... | collective-permute-start | bytes 98312 | tf_op jit(solution)/shard_map/ppermute | solution.py:26
  225.7 1.6 collective-permute-start.24
  (39 other events, 130.4 us)
where the time goes:
time: 234 us; the launch traced here: 230 us
  waiting for transfers between devices  90.9 us (39%)
  starting transfers between devices  61.8 us (26%)
  other arithmetic  28.1 us (12%)
  matrix products  24.9 us (11%)
  local copies, waits for them, and re-layouts  18.4 us (8%)
  Pallas kernels  4.44 us (2%)
    ppermute x13, waiting for transfers between devices, ring(): return lax.ppermute(x, axis, [(i, (i + shift) % n) for i in range(n)])  46.9 us
    all_to_all x4, waiting for transfers between devices, exchange(): return lax.all_to_all(x, CHIPS, split_axis=0, concat_axis=0, tiled=True)  34 us
    all_to_all x4, starting transfers between devices, exchange(): return lax.all_to_all(x, CHIPS, split_axis=0, concat_axis=0, tiled=True)  33.5 us
    dot_general x44, matrix products, dot(): lax.dot_general(a, b, (((ca,), (cb,)), ((), ())), preferred_element_type=...  23.9 us
    ppermute x13, starting transfers between devices, ring(): return lax.ppermute(x, axis, [(i, (i + shift) % n) for i in range(n)])  20.5 us
    ppermute x3, waiting for transfers between devices, on_device(): got = lax.ppermute(away, SP[0], [(i, i ^ gap) for i in range(deep)])  8.57 us
    ppermute x3, starting transfers between devices, on_device(): got = lax.ppermute(away, SP[0], [(i, i ^ gap) for i in range(deep)])  5.88 us
  transfers between devices with their start and end apart: 29, of which 18 were waited for; matrix products, arithmetic and copies ran while one was open for 18% of the time, Pallas kernels for 2%

commit v1 on v0

--- a/solution.py
+++ b/solution.py
@@ -46,6 +46,93 @@
 def silu_parts(value):
     sigma = jax.nn.sigmoid(value)
     return (value * sigma, sigma * (1.0 + value * (1.0 - sigma)))
+
+
+def route_kernel(
+    core_ref, mine_ref, other_ref, tokens_ref, tokens_other_ref, sent_ref, spot_ref
+):
+    tokens = tokens_ref.shape[0] // 2
+    count = 2 * tokens
+    total = sent_ref.shape[0]
+    rows = spot_ref.shape[0] + 4
+    cap = rows // 2
+    experts = total // rows
+    core = core_ref[0]
+    table = jnp.concatenate([mine_ref[...], other_ref[...]], axis=1)
+    ids = table[0:2].astype(jnp.int32)
+    source = (lax.broadcasted_iota(jnp.int32, (1, count), 1) >= tokens).astype(jnp.int32)
+    expert_col = lax.broadcasted_iota(jnp.int32, (experts, count), 0)
+    named = [expert_col == ids[k : k + 1] for k in range(2)]
+    named_any = jnp.where(named[0] | named[1], 1.0, 0.0).astype(bf16)
+    earlier = lax.broadcasted_iota(jnp.int32, (count, count), 0)
+    later = lax.broadcasted_iota(jnp.int32, (count, count), 1)
+    ahead = jnp.where((earlier < later) & ((earlier >= tokens) | (later < tokens)), 1.0, 0.0)
+    before = dot(named_any, ahead.astype(bf16))
+    spots = []
+    factors = []
+    for k in range(2):
+        rank = jnp.sum(jnp.where(named[k], before, 0.0), axis=0, keepdims=True).astype(jnp.int32)
+        expert = ids[k : k + 1]
+        spot = jnp.where(
+            (expert & 1) == core, (expert >> 1) * (2 * rows) + source * cap + rank, -1
+        )
+        spot_ref[k : k + 1, :] = spot
+        spots.append(jnp.concatenate([spot, jnp.where(spot < 0, -1, spot + rows)], axis=1))
+        weight = table[2 + k : 3 + k]
+        factors.append(jnp.concatenate([jnp.ones_like(weight), weight], axis=1))
+    x_all = jnp.concatenate([tokens_ref[:tokens], tokens_other_ref[:tokens]], axis=0)
+    c_all = jnp.concatenate([tokens_ref[tokens:], tokens_other_ref[tokens:]], axis=0)
+    step = 64
+
+    def block(i, carry):
+        row = lax.broadcasted_iota(jnp.int32, (step, 2 * count), 0) + i * step
+        hits = [row == spots[k] for k in range(2)]
+        scale = jnp.sum(
+            jnp.where(hits[0], factors[0], 0.0) + jnp.where(hits[1], factors[1], 0.0),
+            axis=1,
+            keepdims=True,
+        )
+        pick = jnp.where(hits[0] | hits[1], 1.0, 0.0).astype(bf16)
+        made = dot(pick[:, :count], x_all) + dot(pick[:, count:], c_all)
+        sent_ref[pl.ds(pl.multiple_of(i * step, step), step), :] = (made * scale).astype(bf16)
+        return carry
+
+    lax.fori_loop(0, total // step, block, 0)
+
+
+def route(core, mine, other, both, both_other, chips, rows):
+    vmem = pl.BlockSpec(memory_space=pltpu.VMEM)
+    return pl.pallas_call(
+        route_kernel,
+        in_specs=[pl.BlockSpec(memory_space=pltpu.SMEM)] + [vmem] * 4,
+        out_shape=(
+            jax.ShapeDtypeStruct((chips * 2 * rows, both.shape[1]), bf16),
+            jax.ShapeDtypeStruct((rows - 4, both.shape[0]), jnp.int32),
+        ),
+    )(core.reshape(1), mine, other, both, both_other)
+
+
+def join_kernel(core_ref, mine_ref, got_ref, value_ref, write_ref, read_ref):
+    half = value_ref.shape[1] // 2
+    lead = core_ref[0] == 0
+    mine = mine_ref[...]
+    got = got_ref[...].astype(f32)
+    value_ref[:, :half] = jnp.where(lead, mine[:, :half], got[:, :half]).astype(bf16)
+    value_ref[:, half:] = jnp.where(lead, got[:, :half], mine[:, :half]).astype(bf16)
+    sums = (mine[:, half:] + got[:, half:]).astype(bf16)
+    write_ref[...] = sums[:, :STATE]
+    read_ref[...] = sums[:, STATE:]
+
+
+def join(core, mine, got):
+    rows, width = mine.shape
+    vmem = pl.BlockSpec(memory_space=pltpu.VMEM)
+    narrow = jax.ShapeDtypeStruct((rows, STATE), bf16)
+    return pl.pallas_call(
+        join_kernel,
+        in_specs=[pl.BlockSpec(memory_space=pltpu.SMEM), vmem, vmem],
+        out_shape=(jax.ShapeDtypeStruct((rows, 2 * (width - 2 * STATE)), bf16), narrow, narrow),
+    )(core.reshape(1), mine, got)
 
 
 def scan_kernel(msg_ref, out_ref, work_ref):
@@ -181,72 +268,52 @@
         left, right = a[:, : a.shape[1] // 2], a[:, a.shape[1] // 2 :]
         return jnp.where(first, left, right), jnp.where(first, right, left)
 
-    small = jnp.concatenate([routes.astype(f32), route_weight, decay_rate], axis=1)
+    small = jnp.concatenate([routes.T.astype(f32), route_weight.T, decay_rate.T], axis=0)
     small_other = swap(small)
-    input_other = swap(layer_input)
-    cotangent_other = swap(cotangent)
-
-    routes_row = jnp.concatenate([routes.T, small_other[:, 0:2].T.astype(jnp.int32)], axis=1)
-    weight_row = jnp.concatenate([route_weight.T, small_other[:, 2:4].T], axis=1)
-    count = 2 * tokens
-    token_row = lax.broadcasted_iota(jnp.int32, (1, count), 1)
-    source_row = (token_row >= tokens).astype(jnp.int32)
-    expert_col = lax.broadcasted_iota(jnp.int32, (experts, count), 0)
-    named = [expert_col == routes_row[k : k + 1] for k in range(2)]
-    named_any = (named[0] | named[1]).astype(bf16)
-    earlier = lax.broadcasted_iota(jnp.int32, (count, count), 0)
-    later = lax.broadcasted_iota(jnp.int32, (count, count), 1)
-    before_mask = ((earlier < later) & ((earlier < tokens) == (later < tokens))).astype(bf16)
-    before = dot(named_any, before_mask)
-    place = []
-    for k in range(2):
-        rank = jnp.sum(jnp.where(named[k], before, 0.0), axis=0, keepdims=True).astype(jnp.int32)
-        expert = routes_row[k : k + 1]
-        here = (expert & 1) == core
-        place.append(
-            (jnp.where(here, expert >> 1, -1), source_row * cap + rank)
-        )
-    out_col = lax.broadcasted_iota(jnp.int32, (chips * 2 * rows, 2 * count), 0)
-    pick = None
-    scale = None
-    for k in range(2):
-        chip, inner = place[k]
-        spot = jnp.where(chip < 0, -1, chip * (2 * rows) + inner)
-        spots = jnp.concatenate([spot, jnp.where(spot < 0, -1, spot + rows)], axis=1)
-        factor = jnp.concatenate([jnp.ones_like(weight_row[k : k + 1]), weight_row[k : k + 1]], axis=1)
-        hit = out_col == spots
-        part = jnp.where(hit, factor, 0.0)
-        pick = hit if pick is None else pick | hit
-        scale = part if scale is None else scale + part
-    scale = jnp.sum(scale, axis=1, keepdims=True)
-    stacked = jnp.concatenate([layer_input, input_other, cotangent, cotangent_other], axis=0)
-    sent = (dot(pick.astype(bf16), stacked) * scale).astype(bf16)
+    both = jnp.concatenate([layer_input, cotangent], axis=0)
+    sent, spot = route(core, small, small_other, both, swap(both), chips, rows)
     later_inputs = (gate_weight, up_weight, down_weight, heads_value, output_gate, mixer_saved)
-    later_inputs += (proj_weight, state_write, state_read, decay_rate, small_other)
+    later_inputs += (proj_weight, state_write, state_read, small, small_other)
     sent, later_inputs = lax.optimization_barrier((sent, later_inputs))
     gate_weight, up_weight, down_weight, heads_value, output_gate, mixer_saved = later_inputs[:6]
-    proj_weight, state_write, state_read, decay_rate, small_other = later_inputs[6:]
-
-    back_col = lax.broadcasted_iota(jnp.int32, (chips * rows, count), 0)
-    back = None
-    for k in range(2):
-        chip, inner = place[k]
-        hit = back_col == jnp.where(chip < 0, -1, chip * rows + inner)
-        back = hit if back is None else back | hit
-    back = back.astype(bf16)
+    proj_weight, state_write, state_read, small, small_other = later_inputs[6:]
+
+    spot_row = lax.broadcasted_iota(jnp.int32, (chips * 2 * rows, 2 * tokens), 0)
+    back = [
+        sum(
+            jnp.where((spot[k : k + 1] >= 0) & (spot_row == spot[k : k + 1] + j * rows), 1.0, 0.0)
+            for k in range(2)
+        ).astype(bf16)
+        for j in range(2)
+    ]
 
     active_gate, slope_gate = silu_parts(output_gate.astype(f32))
     saved = mixer_saved.astype(f32)
     gated = (saved * active_gate).astype(bf16)
     value_mine, value_send = halves(heads_value)
-    gated_mine, gated_send = halves(gated)
-    side = jnp.concatenate([value_send, gated_send, state_write, state_read], axis=1)
+    side = jnp.concatenate([value_send, state_write, state_read, gated], axis=1)
     side_other = swap(side)
+    slots = chips * rows
+    out_row = lax.broadcasted_iota(jnp.int32, (slots, 2 * slots), 0)
+    in_row = lax.broadcasted_iota(jnp.int32, (slots, 2 * slots), 1)
+    origin = out_row + out_row // rows * rows
+    sort_rows = [(origin + j * rows == in_row).astype(bf16) for j in range(2)]
+    place = lax.broadcasted_iota(jnp.int32, (2 * slots, slots), 0)
+    column = lax.broadcasted_iota(jnp.int32, (2 * slots, slots), 1)
+    target = column + column // rows * rows
+    spread_rows = [
+        (place == target + j * rows).astype(bf16) for j in range(2)
+    ]
+    maps = (sort_rows, spread_rows, back)
+    side_other, small, small_other, maps = lax.optimization_barrier(
+        (side_other, small, small_other, maps)
+    )
+    sort_rows, spread_rows, back = maps
     value = ordered(value_mine, side_other[:, :half])
-    gated_all = jnp.concatenate([gated_mine, side_other[:, half : 2 * half]], axis=0)
-    write = ordered(state_write, side_other[:, 2 * half : 2 * half + STATE])
-    read = ordered(state_read, side_other[:, 2 * half + STATE :])
-    rates = ordered(halves(decay_rate)[0], halves(small_other[:, 4:])[0])
+    gated_all = jnp.concatenate([gated, side_other[:, half + 2 * STATE :]], axis=0)
+    write = ordered(state_write, side_other[:, half : half + STATE])
+    read = ordered(state_read, side_other[:, half + STATE : half + 2 * STATE])
+    rates = ordered(halves(small[4:].T)[0], halves(small_other[4:].T)[0])
     cumul = jnp.cumsum(rates, axis=0)
     spread = (
         lax.broadcasted_iota(jnp.int32, (half_heads, half), 1) // HEAD_DIM
@@ -293,22 +360,16 @@
     ]
     proj = rolled(proj_weight)
     hid = gate_weight.shape[2]
-    slots = chips * rows
-
-    out_row = lax.broadcasted_iota(jnp.int32, (2 * slots, 2 * slots), 0)
-    in_row = lax.broadcasted_iota(jnp.int32, (2 * slots, 2 * slots), 1)
-    kind = (out_row >= slots).astype(jnp.int32)
-    slot = out_row - kind * slots
-    sort_rows = (slot + slot // rows * rows + kind * rows == in_row).astype(bf16)
-    sort_rows, sent = lax.optimization_barrier((sort_rows, sent))
     received = exchange(sent.reshape(chips, 2 * rows, width)).reshape(2 * slots, width)
-    sorted_rows = dot(sort_rows, received).astype(bf16)
-    from_low = ring(sorted_rows, 1)
-    from_up = ring(sorted_rows, -1)
-    input_far = ring(from_low[:slots], 1)
-    cotangent_far = ring(from_up[slots:], -1)
-    input_parts = [sorted_rows[:slots], from_up[:slots], input_far, from_low[:slots]]
-    cotangent_parts = [sorted_rows[slots:], from_up[slots:], cotangent_far, from_low[slots:]]
+    input_own, cotangent_own = (dot(a, received).astype(bf16) for a in sort_rows)
+    input_low = ring(input_own, 1)
+    cotangent_up = ring(cotangent_own, -1)
+    input_up = ring(input_own, -1)
+    cotangent_low = ring(cotangent_own, 1)
+    input_far = ring(input_low, 1)
+    cotangent_far = ring(cotangent_up, -1)
+    input_parts = [input_own, input_up, input_far, input_low]
+    cotangent_parts = [cotangent_own, cotangent_up, cotangent_far, cotangent_low]
     order = (0, 1, 3, 2)
     pre = sum(dot(input_parts[i], gate_up[i]) for i in order)
     hidden_grad = sum(dot(cotangent_parts[i], down[i], 1, 1) for i in order)
@@ -326,7 +387,10 @@
     partial = [dot(deltas, gate_up[i], 1, 1).astype(bf16) for i in range(n_tp)]
     returned = ring_reduce(partial, TP).astype(bf16)
     returned, deltas, hidden = lax.optimization_barrier((returned, deltas, hidden))
-    arrived = exchange(returned.reshape(chips, rows, width)).reshape(slots, width)
+    cut = width // 2
+    returned = dot(spread_rows[0], returned[:, :cut]) + dot(spread_rows[1], returned[:, cut:])
+    arrived = exchange(returned.astype(bf16).reshape(chips, 2 * rows, cut))
+    arrived = arrived.reshape(2 * slots, cut)
 
     both_grad = unrolled([dot(input_parts[i], deltas, 0, 0).astype(bf16) for i in range(n_tp)])
     gate_grad = jnp.concatenate([a[:, :hid] for a in both_grad], axis=0)[None]
@@ -335,7 +399,10 @@
         unrolled([dot(hidden, cotangent_parts[i], 0, 0).astype(bf16) for i in range(n_tp)]), axis=1
     )[None]
 
-    summed = dot(back, arrived, 0, 0)
+    arrived, gate_grad, up_grad, down_grad = lax.optimization_barrier(
+        (arrived, gate_grad, up_grad, down_grad)
+    )
+    summed = jnp.concatenate([dot(back[0], arrived, 0, 0), dot(back[1], arrived, 0, 0)], axis=1)
     summed_other = swap(summed[tokens:].astype(bf16)).astype(f32)
     layer_grad = (cotangent.astype(f32) + summed[:tokens] + summed_other).astype(bf16)
     grads = [layer_grad, ring(layer_grad, -1), ring(layer_grad, 2), ring(layer_grad, 1)]
@@ -354,17 +421,16 @@
     grad_all = jnp.concatenate([grad_mine, swap(grad_mine)], axis=0)
     proj_part = dot(grad_all, gated_all, 0, 0).astype(bf16)
     deep, wide = lax.axis_size(SP[0]), lax.axis_size(SP[1])
-    block = proj_part.shape[0] // chips
+    block = proj_part.shape[0] // chips // 2
     across = lax.axis_index(SP[1])
-    proj_part = jnp.stack(unrolled([
-        proj_part[i * quarter : (i + 1) * quarter].reshape(deep // n_tp, wide, block, half)
-        for i in range(n_tp)
-    ]))
+    pieces = proj_part.reshape(n_tp, deep // n_tp, wide, 2, block, width)
+    pieces = lax.dynamic_index_in_dim(pieces, core, 3, keepdims=False)
+    proj_part = jnp.stack(unrolled([pieces[i] for i in range(n_tp)]))
     proj_sum = ring_reduce(
         [
             lax.dynamic_index_in_dim(
                 proj_part, (across + i) & (wide - 1), 2, keepdims=False
-            ).reshape(deep, block, half)
+            ).reshape(deep, block, width)
             for i in range(wide)
         ],
         SP[1],
@@ -372,18 +438,16 @@
     scanned = scan_chunks(states_got)
     states_back = exchange(scanned)
     depth = lax.axis_index(SP[0])
-    gap = deep // 2
-    while gap:
+    gap = 1
+    while gap < deep:
         upper = (depth & gap) != 0
-        below, above = proj_sum[:gap], proj_sum[gap:]
+        pairs = proj_sum.reshape(-1, 2, block, width)
+        below, above = pairs[:, 0], pairs[:, 1]
         away = jnp.where(upper, below, above).astype(bf16)
         got = lax.ppermute(away, SP[0], [(i, i ^ gap) for i in range(deep)])
         proj_sum = jnp.where(upper, above, below) + got.astype(f32)
-        gap //= 2
-    proj_sum = proj_sum[0]
-    top, bottom = proj_sum[: block // 2], proj_sum[block // 2 :]
-    proj_mine = jnp.where(first, top, bottom)
-    proj_grad = ordered(proj_mine, swap(jnp.where(first, bottom, top)), axis=1)
+        gap *= 2
+    proj_grad = proj_sum[0]
 
     cumul_row = cumul.T
     common = dot(read, write, 1, 1)
@@ -409,16 +473,15 @@
         base,
     )
     outs_got = swap(outs_send)
-    value_out = ordered(outs_mine[:, :half].astype(bf16), outs_got[:, :half], axis=1)
-    sums = (outs_mine[:, half:] + outs_got[:, half:].astype(f32)).astype(bf16)
+    value_out, write_out, read_out = join(core, outs_mine, outs_got)
     return (
         gate_grad,
         up_grad,
         down_grad,
         proj_grad,
         value_out,
-        sums[:, :STATE],
-        sums[:, STATE:],
+        write_out,
+        read_out,
         outgate_grad,
     )
 

time: 234 us -> 224 us (0.957)
  waiting for transfers between devices: 90.9 us -> 66.6 us
  matrix products: 24.9 us -> 37.4 us
  Pallas kernels: 4.44 us -> 10.8 us
  other arithmetic: 28.1 us -> 23.7 us
    all_to_all x4, waiting for transfers between devices: 34 us -> 15.1 us  [exchange(): return lax.all_to_all(x, CHIPS, split_axis=0, concat_axis=0, tiled=True)]
    dot_general x44 -> x46, matrix products: 23.9 us -> 36.5 us  [dot(): lax.dot_general(a, b, (((ca,), (cb,)), ((), ())), preferred_element_type=...]
    pallas_call x0 -> x2, Pallas kernels: none -> 6.37 us  [the longest x1 4.7 us: route(): pl.pallas_call(route_kernel, in_specs=[pl.BlockSpec(memory_space=pltpu.SM...]
    ppermute x3, waiting for transfers between devices: 8.57 us -> 2.98 us  [on_device(): got = lax.ppermute(away, SP[0], [(i, i ^ gap) for i in range(deep)])]
    ppermute x3, starting transfers between devices: 5.88 us -> 9.47 us  [on_device(): got = lax.ppermute(away, SP[0], [(i, i ^ gap) for i in range(deep)])]
    unnamed x117 -> x145, local copies, waits for them, and re-layouts: 3.13 us -> 6.69 us
    select_n x6 -> x4, other arithmetic: 3.89 us -> 0.73 us  [ordered(): jnp.where(first, mine, other)]
    slice x4, local copies, waits for them, and re-layouts: 3.22 us -> 0.15 us  [on_device(): up_grad = jnp.concatenate([a[:, hid:] for a in both_grad], axis=0)[None]]
  transfers between devices with their start and end apart: 29 -> 29, of which waited for: 18 -> 18; matrix products, arithmetic and copies ran while one was open for 18% -> 27% of each run, Pallas kernels for 2% -> 2%
where the time goes in v1:
time: 224 us; the launch traced here: 220 us
  waiting for transfers between devices  66.6 us (30%)
  starting transfers between devices  61.4 us (27%)
  matrix products  37.4 us (17%)
  other arithmetic  23.7 us (11%)
  local copies, waits for them, and re-layouts  17.6 us (8%)
  Pallas kernels  10.8 us (5%)
    ppermute x15, waiting for transfers between devices, ring(): return lax.ppermute(x, axis, [(i, (i + shift) % n) for i in range(n)])  46.9 us
    dot_general x46, matrix products, dot(): lax.dot_general(a, b, (((ca,), (cb,)), ((), ())), preferred_element_type=...  36.5 us
    all_to_all x4, starting transfers between devices, exchange(): return lax.all_to_all(x, CHIPS, split_axis=0, concat_axis=0, tiled=True)  30.7 us
    ppermute x15, starting transfers between devices, ring(): return lax.ppermute(x, axis, [(i, (i + shift) % n) for i in range(n)])  19.8 us
    all_to_all x4, waiting for transfers between devices, exchange(): return lax.all_to_all(x, CHIPS, split_axis=0, concat_axis=0, tiled=True)  15.1 us
    ppermute x3, starting transfers between devices, on_device(): got = lax.ppermute(away, SP[0], [(i, i ^ gap) for i in range(deep)])  9.47 us
    unnamed x145, local copies, waits for them, and re-layouts  6.69 us
    pallas_call x1, Pallas kernels, route(): pl.pallas_call(route_kernel, in_specs=[pl.BlockSpec(memory_space=pltpu.SM...  4.7 us
  transfers between devices with their start and end apart: 29, of which 18 were waited for; matrix products, arithmetic and copies ran while one was open for 27% of the time, Pallas kernels for 2%

profile of v1, /device:TPU:4, one launch (start us, length us, event | category | flops | bytes accessed | tf_op | source)
XLA Modules:
  0.0 219.5 jit_solution(14600619873784816369)
XLA Ops:
  4.8 1.4 fusion.7
  9.9 4.7 %shard_map.197 = (bf16[768,512]{1,0:T(8,128)(2,1)}, s32[8,256]{1,0:T(8,128)}) custom-call(s32[1]{0:T(128)} %bitcast.core_ref, f32[12,128]{1,0:T(8,128)} %copy-done.61, f32[12,128]{1,0:T(8,128)} %copy-done.63, bf16[256,512]{1,0:T(8,128)(2,1)} %copy-done.34, bf16[256,512]{1,0:T(8,128)(2,1)} %copy-done.45), custom_call_target="tpu_custom_call" | custom-call | tf_op jit(solution)/shard_map/pallas_call | solution.py:105
  17.1 11.6 %all-to-all-start = ((bf16[32,24,512]{2,1,0:T(8,128)(2,1)}), bf16[32,24,512]{2,1,0:T(8,128)(2,1)}, u32[]{:S(2)}, u32[]{:S(2)}) async-start(bf16[32,24,512]{2,1,0:T(8,128)(2,1)} %bitcast.309), calls=%async_computation | async-start | bytes 1572864 | tf_op jit(solution)/shard_map/all_to_all | solution.py:43
  28.8 2.8 %dynamic-slice_bitcast_fusion.10 = (bf16[512,256]{1,0:T(8,128)(2,1)}, bf16[512,256]{1,0:T(8,128)(2,1)}, bf16[512,256]{1,0:T(8,128)(2,1)S(1)}, bf16[512,256]{1,0:...) fusion(bf16[4,512,256]{2,1,0:T(8,128)(2,1)} %bitcast.305, ...), kind=kLoop, calls=%fused_computation.181 | loop fusion | bytes 4194320 | tf_op jit(solution)/shard_map/jit(dynamic_index_in_dim)/squeeze | solution.py:343
  32.4 1.6 add_convert_fusion.1
  34.8 1.2 reduce-window.6
  44.5 7.4 %all-to-all-done = bf16[32,24,512]{2,1,0:T(8,128)(2,1)} async-done(((bf16[32,24,512]{2,1,0:T(8,128)(2,1)}), bf16[32,24,512]{2,1,0:T(8,128)(2,1)}, u32[]{:S(2)}, u32[]{:S(2)}) %all-to-all-start) | async-done | bytes 786464 | tf_op jit(solution)/shard_map/all_to_all | solution.py:43
  51.9 1.9 convolution_convert_fusion.9
  53.9 3.1 %collective-permute-start.6 = (bf16[384,512]{1,0:T(8,128)(2,1)S(1)}, bf16[384,512]{1,0:T(8,128)(2,1)S(1)}, u32[]{:S(2)}, u32[]{:S(2)}) collective-permute-start(bf16[384,512]{1,0:T(8,128)(2,1)S(1)} %convolution_convert_fusion.9), channel_id=1, source_target_pairs={{0,3},{1,0},{2,1},{3,2},{4,7},{5,4},{6,5},{7,6},{8,11},{9,8},{10,9... | collective-permute-start | bytes 1179656 | tf_op jit(solution)/shard_map/ppermute | solution.py:31
  56.9 1.8 convolution_convert_fusion.10
  58.7 3.3 %collective-permute-start.3 = (bf16[384,512]{1,0:T(8,128)(2,1)S(1)}, bf16[384,512]{1,0:T(8,128)(2,1)S(1)}, u32[]{:S(2)}, u32[]{:S(2)}) collective-permute-start(bf16[384,512]{1,0:T(8,128)(2,1)S(1)} %convolution_convert_fusion.10), channel_id=1, source_target_pairs={{0,3},{1,0},{2,1},{3,2},{4,7},{5,4},{6,5},{7,6},{8,11},{9,8},{10,9... | collective-permute-start | bytes 1179656 | tf_op jit(solution)/shard_map/ppermute | solution.py:31
  62.9 7.2 %collective-permute-done.7 = bf16[384,512]{1,0:T(8,128)(2,1)S(1)} collective-permute-done((bf16[384,512]{1,0:T(8,128)(2,1)S(1)}, bf16[384,512]{1,0:T(8,128)(2,1)S(1)}, u32[]{:S(2)}, u32[]{:S(2)}) %collective-permute-start.7) | collective-permute-done | bytes 393248 | tf_op jit(solution)/shard_map/ppermute | solution.py:31
  70.1 3.1 %collective-permute-done.3 = bf16[384,512]{1,0:T(8,128)(2,1)S(1)} collective-permute-done((bf16[384,512]{1,0:T(8,128)(2,1)S(1)}, bf16[384,512]{1,0:T(8,128)(2,1)S(1)}, u32[]{:S(2)}, u32[]{:S(2)}) %collective-permute-start.3) | collective-permute-done | bytes 393248 | tf_op jit(solution)/shard_map/ppermute | solution.py:31
  73.3 3.7 %collective-permute-start.5 = (bf16[384,512]{1,0:T(8,128)(2,1)S(1)}, bf16[384,512]{1,0:T(8,128)(2,1)S(1)}, u32[]{:S(2)}, u32[]{:S(2)}) collective-permute-start(bf16[384,512]{1,0:T(8,128)(2,1)S(1)} %collective-permute-done.3), channel_id=1, source_target_pairs={{0,3},{1,0},{2,1},{3,2},{4,7},{5,4},{6,5},{7,6},{8,11},{9,8},{10,9... | collective-permute-start | bytes 1179656 | tf_op jit(solution)/shard_map/ppermute | solution.py:31
  78.9 6.2 %collective-permute-done.8 = bf16[384,512]{1,0:T(8,128)(2,1)S(1)} collective-permute-done((bf16[384,512]{1,0:T(8,128)(2,1)S(1)}, bf16[384,512]{1,0:T(8,128)(2,1)S(1)}, u32[]{:S(2)}, u32[]{:S(2)}) %collective-permute-start.8) | collective-permute-done | bytes 393248 | tf_op jit(solution)/shard_map/ppermute | solution.py:31
  91.1 1.5 collective-permute-start.10
  93.5 1.7 copy.84
  95.1 1.8 fusion.158
  96.9 7.5 %collective-permute-done.11 = bf16[384,512]{1,0:T(8,128)(2,1)} collective-permute-done((bf16[384,512]{1,0:T(8,128)(2,1)}, bf16[384,512]{1,0:T(8,128)(2,1)}, u32[]{:S(2)}, u32[]{:S(2)}) %collective-permute-start.11) | collective-permute-done | bytes 393248 | tf_op jit(solution)/shard_map/ppermute | solution.py:31
  104.4 4.5 %collective-permute-done.10 = bf16[384,512]{1,0:T(8,128)(2,1)} collective-permute-done((bf16[384,512]{1,0:T(8,128)(2,1)}, bf16[384,512]{1,0:T(8,128)(2,1)}, u32[]{:S(2)}, u32[]{:S(2)}) %collective-permute-start.10) | collective-permute-done | bytes 393248 | tf_op jit(solution)/shard_map/ppermute | solution.py:31
  110.0 1.9 add_convert_fusion
  113.4 5.3 %all-to-all-start.1 = ((bf16[32,24,256]{2,1,0:T(8,128)(2,1)}), bf16[32,24,256]{2,1,0:T(8,128)(2,1)S(1)}, u32[]{:S(2)}, u32[]{:S(2)}) async-start(bf16[32,24,256]{2,1,0:T(8,128)(2,1)} %bitcast.304), calls=%async_computation.1 | async-start | bytes 786432 | tf_op jit(solution)/shard_map/all_to_all | solution.py:43
  118.8 1.5 fusion.2
  120.4 1.5 fusion.5
  128.9 4.1 %all-to-all-done.1 = bf16[32,24,256]{2,1,0:T(8,128)(2,1)S(1)} async-done(((bf16[32,24,256]{2,1,0:T(8,128)(2,1)}), bf16[32,24,256]{2,1,0:T(8,128)(2,1)S(1)}, u32[]{:S(2)}, u32[]{:S(2)}) %all-to-all-start.1) | async-done | bytes 393248 | tf_op jit(solution)/shard_map/all_to_all | solution.py:43
  133.0 1.3 fusion.156
  137.5 1.6 collective-permute-start.15
  139.1 1.6 collective-permute-start.13
  140.8 3.6 %collective-permute-done.14 = bf16[128,512]{0,1:T(8,128)(2,1)S(1)} collective-permute-done((bf16[128,512]{0,1:T(8,128)(2,1)S(1)}, bf16[128,512]{0,1:T(8,128)(2,1)S(1)}, u32[]{:S(2)}, u32[]{:S(2)}) %collective-permute-start.14) | collective-permute-done | bytes 131104 | tf_op jit(solution)/shard_map/ppermute | solution.py:31
  144.6 1.7 collective-permute-done.15
  150.8 5.7 %all-to-all-start.2 = ((bf16[32,40,128]{2,1,0:T(8,128)(2,1)}), bf16[32,40,128]{2,1,0:T(8,128)(2,1)S(1)}, u32[]{:S(2)}, u32[]{:S(2)}) async-start(bf16[32,40,128]{2,1,0:T(8,128)(2,1)} %pad_maximum_fusion.20), calls=%async_computation.2 | async-start | bytes 655360 | tf_op jit(solution)/shard_map/all_to_all | solution.py:43
  156.5 2.0 fusion.87
  158.5 1.9 fusion.88
  161.4 1.9 fusion.89
  164.5 1.7 convolution_convert_fusion
  167.3 2.4 %collective-permute-start.18 = (bf16[8,32,512]{2,1,0:T(8,128)(2,1)S(1)}, bf16[8,32,512]{2,1,0:T(8,128)(2,1)S(1)}, u32[]{:S(2)}, u32[]{:S(2)}) collective-permute-start(bf16[8,32,512]{2,1,0:T(8,128)(2,1)S(1)} %bitcast.313), channel_id=1, source_target_pairs={{0,24},{8,0},{16,8},{24,16},{1,25},{9,1},{17,9},{25,17},{2,26},{10... | collective-permute-start | bytes 786440 | tf_op jit(solution)/shard_map/ppermute | solution.py:31
  170.2 7.6 %collective-permute-done.19 = bf16[8,32,512]{2,1,0:T(8,128)(2,1)S(1)} collective-permute-done((bf16[8,32,512]{2,1,0:T(8,128)(2,1)S(1)}, bf16[8,32,512]{2,1,0:T(8,128)(2,1)S(1)}, u32[]{:S(2)}, u32[]{:S(2)}) %collective-permute-start.19) | collective-permute-done | bytes 262176 | tf_op jit(solution)/shard_map/ppermute | solution.py:31
  177.8 3.2 %collective-permute-done.18 = bf16[8,32,512]{2,1,0:T(8,128)(2,1)S(1)} collective-permute-done((bf16[8,32,512]{2,1,0:T(8,128)(2,1)S(1)}, bf16[8,32,512]{2,1,0:T(8,128)(2,1)S(1)}, u32[]{:S(2)}, u32[]{:S(2)}) %collective-permute-start.18) | collective-permute-done | bytes 262176 | tf_op jit(solution)/shard_map/ppermute | solution.py:31
  182.1 1.6 collective-permute-start.20
  184.7 3.0 %collective-permute-done.20 = bf16[4,32,512]{2,1,0:T(8,128)(2,1)S(1)} collective-permute-done((bf16[4,32,512]{2,1,0:T(8,128)(2,1)S(1)}, bf16[4,32,512]{2,1,0:T(8,128)(2,1)S(1)}, u32[]{:S(2)}, u32[]{:S(2)}) %collective-permute-start.20) | collective-permute-done | bytes 131104 | tf_op jit(solution)/shard_map/ppermute | solution.py:447
  187.7 2.5 %collective-permute-start.21 = (bf16[2,32,512]{2,1,0:T(8,128)(2,1)S(1)}, bf16[2,32,512]{2,1,0:T(8,128)(2,1)S(1)}, u32[]{:S(2)}, u32[]{:S(2)}) collective-permute-start(bf16[2,32,512]{2,1,0:T(8,128)(2,1)S(1)} %fusion.102), channel_id=1, source_target_pairs={{0,64},{32,96},{64,0},{96,32},{128,192},{160,224},{192,128},{224,1... | collective-permute-start | bytes 196616 | tf_op jit(solution)/shard_map/ppermute | solution.py:447
  191.2 1.8 shard_map.198
  193.0 8.0 %all-to-all-start.3 = ((bf16[32,32,128]{2,1,0:T(8,128)(2,1)}), bf16[32,32,128]{2,1,0:T(8,128)(2,1)S(1)}, u32[]{:S(2)}, u32[]{:S(2)}) async-start(bf16[32,32,128]{2,1,0:T(8,128)(2,1)} %shard_map.198), calls=%async_computation.3 | async-start | bytes 524288 | tf_op jit(solution)/shard_map/all_to_all | solution.py:43
  201.1 5.5 %collective-permute-start.22 = (bf16[1,32,512]{2,1,0:T(8,128)(2,1)S(1)}, bf16[1,32,512]{2,1,0:T(8,128)(2,1)S(1)}, u32[]{:S(2)}, u32[]{:S(2)}) collective-permute-start(bf16[1,32,512]{2,1,0:T(8,128)(2,1)S(1)} %fusion.112), channel_id=1, source_target_pairs={{0,128},{32,160},{64,192},{96,224},{128,0},{160,32},{192,64},{224,... | collective-permute-start | bytes 98312 | tf_op jit(solution)/shard_map/ppermute | solution.py:447
  206.7 2.0 concatenate.105.base_ref
  208.7 3.6 %all-to-all-done.3.back_ref = bf16[32,32,128]{2,1,0:T(8,128)(2,1)S(1)} async-done(((bf16[32,32,128]{2,1,0:T(8,128)(2,1)}), bf16[32,32,128]{2,1,0:T(8,128)(2,1)S(1)}, u32[]{:S(2)}, u32[]{:S(2)}) %all-to-all-start.3) | async-done | bytes 262176 | tf_op jit(solution)/shard_map/all_to_all | solution.py:43
  213.0 2.6 %shard_map.199 = (f32[128,512]{1,0:T(8,128)}, bf16[128,512]{1,0:T(8,128)(2,1)}) custom-call(s32[1]{0:T(128)} %bitcast.core_ref, bf16[32,32,128]{2,1,0:T(8,128)(2,1)} %copy-done.24, bf16[256,128]{1,0:T(8,128)(2,1)} %pad_maximum_fusion.28.write_ref, bf16[256,256]{1,0:T(8,128)(2,1)} %copy-done.22, bf16[256,256]{1,0:T(8,128)(2,1)} %copy-done.21, ...), custom_call_target="tpu_custom_call" | custom-call | tf_op jit(solution)/shard_map/pallas_call | solution.py:213
  217.9 1.7 shard_map.200
  (290 shorter events, 56.7 us)
Async XLA Ops:
  0.6 143.7 %copy-start = (bf16[2048,512]{1,0:T(8,128)(2,1)S(1)}, bf16[2048,512]{1,0:T(8,128)(2,1)}, u32[]{:S(2)}) copy-start(bf16[2048,512]{1,0:T(8,128)(2,1)} %param.24) | copy-start | bytes 6291460
  0.6 14.9 %copy-start.36 = (bf16[128,512]{1,0:T(8,128)(2,1)S(1)}, bf16[128,512]{1,0:T(8,128)(2,1)}, u32[]{:S(2)}) copy-start(bf16[128,512]{1,0:T(8,128)(2,1)} %param.21) | copy-start | bytes 393220
  0.7 13.9 %copy-start.49 = (bf16[128,512]{1,0:T(8,128)(2,1)S(1)}, bf16[128,512]{1,0:T(8,128)(2,1)}, u32[]{:S(2)}) copy-start(bf16[128,512]{1,0:T(8,128)(2,1)} %param.23) | copy-start | bytes 393220
  0.7 14.9 %copy-start.57 = (bf16[128,128]{1,0:T(8,128)(2,1)S(1)}, bf16[128,128]{1,0:T(8,128)(2,1)}, u32[]{:S(2)}) copy-start(bf16[128,128]{1,0:T(8,128)(2,1)} %param.25) | copy-start | bytes 98308
  0.7 14.9 %copy-start.55 = (bf16[128,128]{1,0:T(8,128)(2,1)S(1)}, bf16[128,128]{1,0:T(8,128)(2,1)}, u32[]{:S(2)}) copy-start(bf16[128,128]{1,0:T(8,128)(2,1)} %param.26) | copy-start | bytes 98308
  2.3 6.9 %collective-permute-start = (f32[12,128]{1,0:T(8,128)S(1)}, f32[12,128]{1,0:T(8,128)S(1)}, u32[]{:S(2)}, u32[]{:S(2)}) collective-permute-start(f32[12,128]{1,0:T(8,128)S(1)} %pad_maximum_fusion.30.mine_ref), channel_id=1, source_target_pairs={{0,4},{4,0},{1,5},{5,1},{2,6},{6,2},{3,7},{7,3},{8,12},{12,8},{9,1... | collective-permute-start | bytes 18440 | tf_op jit(solution)/shard_map/ppermute | solution.py:26
  4.2 4.9 %collective-permute-start.1 = (bf16[256,512]{1,0:T(8,128)(2,1)S(1)}, bf16[256,512]{1,0:T(8,128)(2,1)S(1)}, u32[]{:S(2)}, u32[]{:S(2)}) collective-permute-start(bf16[256,512]{1,0:T(8,128)(2,1)S(1)} %constant_dynamic-update-slice_fusion.tokens_ref), channel_id=1, source_target_pairs={{0,4},{4,0},{1,5},{5,1},{2,6},{6,2},{3,7},{7,3},{8,12},{12,8},{9,1... | collective-permute-start | bytes 786440 | tf_op jit(solution)/shard_map/ppermute | solution.py:26
  16.3 17.7 %collective-permute-start.2 = (bf16[128,1024]{1,0:T(8,128)(2,1)}, bf16[128,1024]{1,0:T(8,128)(2,1)S(1)}, u32[]{:S(2)}, u32[]{:S(2)}) collective-permute-start(bf16[128,1024]{1,0:T(8,128)(2,1)} %pad_maximum_fusion.22), channel_id=1, source_target_pairs={{0,4},{4,0},{1,5},{5,1},{2,6},{6,2},{3,7},{7,3},{8,12},{12,8},{9,1... | collective-permute-start | bytes 786440 | tf_op jit(solution)/shard_map/ppermute | solution.py:26
  17.1 34.8 %all-to-all-start = ((bf16[32,24,512]{2,1,0:T(8,128)(2,1)}), bf16[32,24,512]{2,1,0:T(8,128)(2,1)}, u32[]{:S(2)}, u32[]{:S(2)}) async-start(bf16[32,24,512]{2,1,0:T(8,128)(2,1)} %bitcast.309), calls=%async_computation | async-start | bytes 1572864 | tf_op jit(solution)/shard_map/all_to_all | solution.py:43
  31.6 45.3 %copy-start.25 = (bf16[512,256]{1,0:T(8,128)(2,1)}, bf16[512,256]{1,0:T(8,128)(2,1)S(1)}, u32[]{:S(2)}) copy-start(bf16[512,256]{1,0:T(8,128)(2,1)S(1)} %get-tuple-element.133) | copy-start | bytes 786436
  40.7 108.7 %copy-start.2 = (f32[256,256]{1,0:T(8,128)}, f32[256,256]{1,0:T(8,128)S(1)}, u32[]{:S(2)}) copy-start(f32[256,256]{1,0:T(8,128)S(1)} %get-tuple-element.88.fade_end_ref) | copy-start | bytes 786436
  53.8 23.1 %copy-start.27 = (bf16[512,256]{1,0:T(8,128)(2,1)S(1)}, bf16[512,256]{1,0:T(8,128)(2,1)}, u32[]{:S(2)}) copy-start(bf16[512,256]{1,0:T(8,128)(2,1)} %get-tuple-element.186) | copy-start | bytes 786436
  53.9 23.1 %collective-permute-start.6 = (bf16[384,512]{1,0:T(8,128)(2,1)S(1)}, bf16[384,512]{1,0:T(8,128)(2,1)S(1)}, u32[]{:S(2)}, u32[]{:S(2)}) collective-permute-start(bf16[384,512]{1,0:T(8,128)(2,1)S(1)} %convolution_convert_fusion.9), channel_id=1, source_target_pairs={{0,3},{1,0},{2,1},{3,2},{4,7},{5,4},{6,5},{7,6},{8,11},{9,8},{10,9... | collective-permute-start | bytes 1179656 | tf_op jit(solution)/shard_map/ppermute | solution.py:31
  56.9 13.2 %collective-permute-start.7 = (bf16[384,512]{1,0:T(8,128)(2,1)S(1)}, bf16[384,512]{1,0:T(8,128)(2,1)S(1)}, u32[]{:S(2)}, u32[]{:S(2)}) collective-permute-start(bf16[384,512]{1,0:T(8,128)(2,1)S(1)} %convolution_convert_fusion.9), channel_id=1, source_target_pairs={{0,1},{1,2},{2,3},{3,0},{4,5},{5,6},{6,7},{7,4},{8,9},{9,10},{10,1... | collective-permute-start | bytes 1179656 | tf_op jit(solution)/shard_map/ppermute | solution.py:31
  58.7 18.7 %copy-start.11 = (bf16[384,512]{1,0:T(8,128)(2,1)}, bf16[384,512]{1,0:T(8,128)(2,1)S(1)}, u32[]{:S(2)}) copy-start(bf16[384,512]{1,0:T(8,128)(2,1)S(1)} %convolution_convert_fusion.10) | copy-start | bytes 1179652
  58.7 14.5 %collective-permute-start.3 = (bf16[384,512]{1,0:T(8,128)(2,1)S(1)}, bf16[384,512]{1,0:T(8,128)(2,1)S(1)}, u32[]{:S(2)}, u32[]{:S(2)}) collective-permute-start(bf16[384,512]{1,0:T(8,128)(2,1)S(1)} %convolution_convert_fusion.10), channel_id=1, source_target_pairs={{0,3},{1,0},{2,1},{3,2},{4,7},{5,4},{6,5},{7,6},{8,11},{9,8},{10,9... | collective-permute-start | bytes 1179656 | tf_op jit(solution)/shard_map/ppermute | solution.py:31
  62.1 16.5 %collective-permute-start.4 = (bf16[384,512]{1,0:T(8,128)(2,1)S(1)}, bf16[384,512]{1,0:T(8,128)(2,1)S(1)}, u32[]{:S(2)}, u32[]{:S(2)}) collective-permute-start(bf16[384,512]{1,0:T(8,128)(2,1)S(1)} %convolution_convert_fusion.10), channel_id=1, source_target_pairs={{0,1},{1,2},{2,3},{3,0},{4,5},{5,6},{6,7},{7,4},{8,9},{9,10},{10,1... | collective-permute-start | bytes 1179656 | tf_op jit(solution)/shard_map/ppermute | solution.py:31
  62.4 15.1 %copy-start.28 = (bf16[512,256]{1,0:T(8,128)(2,1)S(1)}, bf16[512,256]{1,0:T(8,128)(2,1)}, u32[]{:S(2)}) copy-start(bf16[512,256]{1,0:T(8,128)(2,1)} %get-tuple-element.132) | copy-start | bytes 786436
  62.4 15.1 %copy-start.29 = (bf16[512,256]{1,0:T(8,128)(2,1)S(1)}, bf16[512,256]{1,0:T(8,128)(2,1)}, u32[]{:S(2)}) copy-start(bf16[512,256]{1,0:T(8,128)(2,1)} %get-tuple-element.187) | copy-start | bytes 786436
  70.1 15.0 %collective-permute-start.8 = (bf16[384,512]{1,0:T(8,128)(2,1)S(1)}, bf16[384,512]{1,0:T(8,128)(2,1)S(1)}, u32[]{:S(2)}, u32[]{:S(2)}) collective-permute-start(bf16[384,512]{1,0:T(8,128)(2,1)S(1)} %collective-permute-done.7), channel_id=1, source_target_pairs={{0,1},{1,2},{2,3},{3,0},{4,5},{5,6},{6,7},{7,4},{8,9},{9,10},{10,1... | collective-permute-start | bytes 1179656 | tf_op jit(solution)/shard_map/ppermute | solution.py:31
  73.3 12.3 %collective-permute-start.5 = (bf16[384,512]{1,0:T(8,128)(2,1)S(1)}, bf16[384,512]{1,0:T(8,128)(2,1)S(1)}, u32[]{:S(2)}, u32[]{:S(2)}) collective-permute-start(bf16[384,512]{1,0:T(8,128)(2,1)S(1)} %collective-permute-done.3), channel_id=1, source_target_pairs={{0,3},{1,0},{2,1},{3,2},{4,7},{5,4},{6,5},{7,6},{8,11},{9,8},{10,9... | collective-permute-start | bytes 1179656 | tf_op jit(solution)/shard_map/ppermute | solution.py:31
  90.5 13.8 %collective-permute-start.11 = (bf16[384,512]{1,0:T(8,128)(2,1)}, bf16[384,512]{1,0:T(8,128)(2,1)}, u32[]{:S(2)}, u32[]{:S(2)}) collective-permute-start(bf16[384,512]{1,0:T(8,128)(2,1)} %convolution_convert_fusion.5), channel_id=1, source_target_pairs={{0,2},{1,3},{2,0},{3,1},{4,6},{5,7},{6,4},{7,5},{8,10},{9,11},{10,... | collective-permute-start | bytes 1179656 | tf_op jit(solution)/shard_map/ppermute | solution.py:31
  91.1 17.8 %collective-permute-start.10 = (bf16[384,512]{1,0:T(8,128)(2,1)}, bf16[384,512]{1,0:T(8,128)(2,1)}, u32[]{:S(2)}, u32[]{:S(2)}) collective-permute-start(bf16[384,512]{1,0:T(8,128)(2,1)} %convolution_convert_fusion.6), channel_id=1, source_target_pairs={{0,3},{1,0},{2,1},{3,2},{4,7},{5,4},{6,5},{7,6},{8,11},{9,8},{10,9... | collective-permute-start | bytes 1179656 | tf_op jit(solution)/shard_map/ppermute | solution.py:31
  92.6 17.4 %collective-permute-start.9 = (bf16[384,512]{1,0:T(8,128)(2,1)}, bf16[384,512]{1,0:T(8,128)(2,1)}, u32[]{:S(2)}, u32[]{:S(2)}) collective-permute-start(bf16[384,512]{1,0:T(8,128)(2,1)} %convolution_convert_fusion.7), channel_id=1, source_target_pairs={{0,1},{1,2},{2,3},{3,0},{4,5},{5,6},{6,7},{7,4},{8,9},{9,10},{10,1... | collective-permute-start | bytes 1179656 | tf_op jit(solution)/shard_map/ppermute | solution.py:31
  96.9 15.4 %copy-start.1 = (bf16[768,384]{1,0:T(8,128)(2,1)S(1)}, bf16[768,384]{1,0:T(8,128)(2,1)}, u32[]{:S(2)}) copy-start(bf16[768,384]{1,0:T(8,128)(2,1)} %get-tuple-element.64) | copy-start | bytes 1769476
  113.4 19.6 %all-to-all-start.1 = ((bf16[32,24,256]{2,1,0:T(8,128)(2,1)}), bf16[32,24,256]{2,1,0:T(8,128)(2,1)S(1)}, u32[]{:S(2)}, u32[]{:S(2)}) async-start(bf16[32,24,256]{2,1,0:T(8,128)(2,1)} %bitcast.304), calls=%async_computation.1 | async-start | bytes 786432 | tf_op jit(solution)/shard_map/all_to_all | solution.py:43
  134.7 1.4 collective-permute-start.12
  136.2 8.2 %collective-permute-start.14 = (bf16[128,512]{0,1:T(8,128)(2,1)S(1)}, bf16[128,512]{0,1:T(8,128)(2,1)S(1)}, u32[]{:S(2)}, u32[]{:S(2)}) collective-permute-start(bf16[128,512]{0,1:T(8,128)(2,1)S(1)} %fusion.70), channel_id=1, source_target_pairs={{0,2},{1,3},{2,0},{3,1},{4,6},{5,7},{6,4},{7,5},{8,10},{9,11},{10,... | collective-permute-start | bytes 393224 | tf_op jit(solution)/shard_map/ppermute | solution.py:31
  137.5 8.8 %collective-permute-start.15 = (bf16[128,512]{0,1:T(8,128)(2,1)S(1)}, bf16[128,512]{0,1:T(8,128)(2,1)S(1)}, u32[]{:S(2)}, u32[]{:S(2)}) collective-permute-start(bf16[128,512]{0,1:T(8,128)(2,1)S(1)} %fusion.70), channel_id=1, source_target_pairs={{0,1},{1,2},{2,3},{3,0},{4,5},{5,6},{6,7},{7,4},{8,9},{9,10},{10,1... | collective-permute-start | bytes 393224 | tf_op jit(solution)/shard_map/ppermute | solution.py:31
  139.1 7.5 %collective-permute-start.13 = (bf16[128,512]{0,1:T(8,128)(2,1)S(1)}, bf16[128,512]{0,1:T(8,128)(2,1)S(1)}, u32[]{:S(2)}, u32[]{:S(2)}) collective-permute-start(bf16[128,512]{0,1:T(8,128)(2,1)S(1)} %fusion.70), channel_id=1, source_target_pairs={{0,3},{1,0},{2,1},{3,2},{4,7},{5,4},{6,5},{7,6},{8,11},{9,8},{10,9... | collective-permute-start | bytes 393224 | tf_op jit(solution)/shard_map/ppermute | solution.py:31
  147.9 1.4 collective-permute-start.23
  148.9 15.6 %collective-permute-start.16 = (bf16[128,2048]{0,1:T(8,128)(2,1)}, bf16[128,2048]{0,1:T(8,128)(2,1)}, u32[]{:S(2)}, u32[]{:S(2)}) collective-permute-start(bf16[128,2048]{0,1:T(8,128)(2,1)} %pad_maximum_fusion.8), channel_id=1, source_target_pairs={{0,4},{4,0},{1,5},{5,1},{2,6},{6,2},{3,7},{7,3},{8,12},{12,8},{9,1... | collective-permute-start | bytes 1572872 | tf_op jit(solution)/shard_map/ppermute | solution.py:26
  149.5 13.9 %copy-start.19 = (bf16[256,256]{1,0:T(8,128)(2,1)}, bf16[256,256]{1,0:T(8,128)(2,1)S(1)}, u32[]{:S(2)}) copy-start(bf16[256,256]{1,0:T(8,128)(2,1)S(1)} %get-tuple-element.161.delta_end_ref) | copy-start | bytes 393220
  149.5 13.9 %copy-start.20 = (bf16[256,256]{1,0:T(8,128)(2,1)}, bf16[256,256]{1,0:T(8,128)(2,1)S(1)}, u32[]{:S(2)}) copy-start(bf16[256,256]{1,0:T(8,128)(2,1)S(1)} %get-tuple-element.162.delta_start_ref) | copy-start | bytes 393220
  150.0 14.5 %copy-start.41 = (bf16[128,512]{0,1:T(8,128)(2,1)S(1)}, bf16[128,512]{0,1:T(8,128)(2,1)}, u32[]{:S(2)}) copy-start(bf16[128,512]{0,1:T(8,128)(2,1)} %copy-done.40) | copy-start | bytes 393220
  150.8 39.6 %all-to-all-start.2 = ((bf16[32,40,128]{2,1,0:T(8,128)(2,1)}), bf16[32,40,128]{2,1,0:T(8,128)(2,1)S(1)}, u32[]{:S(2)}, u32[]{:S(2)}) async-start(bf16[32,40,128]{2,1,0:T(8,128)(2,1)} %pad_maximum_fusion.20), calls=%async_computation.2 | async-start | bytes 655360 | tf_op jit(solution)/shard_map/all_to_all | solution.py:43
  167.0 16.7 %copy-start.47 = (f32[256,256]{1,0:T(8,128)S(1)}, f32[256,256]{1,0:T(8,128)}, u32[]{:S(2)}) copy-start(f32[256,256]{1,0:T(8,128)} %fusion.158) | copy-start | bytes 786436
  167.0 10.8 %collective-permute-start.19 = (bf16[8,32,512]{2,1,0:T(8,128)(2,1)S(1)}, bf16[8,32,512]{2,1,0:T(8,128)(2,1)S(1)}, u32[]{:S(2)}, u32[]{:S(2)}) collective-permute-start(bf16[8,32,512]{2,1,0:T(8,128)(2,1)S(1)} %bitcast.314), channel_id=1, source_target_pairs={{0,16},{8,24},{16,0},{24,8},{1,17},{9,25},{17,1},{25,9},{2,18},{10... | collective-permute-start | bytes 786440 | tf_op jit(solution)/shard_map/ppermute | solution.py:31
  167.3 13.7 %collective-permute-start.18 = (bf16[8,32,512]{2,1,0:T(8,128)(2,1)S(1)}, bf16[8,32,512]{2,1,0:T(8,128)(2,1)S(1)}, u32[]{:S(2)}, u32[]{:S(2)}) collective-permute-start(bf16[8,32,512]{2,1,0:T(8,128)(2,1)S(1)} %bitcast.313), channel_id=1, source_target_pairs={{0,24},{8,0},{16,8},{24,16},{1,25},{9,1},{17,9},{25,17},{2,26},{10... | collective-permute-start | bytes 786440 | tf_op jit(solution)/shard_map/ppermute | solution.py:31
  169.7 12.2 %collective-permute-start.17 = (bf16[8,32,512]{2,1,0:T(8,128)(2,1)S(1)}, bf16[8,32,512]{2,1,0:T(8,128)(2,1)S(1)}, u32[]{:S(2)}, u32[]{:S(2)}) collective-permute-start(bf16[8,32,512]{2,1,0:T(8,128)(2,1)S(1)} %bitcast.312), channel_id=1, source_target_pairs={{0,8},{8,16},{16,24},{24,0},{1,9},{9,17},{17,25},{25,1},{2,10},{10... | collective-permute-start | bytes 786440 | tf_op jit(solution)/shard_map/ppermute | solution.py:31
  182.1 24.5 %copy-start.23 = (bf16[256,128]{1,0:T(8,128)(2,1)S(1)}, bf16[256,128]{1,0:T(8,128)(2,1)}, u32[]{:S(2)}) copy-start(bf16[256,128]{1,0:T(8,128)(2,1)} %pad_maximum_fusion.28.write_ref) | copy-start | bytes 196612
  182.1 24.6 %copy-start.52 = (f32[256,64]{1,0:T(8,128)S(1)}, f32[256,64]{1,0:T(8,128)}, u32[]{:S(2)}) copy-start(f32[256,64]{1,0:T(8,128)} %fusion.87) | copy-start | bytes 196612
  182.1 24.6 %copy-start.53 = (f32[256,64]{1,0:T(8,128)S(1)}, f32[256,64]{1,0:T(8,128)}, u32[]{:S(2)}) copy-start(f32[256,64]{1,0:T(8,128)} %fusion.88) | copy-start | bytes 196612
  182.1 5.5 %collective-permute-start.20 = (bf16[4,32,512]{2,1,0:T(8,128)(2,1)S(1)}, bf16[4,32,512]{2,1,0:T(8,128)(2,1)S(1)}, u32[]{:S(2)}, u32[]{:S(2)}) collective-permute-start(bf16[4,32,512]{2,1,0:T(8,128)(2,1)S(1)} %fusion.86), channel_id=1, source_target_pairs={{0,32},{32,0},{64,96},{96,64},{128,160},{160,128},{192,224},{224,1... | collective-permute-start | bytes 393224 | tf_op jit(solution)/shard_map/ppermute | solution.py:447
  187.7 13.3 %collective-permute-start.21 = (bf16[2,32,512]{2,1,0:T(8,128)(2,1)S(1)}, bf16[2,32,512]{2,1,0:T(8,128)(2,1)S(1)}, u32[]{:S(2)}, u32[]{:S(2)}) collective-permute-start(bf16[2,32,512]{2,1,0:T(8,128)(2,1)S(1)} %fusion.102), channel_id=1, source_target_pairs={{0,64},{32,96},{64,0},{96,32},{128,192},{160,224},{192,128},{224,1... | collective-permute-start | bytes 196616 | tf_op jit(solution)/shard_map/ppermute | solution.py:447
  193.0 19.4 %all-to-all-start.3 = ((bf16[32,32,128]{2,1,0:T(8,128)(2,1)}), bf16[32,32,128]{2,1,0:T(8,128)(2,1)S(1)}, u32[]{:S(2)}, u32[]{:S(2)}) async-start(bf16[32,32,128]{2,1,0:T(8,128)(2,1)} %shard_map.198), calls=%async_computation.3 | async-start | bytes 524288 | tf_op jit(solution)/shard_map/all_to_all | solution.py:43
  201.1 14.6 %collective-permute-start.22 = (bf16[1,32,512]{2,1,0:T(8,128)(2,1)S(1)}, bf16[1,32,512]{2,1,0:T(8,128)(2,1)S(1)}, u32[]{:S(2)}, u32[]{:S(2)}) collective-permute-start(bf16[1,32,512]{2,1,0:T(8,128)(2,1)S(1)} %fusion.112), channel_id=1, source_target_pairs={{0,128},{32,160},{64,192},{96,224},{128,0},{160,32},{192,64},{224,... | collective-permute-start | bytes 98312 | tf_op jit(solution)/shard_map/ppermute | solution.py:447
  215.7 1.6 collective-permute-start.24
  (53 other events, 258.0 us)

commit v2 on v1

--- a/solution.py
+++ b/solution.py
@@ -49,9 +49,9 @@
 
 
 def route_kernel(
-    core_ref, mine_ref, other_ref, tokens_ref, tokens_other_ref, sent_ref, spot_ref
+    core_ref, mine_ref, other_ref, x_ref, x_other_ref, c_ref, c_other_ref, sent_ref, spot_ref
 ):
-    tokens = tokens_ref.shape[0] // 2
+    tokens = x_ref.shape[0]
     count = 2 * tokens
     total = sent_ref.shape[0]
     rows = spot_ref.shape[0] + 4
@@ -80,9 +80,9 @@
         spots.append(jnp.concatenate([spot, jnp.where(spot < 0, -1, spot + rows)], axis=1))
         weight = table[2 + k : 3 + k]
         factors.append(jnp.concatenate([jnp.ones_like(weight), weight], axis=1))
-    x_all = jnp.concatenate([tokens_ref[:tokens], tokens_other_ref[:tokens]], axis=0)
-    c_all = jnp.concatenate([tokens_ref[tokens:], tokens_other_ref[tokens:]], axis=0)
-    step = 64
+    x_all = jnp.concatenate([x_ref[...], x_other_ref[...]], axis=0)
+    c_all = jnp.concatenate([c_ref[...], c_other_ref[...]], axis=0)
+    step = total // 4
 
     def block(i, carry):
         row = lax.broadcasted_iota(jnp.int32, (step, 2 * count), 0) + i * step
@@ -100,16 +100,104 @@
     lax.fori_loop(0, total // step, block, 0)
 
 
-def route(core, mine, other, both, both_other, chips, rows):
+def route(core, mine, other, x, x_other, c, c_other, chips, rows):
     vmem = pl.BlockSpec(memory_space=pltpu.VMEM)
     return pl.pallas_call(
         route_kernel,
-        in_specs=[pl.BlockSpec(memory_space=pltpu.SMEM)] + [vmem] * 4,
+        in_specs=[pl.BlockSpec(memory_space=pltpu.SMEM)] + [vmem] * 6,
         out_shape=(
-            jax.ShapeDtypeStruct((chips * 2 * rows, both.shape[1]), bf16),
-            jax.ShapeDtypeStruct((rows - 4, both.shape[0]), jnp.int32),
+            jax.ShapeDtypeStruct((chips * 2 * rows, x.shape[1]), bf16),
+            jax.ShapeDtypeStruct((rows - 4, 2 * x.shape[0]), jnp.int32),
         ),
-    )(core.reshape(1), mine, other, both, both_other)
+    )(core.reshape(1), mine, other, x, x_other, c, c_other)
+
+
+GROUP = 4
+ROWS = 24
+
+
+def split_kernel(got_ref, x_ref, c_ref):
+    slots = x_ref.shape[0]
+    part = x_ref.shape[0] // (got_ref.shape[0] // ROWS // GROUP)
+    out_row = lax.broadcasted_iota(jnp.int32, (2 * part, 2 * part), 0)
+    in_row = lax.broadcasted_iota(jnp.int32, (2 * part, 2 * part), 1)
+    kind = (out_row >= part).astype(jnp.int32)
+    slot = out_row - kind * part
+    rows = part // GROUP
+    chip = sum((slot >= k * rows).astype(jnp.int32) for k in range(1, GROUP))
+    perm = jnp.where(slot + chip * rows + kind * rows == in_row, 1.0, 0.0).astype(bf16)
+
+    def block(i, carry):
+        start = pl.multiple_of(i * 2 * part, 2 * part)
+        made = dot(perm, got_ref[pl.ds(start, 2 * part), :]).astype(bf16)
+        place = pl.multiple_of(i * part, part)
+        x_ref[pl.ds(place, part), :] = made[:part]
+        c_ref[pl.ds(place, part), :] = made[part:]
+        return carry
+
+    lax.fori_loop(0, slots // part, block, 0)
+
+
+def split(got):
+    shape = jax.ShapeDtypeStruct((got.shape[0] // 2, got.shape[1]), bf16)
+    return pl.pallas_call(split_kernel, out_shape=(shape, shape))(got)
+
+
+def spread_kernel(own_ref, low_ref, up_ref, far_ref, sent_ref):
+    slots, width = own_ref.shape
+    cut = width // 2
+    part = slots // (sent_ref.shape[0] // ROWS // GROUP)
+    out_row = lax.broadcasted_iota(jnp.int32, (2 * part, part), 0)
+    slot = lax.broadcasted_iota(jnp.int32, (2 * part, part), 1)
+    rows = part // GROUP
+    chip = sum((slot >= k * rows).astype(jnp.int32) for k in range(1, GROUP))
+    perms = [
+        jnp.where(slot + chip * rows + j * rows == out_row, 1.0, 0.0).astype(bf16)
+        for j in range(2)
+    ]
+
+    def block(i, carry):
+        here = pl.ds(pl.multiple_of(i * part, part), part)
+        total = own_ref[here, :].astype(f32) + low_ref[here, :].astype(f32)
+        total = total + up_ref[here, :].astype(f32) + far_ref[here, :].astype(f32)
+        total = total.astype(bf16)
+        made = dot(perms[0], total[:, :cut]) + dot(perms[1], total[:, cut:])
+        start = pl.multiple_of(i * 2 * part, 2 * part)
+        sent_ref[pl.ds(start, 2 * part), :] = made.astype(bf16)
+        return carry
+
+    lax.fori_loop(0, slots // part, block, 0)
+
+
+def spread(own, low, up, far):
+    shape = jax.ShapeDtypeStruct((2 * own.shape[0], own.shape[1] // 2), bf16)
+    return pl.pallas_call(spread_kernel, out_shape=shape)(own, low, up, far)
+
+
+def mix_kernel(delta_ref, value_ref, write_ref, read_ref, wide_ref, row_ref, base_ref):
+    half = value_ref.shape[1]
+    write = write_ref[...]
+    read = read_ref[...]
+    common = dot(write, read, 1, 1)
+    score = None
+    turned = None
+    for h in range(half // HEAD_DIM):
+        lanes = slice(h * HEAD_DIM, (h + 1) * HEAD_DIM)
+        mix = jnp.exp(-jnp.abs(wide_ref[:, h * HEAD_DIM : h * HEAD_DIM + 1] - row_ref[h : h + 1, :]))
+        delta = delta_ref[:, lanes]
+        value = value_ref[:, lanes]
+        base_ref[:, lanes] = dot((mix * common).astype(bf16), delta)
+        here = dot(delta, value, 1, 1) * mix
+        there = dot(value, delta, 1, 1) * mix
+        score = here if score is None else score + here
+        turned = there if turned is None else turned + there
+    base_ref[:, half : half + STATE] = dot(turned.astype(bf16), read)
+    base_ref[:, half + STATE :] = dot(score.astype(bf16), write)
+
+
+def mix_chunk(delta, value, write, read, wide, row):
+    shape = jax.ShapeDtypeStruct((value.shape[0], value.shape[1] + 2 * STATE), f32)
+    return pl.pallas_call(mix_kernel, out_shape=shape)(delta, value, write, read, wide, row)
 
 
 def join_kernel(core_ref, mine_ref, got_ref, value_ref, write_ref, read_ref):
@@ -270,8 +358,19 @@
 
     small = jnp.concatenate([routes.T.astype(f32), route_weight.T, decay_rate.T], axis=0)
     small_other = swap(small)
-    both = jnp.concatenate([layer_input, cotangent], axis=0)
-    sent, spot = route(core, small, small_other, both, swap(both), chips, rows)
+    input_other = swap(layer_input)
+    cotangent_other = swap(cotangent)
+    sent, spot = route(
+        core,
+        small,
+        small_other,
+        layer_input,
+        input_other,
+        cotangent,
+        cotangent_other,
+        chips,
+        rows,
+    )
     later_inputs = (gate_weight, up_weight, down_weight, heads_value, output_gate, mixer_saved)
     later_inputs += (proj_weight, state_write, state_read, small, small_other)
     sent, later_inputs = lax.optimization_barrier((sent, later_inputs))
@@ -294,32 +393,30 @@
     side = jnp.concatenate([value_send, state_write, state_read, gated], axis=1)
     side_other = swap(side)
     slots = chips * rows
-    out_row = lax.broadcasted_iota(jnp.int32, (slots, 2 * slots), 0)
-    in_row = lax.broadcasted_iota(jnp.int32, (slots, 2 * slots), 1)
-    origin = out_row + out_row // rows * rows
-    sort_rows = [(origin + j * rows == in_row).astype(bf16) for j in range(2)]
-    place = lax.broadcasted_iota(jnp.int32, (2 * slots, slots), 0)
-    column = lax.broadcasted_iota(jnp.int32, (2 * slots, slots), 1)
-    target = column + column // rows * rows
-    spread_rows = [
-        (place == target + j * rows).astype(bf16) for j in range(2)
-    ]
-    maps = (sort_rows, spread_rows, back)
-    side_other, small, small_other, maps = lax.optimization_barrier(
-        (side_other, small, small_other, maps)
-    )
-    sort_rows, spread_rows, back = maps
+    slots = chips * rows
+    side_other, small, small_other, back = lax.optimization_barrier(
+        (side_other, small, small_other, back)
+    )
     value = ordered(value_mine, side_other[:, :half])
     gated_all = jnp.concatenate([gated, side_other[:, half + 2 * STATE :]], axis=0)
     write = ordered(state_write, side_other[:, half : half + STATE])
     read = ordered(state_read, side_other[:, half + STATE : half + 2 * STATE])
-    rates = ordered(halves(small[4:].T)[0], halves(small_other[4:].T)[0])
-    cumul = jnp.cumsum(rates, axis=0)
-    spread = (
+    rates = ordered(
+        *(jnp.where(first, a[4 : 4 + half_heads], a[4 + half_heads :]) for a in (small, small_other)),
+        axis=1,
+    )
+    cumul_row = jnp.cumsum(rates, axis=1)
+    spread_heads = (
         lax.broadcasted_iota(jnp.int32, (half_heads, half), 1) // HEAD_DIM
         == lax.broadcasted_iota(jnp.int32, (half_heads, half), 0)
     ).astype(f32)
-    cumul_wide = jnp.dot(cumul, spread, precision=lax.Precision.HIGHEST)
+    cumul_wide = lax.dot_general(
+        cumul_row,
+        spread_heads,
+        (((0,), (0,)), ((), ())),
+        precision=lax.Precision.HIGHEST,
+        preferred_element_type=f32,
+    )
     total_wide = cumul_wide[-1:]
     fade_end = jnp.exp(cumul_wide - total_wide)
     fade_start = jnp.exp(-cumul_wide)
@@ -361,7 +458,7 @@
     proj = rolled(proj_weight)
     hid = gate_weight.shape[2]
     received = exchange(sent.reshape(chips, 2 * rows, width)).reshape(2 * slots, width)
-    input_own, cotangent_own = (dot(a, received).astype(bf16) for a in sort_rows)
+    input_own, cotangent_own = split(received)
     input_low = ring(input_own, 1)
     cotangent_up = ring(cotangent_own, -1)
     input_up = ring(input_own, -1)
@@ -379,17 +476,18 @@
     deltas = jnp.concatenate(
         [(hidden_grad * pre_up * slope).astype(bf16), (hidden_grad * active).astype(bf16)], axis=1
     )
-    ready = (write, read, value, gated_all, cumul, fade_end, fade_start, value_end, value_start)
-    ready += (write_states, total_rows)
+    ready = (write, read, value, gated_all, fade_end, fade_start, value_end, value_start)
+    ready += (write_states, total_rows, cumul_wide, cumul_row)
     deltas, ready = lax.optimization_barrier((deltas, ready))
-    write, read, value, gated_all, cumul, fade_end, fade_start, value_end, value_start = ready[:9]
-    write_states, total_rows = ready[9:]
+    write, read, value, gated_all, fade_end, fade_start, value_end, value_start = ready[:8]
+    write_states, total_rows, cumul_wide, cumul_row = ready[8:]
     partial = [dot(deltas, gate_up[i], 1, 1).astype(bf16) for i in range(n_tp)]
-    returned = ring_reduce(partial, TP).astype(bf16)
+    own, right, far, left = partial
+    opposite = ring(far, 2)
+    returned = spread(own, ring(right, 1), ring(left, -1), opposite)
     returned, deltas, hidden = lax.optimization_barrier((returned, deltas, hidden))
     cut = width // 2
-    returned = dot(spread_rows[0], returned[:, :cut]) + dot(spread_rows[1], returned[:, cut:])
-    arrived = exchange(returned.astype(bf16).reshape(chips, 2 * rows, cut))
+    arrived = exchange(returned.reshape(chips, 2 * rows, cut))
     arrived = arrived.reshape(2 * slots, cut)
 
     both_grad = unrolled([dot(input_parts[i], deltas, 0, 0).astype(bf16) for i in range(n_tp)])
@@ -449,18 +547,7 @@
         gap *= 2
     proj_grad = proj_sum[0]
 
-    cumul_row = cumul.T
-    common = dot(read, write, 1, 1)
-    score = None
-    value_parts = []
-    for h in range(half_heads):
-        mix = jnp.exp(-jnp.abs(cumul[:, h : h + 1] - cumul_row[h : h + 1]))
-        lanes = slice(h * HEAD_DIM, (h + 1) * HEAD_DIM)
-        match = dot(delta[:, lanes], value[:, lanes], 1, 1) * mix
-        score = match if score is None else score + match
-        value_parts.append(dot((mix * common).astype(bf16), delta[:, lanes], 0, 0))
-    score = score.astype(bf16)
-    base = jnp.concatenate(value_parts + [dot(score, read, 0, 0), dot(score, write)], axis=1)
+    base = mix_chunk(delta, value, write, read, cumul_wide, cumul_row)
     outs_mine, outs_send = tail(
         core,
         states_back,

time: 224 us -> 215 us (0.960)
  matrix products: 37.4 us -> 23.7 us
  Pallas kernels: 10.8 us -> 19.3 us
  other arithmetic: 23.7 us -> 18.3 us
  local copies, waits for them, and re-layouts: 17.6 us -> 12.7 us
  waiting for transfers between devices: 66.6 us -> 71 us
  starting transfers between devices: 61.4 us -> 64.6 us
    dot_general x46 -> x31, matrix products: 36.5 us -> 23.4 us  [dot(): lax.dot_general(a, b, (((ca,), (cb,)), ((), ())), preferred_element_type=...]
    pallas_call x0 -> x3, Pallas kernels: none -> 9.72 us  [the longest x1 3.57 us: spread(): return pl.pallas_call(spread_kernel, out_shape=shape)(own, low, up, far)]
    all_to_all x4, waiting for transfers between devices: 15.1 us -> 22 us  [exchange(): return lax.all_to_all(x, CHIPS, split_axis=0, concat_axis=0, tiled=True)]
    ppermute x3, waiting for transfers between devices: 2.98 us -> 0.01 us  [on_device(): got = lax.ppermute(away, SP[0], [(i, i ^ gap) for i in range(deep)])]
    concatenate x2 -> x0, local copies, waits for them, and re-layouts: 2.87 us -> none  [the longest x1 1.95 us: on_device(): jnp.concatenate(value_parts + [dot(score, read, 0, 0), dot(score, write)]...]
    convert_element_type x2 -> x0, other arithmetic: 2.6 us -> none  [the longest x1 1.4 us: on_device(): sort_rows = [(origin + j * rows == in_row).astype(bf16) for j in range(2)]]
    all_to_all x4, starting transfers between devices: 30.7 us -> 33.1 us  [exchange(): return lax.all_to_all(x, CHIPS, split_axis=0, concat_axis=0, tiled=True)]
    unnamed x145 -> x124, local copies, waits for them, and re-layouts: 6.69 us -> 7.49 us
  transfers between devices with their start and end apart: 29 -> 30, of which waited for: 18 -> 17; matrix products, arithmetic and copies ran while one was open for 27% -> 17% of each run, Pallas kernels for 2% -> 3%
where the time goes in v2:
time: 215 us; the launch traced here: 211 us
  waiting for transfers between devices  71 us (33%)
  starting transfers between devices  64.6 us (30%)
  matrix products  23.7 us (11%)
  Pallas kernels  19.3 us (9%)
  other arithmetic  18.3 us (9%)
  local copies, waits for them, and re-layouts  12.7 us (6%)
    ppermute x15, waiting for transfers between devices, ring(): return lax.ppermute(x, axis, [(i, (i + shift) % n) for i in range(n)])  46 us
    all_to_all x4, starting transfers between devices, exchange(): return lax.all_to_all(x, CHIPS, split_axis=0, concat_axis=0, tiled=True)  33.1 us
    dot_general x31, matrix products, dot(): lax.dot_general(a, b, (((ca,), (cb,)), ((), ())), preferred_element_type=...  23.4 us
    all_to_all x4, waiting for transfers between devices, exchange(): return lax.all_to_all(x, CHIPS, split_axis=0, concat_axis=0, tiled=True)  22 us
    ppermute x15, starting transfers between devices, ring(): return lax.ppermute(x, axis, [(i, (i + shift) % n) for i in range(n)])  21.5 us
    ppermute x3, starting transfers between devices, on_device(): got = lax.ppermute(away, SP[0], [(i, i ^ gap) for i in range(deep)])  8.45 us
    unnamed x124, local copies, waits for them, and re-layouts  7.49 us
  transfers between devices with their start and end apart: 30, of which 17 were waited for; matrix products, arithmetic and copies ran while one was open for 17% of the time, Pallas kernels for 3%

profile of v2, /device:TPU:4, one launch (start us, length us, event | category | flops | bytes accessed | tf_op | source)
XLA Modules:
  0.0 211.4 jit_solution(7272735539827650822)
XLA Ops:
  5.5 3.4 %shard_map.197 = (bf16[768,512]{1,0:T(8,128)(2,1)}, s32[8,256]{1,0:T(8,128)}) custom-call(s32[1]{0:T(128)} %bitcast.core_ref, f32[12,128]{1,0:T(8,128)} %copy-done.52, f32[12,128]{1,0:T(8,128)} %copy-done.54, bf16[128,512]{1,0:T(8,128)(2,1)} %x_ref.1, bf16[128,512]{1,0:T(8,128)(2,1)} %copy-done.45, bf16[128,512]{1,0:T(8,128)(2,1)} %c_ref.1, ...), custom_call_target="tpu_custom_call" | custom-call | tf_op jit(solution)/shard_map/pallas_call | solution.py:105
  8.9 11.7 %all-to-all-start = ((bf16[32,24,512]{2,1,0:T(8,128)(2,1)}), bf16[32,24,512]{2,1,0:T(8,128)(2,1)S(1)}, u32[]{:S(2)}, u32[]{:S(2)}) async-start(bf16[32,24,512]{2,1,0:T(8,128)(2,1)} %bitcast.279), calls=%async_computation | async-start | bytes 1572864 | tf_op jit(solution)/shard_map/all_to_all | solution.py:43
  21.0 2.8 %dynamic-slice_bitcast_fusion.10 = (bf16[512,256]{1,0:T(8,128)(2,1)}, bf16[512,256]{1,0:T(8,128)(2,1)}, bf16[512,256]{1,0:T(8,128)(2,1)}, bf16[512,256]{1,0:T(8,...) fusion(bf16[4,512,256]{2,1,0:T(8,128)(2,1)} %bitcast.275, ...), kind=kLoop, calls=%fused_computation.149 | loop fusion | bytes 4194320 | tf_op jit(solution)/shard_map/jit(dynamic_index_in_dim)/squeeze | solution.py:440
  23.9 1.6 add_convert_fusion
  26.2 1.2 reduce-window.6
  33.9 9.8 %all-to-all-done = bf16[32,24,512]{2,1,0:T(8,128)(2,1)S(1)} async-done(((bf16[32,24,512]{2,1,0:T(8,128)(2,1)}), bf16[32,24,512]{2,1,0:T(8,128)(2,1)S(1)}, u32[]{:S(2)}, u32[]{:S(2)}) %all-to-all-start) | async-done | bytes 786464 | tf_op jit(solution)/shard_map/all_to_all | solution.py:43
  44.6 3.3 %shard_map.198 = (bf16[384,512]{1,0:T(8,128)(2,1)}, bf16[384,512]{1,0:T(8,128)(2,1)}) custom-call(bf16[768,512]{1,0:T(8,128)(2,1)} %bitcast.271), custom_call_target="tpu_custom_call" | custom-call | tf_op jit(solution)/shard_map/pallas_call | solution.py:143
  47.8 3.0 %collective-permute-start.6 = (bf16[384,512]{1,0:T(8,128)(2,1)}, bf16[384,512]{1,0:T(8,128)(2,1)S(1)}, u32[]{:S(2)}, u32[]{:S(2)}) collective-permute-start(bf16[384,512]{1,0:T(8,128)(2,1)} %get-tuple-element.58), channel_id=1, source_target_pairs={{0,3},{1,0},{2,1},{3,2},{4,7},{5,4},{6,5},{7,6},{8,11},{9,8},{10,9... | collective-permute-start | bytes 1179656 | tf_op jit(solution)/shard_map/ppermute | solution.py:31
  50.9 3.2 %collective-permute-start.3 = (bf16[384,512]{1,0:T(8,128)(2,1)}, bf16[384,512]{1,0:T(8,128)(2,1)S(1)}, u32[]{:S(2)}, u32[]{:S(2)}) collective-permute-start(bf16[384,512]{1,0:T(8,128)(2,1)} %get-tuple-element.56), channel_id=1, source_target_pairs={{0,3},{1,0},{2,1},{3,2},{4,7},{5,4},{6,5},{7,6},{8,11},{9,8},{10,9... | collective-permute-start | bytes 1179656 | tf_op jit(solution)/shard_map/ppermute | solution.py:31
  54.1 1.4 fusion.66
  55.5 1.7 fusion.43
  57.2 7.1 %collective-permute-done.7 = bf16[384,512]{1,0:T(8,128)(2,1)S(1)} collective-permute-done((bf16[384,512]{1,0:T(8,128)(2,1)}, bf16[384,512]{1,0:T(8,128)(2,1)S(1)}, u32[]{:S(2)}, u32[]{:S(2)}) %collective-permute-start.7) | collective-permute-done | bytes 393248 | tf_op jit(solution)/shard_map/ppermute | solution.py:31
  64.3 2.8 %collective-permute-done.3 = bf16[384,512]{1,0:T(8,128)(2,1)S(1)} collective-permute-done((bf16[384,512]{1,0:T(8,128)(2,1)}, bf16[384,512]{1,0:T(8,128)(2,1)S(1)}, u32[]{:S(2)}, u32[]{:S(2)}) %collective-permute-start.3) | collective-permute-done | bytes 393248 | tf_op jit(solution)/shard_map/ppermute | solution.py:31
  67.1 3.6 %collective-permute-start.5 = (bf16[384,512]{1,0:T(8,128)(2,1)S(1)}, bf16[384,512]{1,0:T(8,128)(2,1)S(1)}, u32[]{:S(2)}, u32[]{:S(2)}) collective-permute-start(bf16[384,512]{1,0:T(8,128)(2,1)S(1)} %collective-permute-done.3), channel_id=1, source_target_pairs={{0,3},{1,0},{2,1},{3,2},{4,7},{5,4},{6,5},{7,6},{8,11},{9,8},{10,9... | collective-permute-start | bytes 1179656 | tf_op jit(solution)/shard_map/ppermute | solution.py:31
  73.0 5.8 %collective-permute-done.8 = bf16[384,512]{1,0:T(8,128)(2,1)S(1)} collective-permute-done((bf16[384,512]{1,0:T(8,128)(2,1)S(1)}, bf16[384,512]{1,0:T(8,128)(2,1)S(1)}, u32[]{:S(2)}, u32[]{:S(2)}) %collective-permute-start.8) | collective-permute-done | bytes 393248 | tf_op jit(solution)/shard_map/ppermute | solution.py:31
  80.8 1.2 convolution_convert_fusion.7
  82.0 1.2 convolution_convert_fusion.6
  83.1 1.2 convolution_convert_fusion.5
  84.3 3.2 %collective-permute-start.11 = (bf16[384,512]{1,0:T(8,128)(2,1)}, bf16[384,512]{1,0:T(8,128)(2,1)}, u32[]{:S(2)}, u32[]{:S(2)}) collective-permute-start(bf16[384,512]{1,0:T(8,128)(2,1)} %convolution_convert_fusion.6), channel_id=1, source_target_pairs={{0,3},{1,0},{2,1},{3,2},{4,7},{5,4},{6,5},{7,6},{8,11},{9,8},{10,9... | collective-permute-start | bytes 1179656 | tf_op jit(solution)/shard_map/ppermute | solution.py:31
  87.6 2.2 %convolution_convert_fusion.8.own_ref = bf16[384,512]{1,0:T(8,128)(2,1)} fusion(bf16[384,512]{0,1:T(8,128)(2,1)S(1)} %pad_maximum_fusion.9, bf16[512,256]{1,0:T(8,128)(2,1)} %get-tuple-element.132, bf16[512,256]{1,0:T(8,128)(2,1)} %get-tuple-element.169), kind=kOutput, calls=%fused_computation.12 | convolution fusion | flops 202571776 | bytes 1310720 | tf_op jit(solution)/shard_map/dot_general | solution.py:22
  89.7 13.2 %collective-permute-done.10.low_ref = bf16[384,512]{1,0:T(8,128)(2,1)S(1)} collective-permute-done((bf16[384,512]{1,0:T(8,128)(2,1)}, bf16[384,512]{1,0:T(8,128)(2,1)S(1)}, u32[]{:S(2)}, u32[]{:S(2)}) %collective-permute-start.10) | collective-permute-done | bytes 393248 | tf_op jit(solution)/shard_map/ppermute | solution.py:31
  103.8 3.6 %shard_map.199 = bf16[768,256]{1,0:T(8,128)(2,1)} custom-call(bf16[384,512]{1,0:T(8,128)(2,1)} %convolution_convert_fusion.8.own_ref, bf16[384,512]{1,0:T(8,128)(2,1)} %copy-done.40, bf16[384,512]{1,0:T(8,128)(2,1)} %collective-permute-done.11.up_ref, bf16[384,512]{1,0:T(8,128)(2,1)} %collective-permute-done.12.far_ref), custom_call_target="tpu_custom_call" | custom-call | tf_op jit(solution)/shard_map/pallas_call | solution.py:174
  107.3 5.7 %all-to-all-start.1 = ((bf16[32,24,256]{2,1,0:T(8,128)(2,1)}), bf16[32,24,256]{2,1,0:T(8,128)(2,1)S(1)}, u32[]{:S(2)}, u32[]{:S(2)}) async-start(bf16[32,24,256]{2,1,0:T(8,128)(2,1)} %bitcast.274), calls=%async_computation.1 | async-start | bytes 786432 | tf_op jit(solution)/shard_map/all_to_all | solution.py:43
  113.1 1.5 fusion
  114.6 1.5 fusion.3
  122.1 1.1 maximum_bitcast_fusion.2
  123.2 1.1 all-to-all-done.1
  124.3 1.3 fusion.107
  127.5 1.2 collective-permute-start.15
  128.7 2.4 %collective-permute-start.16 = (bf16[128,512]{0,1:T(8,128)(2,1)S(1)}, bf16[128,512]{0,1:T(8,128)(2,1)S(1)}, u32[]{:S(2)}, u32[]{:S(2)}) collective-permute-start(bf16[128,512]{0,1:T(8,128)(2,1)S(1)} %fusion.59), channel_id=1, source_target_pairs={{0,1},{1,2},{2,3},{3,0},{4,5},{5,6},{6,7},{7,4},{8,9},{9,10},{10,1... | collective-permute-start | bytes 393224 | tf_op jit(solution)/shard_map/ppermute | solution.py:31
  132.0 3.5 %collective-permute-done.15 = bf16[128,512]{0,1:T(8,128)(2,1)S(1)} collective-permute-done((bf16[128,512]{0,1:T(8,128)(2,1)S(1)}, bf16[128,512]{0,1:T(8,128)(2,1)S(1)}, u32[]{:S(2)}, u32[]{:S(2)}) %collective-permute-start.15) | collective-permute-done | bytes 131104 | tf_op jit(solution)/shard_map/ppermute | solution.py:31
  135.7 1.8 collective-permute-done.16
  138.1 2.0 fusion.46
  141.6 1.7 collective-permute-done.17
  143.4 1.9 convolution_convert_fusion
  146.0 2.0 collective-permute-start.20
  148.7 1.3 collective-permute-start.18
  150.5 6.3 %collective-permute-done.20 = bf16[8,32,512]{2,1,0:T(8,128)(2,1)S(1)} collective-permute-done((bf16[8,32,512]{2,1,0:T(8,128)(2,1)S(1)}, bf16[8,32,512]{2,1,0:T(8,128)(2,1)S(1)}, u32[]{:S(2)}, u32[]{:S(2)}) %collective-permute-start.20) | collective-permute-done | bytes 262176 | tf_op jit(solution)/shard_map/ppermute | solution.py:31
  156.8 4.1 %collective-permute-done.19 = bf16[8,32,512]{2,1,0:T(8,128)(2,1)S(1)} collective-permute-done((bf16[8,32,512]{2,1,0:T(8,128)(2,1)S(1)}, bf16[8,32,512]{2,1,0:T(8,128)(2,1)S(1)}, u32[]{:S(2)}, u32[]{:S(2)}) %collective-permute-start.19) | collective-permute-done | bytes 262176 | tf_op jit(solution)/shard_map/ppermute | solution.py:31
  163.3 8.8 %all-to-all-start.2 = ((bf16[32,40,128]{2,1,0:T(8,128)(2,1)}), bf16[32,40,128]{2,1,0:T(8,128)(2,1)S(1)}, u32[]{:S(2)}, u32[]{:S(2)}) async-start(bf16[32,40,128]{2,1,0:T(8,128)(2,1)} %pad_maximum_fusion.18), calls=%async_computation.2 | async-start | bytes 655360 | tf_op jit(solution)/shard_map/all_to_all | solution.py:43
  172.2 2.5 %collective-permute-start.22 = (bf16[2,32,512]{2,1,0:T(8,128)(2,1)S(1)}, bf16[2,32,512]{2,1,0:T(8,128)(2,1)S(1)}, u32[]{:S(2)}, u32[]{:S(2)}) collective-permute-start(bf16[2,32,512]{2,1,0:T(8,128)(2,1)S(1)} %fusion.76), channel_id=1, source_target_pairs={{0,64},{32,96},{64,0},{96,32},{128,192},{160,224},{192,128},{224,1... | collective-permute-start | bytes 196616 | tf_op jit(solution)/shard_map/ppermute | solution.py:545
  174.6 10.7 %all-to-all-done.2.msg_ref = bf16[32,40,128]{2,1,0:T(8,128)(2,1)S(1)} async-done(((bf16[32,40,128]{2,1,0:T(8,128)(2,1)}), bf16[32,40,128]{2,1,0:T(8,128)(2,1)S(1)}, u32[]{:S(2)}, u32[]{:S(2)}) %all-to-all-start.2) | async-done | bytes 327712 | tf_op jit(solution)/shard_map/all_to_all | solution.py:43
  186.0 1.8 shard_map.200
  187.8 6.9 %all-to-all-start.3 = ((bf16[32,32,128]{2,1,0:T(8,128)(2,1)}), bf16[32,32,128]{2,1,0:T(8,128)(2,1)S(1)}, u32[]{:S(2)}, u32[]{:S(2)}) async-start(bf16[32,32,128]{2,1,0:T(8,128)(2,1)} %shard_map.200), calls=%async_computation.3 | async-start | bytes 524288 | tf_op jit(solution)/shard_map/all_to_all | solution.py:43
  194.8 5.5 %collective-permute-start.23 = (bf16[1,32,512]{2,1,0:T(8,128)(2,1)S(1)}, bf16[1,32,512]{2,1,0:T(8,128)(2,1)S(1)}, u32[]{:S(2)}, u32[]{:S(2)}) collective-permute-start(bf16[1,32,512]{2,1,0:T(8,128)(2,1)S(1)} %fusion.78), channel_id=1, source_target_pairs={{0,128},{32,160},{64,192},{96,224},{128,0},{160,32},{192,64},{224,... | collective-permute-start | bytes 98312 | tf_op jit(solution)/shard_map/ppermute | solution.py:545
  200.9 2.9 %shard_map.201.base_ref = f32[256,512]{1,0:T(8,128)} custom-call(bf16[256,256]{1,0:T(8,128)(2,1)} %pad_maximum_fusion.24.delta_ref, bf16[256,256]{1,0:T(8,128)(2,1)} %pad_maximum_fusion.22.value_ref, bf16[256,128]{1,0:T(8,128)(2,1)} %get-tuple-element.89.write_ref, bf16[256,128]{1,0:T(8,128)(2,1)} %copy-done.20, f32[256,256]{1,0:T(8,128)} %copy-done.2, ...), custom_call_target="tpu_custom_call" | custom-call | tf_op jit(solution)/shard_map/pallas_call | solution.py:200
  204.9 2.6 %shard_map.202 = (f32[128,512]{1,0:T(8,128)}, bf16[128,512]{1,0:T(8,128)(2,1)}) custom-call(s32[1]{0:T(128)} %bitcast.core_ref, bf16[32,32,128]{2,1,0:T(8,128)(2,1)} %copy-done.19, bf16[256,128]{1,0:T(8,128)(2,1)} %get-tuple-element.89.write_ref, bf16[256,256]{1,0:T(8,128)(2,1)} %copy-done.18, bf16[256,256]{1,0:T(8,128)(2,1)} %copy-done.17, ...), custom_call_target="tpu_custom_call" | custom-call | tf_op jit(solution)/shard_map/pallas_call | solution.py:301
  209.7 1.7 shard_map.203
  (249 shorter events, 37.6 us)
Async XLA Ops:
  0.6 134.8 %copy-start = (bf16[2048,512]{1,0:T(8,128)(2,1)S(1)}, bf16[2048,512]{1,0:T(8,128)(2,1)}, u32[]{:S(2)}) copy-start(bf16[2048,512]{1,0:T(8,128)(2,1)} %param.24) | copy-start | bytes 6291460
  0.7 20.1 %copy-start.33 = (bf16[128,512]{1,0:T(8,128)(2,1)S(1)}, bf16[128,512]{1,0:T(8,128)(2,1)}, u32[]{:S(2)}) copy-start(bf16[128,512]{1,0:T(8,128)(2,1)} %param.21) | copy-start | bytes 393220
  0.7 20.0 %copy-start.44 = (bf16[128,512]{1,0:T(8,128)(2,1)S(1)}, bf16[128,512]{1,0:T(8,128)(2,1)}, u32[]{:S(2)}) copy-start(bf16[128,512]{1,0:T(8,128)(2,1)} %param.22) | copy-start | bytes 393220
  0.7 20.0 %copy-start.42 = (bf16[128,512]{1,0:T(8,128)(2,1)S(1)}, bf16[128,512]{1,0:T(8,128)(2,1)}, u32[]{:S(2)}) copy-start(bf16[128,512]{1,0:T(8,128)(2,1)} %param.23) | copy-start | bytes 393220
  0.7 20.1 %copy-start.49 = (bf16[128,128]{1,0:T(8,128)(2,1)S(1)}, bf16[128,128]{1,0:T(8,128)(2,1)}, u32[]{:S(2)}) copy-start(bf16[128,128]{1,0:T(8,128)(2,1)} %param.25) | copy-start | bytes 98308
  0.7 20.1 %copy-start.48 = (bf16[128,128]{1,0:T(8,128)(2,1)S(1)}, bf16[128,128]{1,0:T(8,128)(2,1)}, u32[]{:S(2)}) copy-start(bf16[128,128]{1,0:T(8,128)(2,1)} %param.26) | copy-start | bytes 98308
  2.2 2.5 %collective-permute-start = (f32[12,128]{1,0:T(8,128)S(1)}, f32[12,128]{1,0:T(8,128)S(1)}, u32[]{:S(2)}, u32[]{:S(2)}) collective-permute-start(f32[12,128]{1,0:T(8,128)S(1)} %pad_maximum_fusion.28.mine_ref), channel_id=1, source_target_pairs={{0,4},{4,0},{1,5},{5,1},{2,6},{6,2},{3,7},{7,3},{8,12},{12,8},{9,1... | collective-permute-start | bytes 18440 | tf_op jit(solution)/shard_map/ppermute | solution.py:26
  2.3 2.4 %collective-permute-start.1 = (bf16[128,512]{1,0:T(8,128)(2,1)}, bf16[128,512]{1,0:T(8,128)(2,1)S(1)}, u32[]{:S(2)}, u32[]{:S(2)}) collective-permute-start(bf16[128,512]{1,0:T(8,128)(2,1)} %x_ref.1), channel_id=1, source_target_pairs={{0,4},{4,0},{1,5},{5,1},{2,6},{6,2},{3,7},{7,3},{8,12},{12,8},{9,1... | collective-permute-start | bytes 393224 | tf_op jit(solution)/shard_map/ppermute | solution.py:26
  2.8 2.0 collective-permute-start.2
  8.9 12.0 %copy-start.58 = (s32[8,256]{1,0:T(8,128)S(1)}, s32[8,256]{1,0:T(8,128)}, u32[]{:S(2)}) copy-start(s32[8,256]{1,0:T(8,128)} %get-tuple-element.68) | copy-start | bytes 24580
  8.9 34.7 %all-to-all-start = ((bf16[32,24,512]{2,1,0:T(8,128)(2,1)}), bf16[32,24,512]{2,1,0:T(8,128)(2,1)S(1)}, u32[]{:S(2)}, u32[]{:S(2)}) async-start(bf16[32,24,512]{2,1,0:T(8,128)(2,1)} %bitcast.279), calls=%async_computation | async-start | bytes 1572864 | tf_op jit(solution)/shard_map/all_to_all | solution.py:43
  20.8 4.6 %collective-permute-start.9 = (bf16[128,1024]{1,0:T(8,128)(2,1)S(1)}, bf16[128,1024]{1,0:T(8,128)(2,1)S(1)}, u32[]{:S(2)}, u32[]{:S(2)}) collective-permute-start(bf16[128,1024]{1,0:T(8,128)(2,1)S(1)} %pad_maximum_fusion.20), channel_id=1, source_target_pairs={{0,4},{4,0},{1,5},{5,1},{2,6},{6,2},{3,7},{7,3},{8,12},{12,8},{9,1... | collective-permute-start | bytes 786440 | tf_op jit(solution)/shard_map/ppermute | solution.py:26
  28.8 19.1 %copy-start.2 = (f32[256,256]{1,0:T(8,128)}, f32[256,256]{1,0:T(8,128)S(1)}, u32[]{:S(2)}) copy-start(f32[256,256]{1,0:T(8,128)S(1)} %fusion.87.wide_ref) | copy-start | bytes 786436
  32.4 117.8 %copy-start.20 = (bf16[256,128]{1,0:T(8,128)(2,1)}, bf16[256,128]{1,0:T(8,128)(2,1)S(1)}, u32[]{:S(2)}) copy-start(bf16[256,128]{1,0:T(8,128)(2,1)S(1)} %get-tuple-element.83.read_ref) | copy-start | bytes 196612
  33.8 36.9 %copy-start.25 = (bf16[512,256]{1,0:T(8,128)(2,1)S(1)}, bf16[512,256]{1,0:T(8,128)(2,1)}, u32[]{:S(2)}) copy-start(bf16[512,256]{1,0:T(8,128)(2,1)} %get-tuple-element.131) | copy-start | bytes 786436
  47.8 22.9 %copy-start.27 = (bf16[512,256]{1,0:T(8,128)(2,1)S(1)}, bf16[512,256]{1,0:T(8,128)(2,1)}, u32[]{:S(2)}) copy-start(bf16[512,256]{1,0:T(8,128)(2,1)} %get-tuple-element.170) | copy-start | bytes 786436
  47.8 22.8 %collective-permute-start.6 = (bf16[384,512]{1,0:T(8,128)(2,1)}, bf16[384,512]{1,0:T(8,128)(2,1)S(1)}, u32[]{:S(2)}, u32[]{:S(2)}) collective-permute-start(bf16[384,512]{1,0:T(8,128)(2,1)} %get-tuple-element.58), channel_id=1, source_target_pairs={{0,3},{1,0},{2,1},{3,2},{4,7},{5,4},{6,5},{7,6},{8,11},{9,8},{10,9... | collective-permute-start | bytes 1179656 | tf_op jit(solution)/shard_map/ppermute | solution.py:31
  50.9 13.4 %collective-permute-start.7 = (bf16[384,512]{1,0:T(8,128)(2,1)}, bf16[384,512]{1,0:T(8,128)(2,1)S(1)}, u32[]{:S(2)}, u32[]{:S(2)}) collective-permute-start(bf16[384,512]{1,0:T(8,128)(2,1)} %get-tuple-element.58), channel_id=1, source_target_pairs={{0,1},{1,2},{2,3},{3,0},{4,5},{5,6},{6,7},{7,4},{8,9},{9,10},{10,1... | collective-permute-start | bytes 1179656 | tf_op jit(solution)/shard_map/ppermute | solution.py:31
  50.9 16.2 %collective-permute-start.3 = (bf16[384,512]{1,0:T(8,128)(2,1)}, bf16[384,512]{1,0:T(8,128)(2,1)S(1)}, u32[]{:S(2)}, u32[]{:S(2)}) collective-permute-start(bf16[384,512]{1,0:T(8,128)(2,1)} %get-tuple-element.56), channel_id=1, source_target_pairs={{0,3},{1,0},{2,1},{3,2},{4,7},{5,4},{6,5},{7,6},{8,11},{9,8},{10,9... | collective-permute-start | bytes 1179656 | tf_op jit(solution)/shard_map/ppermute | solution.py:31
  54.1 18.6 %collective-permute-start.4 = (bf16[384,512]{1,0:T(8,128)(2,1)}, bf16[384,512]{1,0:T(8,128)(2,1)S(1)}, u32[]{:S(2)}, u32[]{:S(2)}) collective-permute-start(bf16[384,512]{1,0:T(8,128)(2,1)} %get-tuple-element.56), channel_id=1, source_target_pairs={{0,1},{1,2},{2,3},{3,0},{4,5},{5,6},{6,7},{7,4},{8,9},{9,10},{10,1... | collective-permute-start | bytes 1179656 | tf_op jit(solution)/shard_map/ppermute | solution.py:31
  55.5 15.7 %copy-start.23 = (bf16[512,256]{1,0:T(8,128)(2,1)S(1)}, bf16[512,256]{1,0:T(8,128)(2,1)}, u32[]{:S(2)}) copy-start(bf16[512,256]{1,0:T(8,128)(2,1)} %get-tuple-element.130) | copy-start | bytes 786436
  55.5 15.7 %copy-start.24 = (bf16[512,256]{1,0:T(8,128)(2,1)S(1)}, bf16[512,256]{1,0:T(8,128)(2,1)}, u32[]{:S(2)}) copy-start(bf16[512,256]{1,0:T(8,128)(2,1)} %get-tuple-element.171) | copy-start | bytes 786436
  64.3 14.6 %collective-permute-start.8 = (bf16[384,512]{1,0:T(8,128)(2,1)S(1)}, bf16[384,512]{1,0:T(8,128)(2,1)S(1)}, u32[]{:S(2)}, u32[]{:S(2)}) collective-permute-start(bf16[384,512]{1,0:T(8,128)(2,1)S(1)} %collective-permute-done.7), channel_id=1, source_target_pairs={{0,1},{1,2},{2,3},{3,0},{4,5},{5,6},{6,7},{7,4},{8,9},{9,10},{10,1... | collective-permute-start | bytes 1179656 | tf_op jit(solution)/shard_map/ppermute | solution.py:31
  67.1 12.2 %collective-permute-start.5 = (bf16[384,512]{1,0:T(8,128)(2,1)S(1)}, bf16[384,512]{1,0:T(8,128)(2,1)S(1)}, u32[]{:S(2)}, u32[]{:S(2)}) collective-permute-start(bf16[384,512]{1,0:T(8,128)(2,1)S(1)} %collective-permute-done.3), channel_id=1, source_target_pairs={{0,3},{1,0},{2,1},{3,2},{4,7},{5,4},{6,5},{7,6},{8,11},{9,8},{10,9... | collective-permute-start | bytes 1179656 | tf_op jit(solution)/shard_map/ppermute | solution.py:31
  84.3 18.7 %collective-permute-start.10 = (bf16[384,512]{1,0:T(8,128)(2,1)}, bf16[384,512]{1,0:T(8,128)(2,1)S(1)}, u32[]{:S(2)}, u32[]{:S(2)}) collective-permute-start(bf16[384,512]{1,0:T(8,128)(2,1)} %convolution_convert_fusion.7), channel_id=1, source_target_pairs={{0,1},{1,2},{2,3},{3,0},{4,5},{5,6},{6,7},{7,4},{8,9},{9,10},{10,1... | collective-permute-start | bytes 1179656 | tf_op jit(solution)/shard_map/ppermute | solution.py:31
  84.3 18.7 %collective-permute-start.11 = (bf16[384,512]{1,0:T(8,128)(2,1)}, bf16[384,512]{1,0:T(8,128)(2,1)}, u32[]{:S(2)}, u32[]{:S(2)}) collective-permute-start(bf16[384,512]{1,0:T(8,128)(2,1)} %convolution_convert_fusion.6), channel_id=1, source_target_pairs={{0,3},{1,0},{2,1},{3,2},{4,7},{5,4},{6,5},{7,6},{8,11},{9,8},{10,9... | collective-permute-start | bytes 1179656 | tf_op jit(solution)/shard_map/ppermute | solution.py:31
  87.6 15.5 %collective-permute-start.12 = (bf16[384,512]{1,0:T(8,128)(2,1)}, bf16[384,512]{1,0:T(8,128)(2,1)}, u32[]{:S(2)}, u32[]{:S(2)}) collective-permute-start(bf16[384,512]{1,0:T(8,128)(2,1)} %convolution_convert_fusion.5), channel_id=1, source_target_pairs={{0,2},{1,3},{2,0},{3,1},{4,6},{5,7},{6,4},{7,5},{8,10},{9,11},{10,... | collective-permute-start | bytes 1179656 | tf_op jit(solution)/shard_map/ppermute | solution.py:31
  107.3 17.0 %all-to-all-start.1 = ((bf16[32,24,256]{2,1,0:T(8,128)(2,1)}), bf16[32,24,256]{2,1,0:T(8,128)(2,1)S(1)}, u32[]{:S(2)}, u32[]{:S(2)}) async-start(bf16[32,24,256]{2,1,0:T(8,128)(2,1)} %bitcast.274), calls=%async_computation.1 | async-start | bytes 786432 | tf_op jit(solution)/shard_map/all_to_all | solution.py:43
  126.0 12.0 %copy-start.43 = (bf16[128,512]{1,0:T(8,128)(2,1)S(1)}, bf16[128,512]{1,0:T(8,128)(2,1)}, u32[]{:S(2)}) copy-start(bf16[128,512]{1,0:T(8,128)(2,1)} %param.23) | copy-start | bytes 393220
  126.0 1.4 collective-permute-start.13
  127.5 8.0 %collective-permute-start.15 = (bf16[128,512]{0,1:T(8,128)(2,1)S(1)}, bf16[128,512]{0,1:T(8,128)(2,1)S(1)}, u32[]{:S(2)}, u32[]{:S(2)}) collective-permute-start(bf16[128,512]{0,1:T(8,128)(2,1)S(1)} %fusion.59), channel_id=1, source_target_pairs={{0,2},{1,3},{2,0},{3,1},{4,6},{5,7},{6,4},{7,5},{8,10},{9,11},{10,... | collective-permute-start | bytes 393224 | tf_op jit(solution)/shard_map/ppermute | solution.py:31
  128.7 8.8 %collective-permute-start.16 = (bf16[128,512]{0,1:T(8,128)(2,1)S(1)}, bf16[128,512]{0,1:T(8,128)(2,1)S(1)}, u32[]{:S(2)}, u32[]{:S(2)}) collective-permute-start(bf16[128,512]{0,1:T(8,128)(2,1)S(1)} %fusion.59), channel_id=1, source_target_pairs={{0,1},{1,2},{2,3},{3,0},{4,5},{5,6},{6,7},{7,4},{8,9},{9,10},{10,1... | collective-permute-start | bytes 393224 | tf_op jit(solution)/shard_map/ppermute | solution.py:31
  131.2 6.6 %collective-permute-start.14 = (bf16[128,512]{0,1:T(8,128)(2,1)S(1)}, bf16[128,512]{0,1:T(8,128)(2,1)S(1)}, u32[]{:S(2)}, u32[]{:S(2)}) collective-permute-start(bf16[128,512]{0,1:T(8,128)(2,1)S(1)} %fusion.59), channel_id=1, source_target_pairs={{0,3},{1,0},{2,1},{3,2},{4,7},{5,4},{6,5},{7,6},{8,11},{9,8},{10,9... | collective-permute-start | bytes 393224 | tf_op jit(solution)/shard_map/ppermute | solution.py:31
  140.0 1.5 collective-permute-start.24
  141.0 2.4 %collective-permute-start.17 = (bf16[128,2048]{0,1:T(8,128)(2,1)}, bf16[128,2048]{0,1:T(8,128)(2,1)}, u32[]{:S(2)}, u32[]{:S(2)}) collective-permute-start(bf16[128,2048]{0,1:T(8,128)(2,1)} %pad_maximum_fusion.8), channel_id=1, source_target_pairs={{0,4},{4,0},{1,5},{5,1},{2,6},{6,2},{3,7},{7,3},{8,12},{12,8},{9,1... | collective-permute-start | bytes 1572872 | tf_op jit(solution)/shard_map/ppermute | solution.py:26
  145.9 16.7 %copy-start.34 = (bf16[2,16,2,8,128]{4,3,2,1,0:T(8,128)(2,1)S(1)}, bf16[2,16,2,8,128]{4,3,2,1,0:T(8,128)(2,1)}, u32[]{:S(2)}) copy-start(bf16[2,16,2,8,128]{4,3,2,1,0:T(8,128)(2,1)} %pad_maximum_fusion.23) | copy-start | bytes 393220
  145.9 16.7 %copy-start.41 = (bf16[2,16,8,128]{3,2,1,0:T(8,128)(2,1)S(1)}, bf16[2,16,8,128]{3,2,1,0:T(8,128)(2,1)}, u32[]{:S(2)}) copy-start(bf16[2,16,8,128]{3,2,1,0:T(8,128)(2,1)} %broadcast_in_dim.37) | copy-start | bytes 196612
  146.0 10.8 %collective-permute-start.20 = (bf16[8,32,512]{2,1,0:T(8,128)(2,1)S(1)}, bf16[8,32,512]{2,1,0:T(8,128)(2,1)S(1)}, u32[]{:S(2)}, u32[]{:S(2)}) collective-permute-start(bf16[8,32,512]{2,1,0:T(8,128)(2,1)S(1)} %bitcast.284), channel_id=1, source_target_pairs={{0,16},{8,24},{16,0},{24,8},{1,17},{9,25},{17,1},{25,9},{2,18},{10... | collective-permute-start | bytes 786440 | tf_op jit(solution)/shard_map/ppermute | solution.py:31
  148.0 13.0 %collective-permute-start.19 = (bf16[8,32,512]{2,1,0:T(8,128)(2,1)S(1)}, bf16[8,32,512]{2,1,0:T(8,128)(2,1)S(1)}, u32[]{:S(2)}, u32[]{:S(2)}) collective-permute-start(bf16[8,32,512]{2,1,0:T(8,128)(2,1)S(1)} %bitcast.283), channel_id=1, source_target_pairs={{0,24},{8,0},{16,8},{24,16},{1,25},{9,1},{17,9},{25,17},{2,26},{10... | collective-permute-start | bytes 786440 | tf_op jit(solution)/shard_map/ppermute | solution.py:31
  148.7 13.1 %collective-permute-start.18 = (bf16[8,32,512]{2,1,0:T(8,128)(2,1)S(1)}, bf16[8,32,512]{2,1,0:T(8,128)(2,1)S(1)}, u32[]{:S(2)}, u32[]{:S(2)}) collective-permute-start(bf16[8,32,512]{2,1,0:T(8,128)(2,1)S(1)} %bitcast.282), channel_id=1, source_target_pairs={{0,8},{8,16},{16,24},{24,0},{1,9},{9,17},{17,25},{25,1},{2,10},{10... | collective-permute-start | bytes 786440 | tf_op jit(solution)/shard_map/ppermute | solution.py:31
  162.0 38.3 %copy-start.29 = (bf16[128,256]{1,0:T(8,128)(2,1)S(1)}, bf16[128,256]{1,0:T(8,128)(2,1)}, u32[]{:S(2)}) copy-start(bf16[128,256]{1,0:T(8,128)(2,1)} %copy-done.28) | copy-start | bytes 196612
  162.0 38.3 %copy-start.31 = (bf16[128,256]{1,0:T(8,128)(2,1)S(1)}, bf16[128,256]{1,0:T(8,128)(2,1)}, u32[]{:S(2)}) copy-start(bf16[128,256]{1,0:T(8,128)(2,1)} %copy-done.30) | copy-start | bytes 196612
  162.0 10.1 %collective-permute-start.21 = (bf16[4,32,512]{2,1,0:T(8,128)(2,1)S(1)}, bf16[4,32,512]{2,1,0:T(8,128)(2,1)S(1)}, u32[]{:S(2)}, u32[]{:S(2)}) collective-permute-start(bf16[4,32,512]{2,1,0:T(8,128)(2,1)S(1)} %fusion.72), channel_id=1, source_target_pairs={{0,32},{32,0},{64,96},{96,64},{128,160},{160,128},{192,224},{224,1... | collective-permute-start | bytes 393224 | tf_op jit(solution)/shard_map/ppermute | solution.py:545
  163.3 22.0 %all-to-all-start.2 = ((bf16[32,40,128]{2,1,0:T(8,128)(2,1)}), bf16[32,40,128]{2,1,0:T(8,128)(2,1)S(1)}, u32[]{:S(2)}, u32[]{:S(2)}) async-start(bf16[32,40,128]{2,1,0:T(8,128)(2,1)} %pad_maximum_fusion.18), calls=%async_computation.2 | async-start | bytes 655360 | tf_op jit(solution)/shard_map/all_to_all | solution.py:43
  172.2 22.6 %collective-permute-start.22 = (bf16[2,32,512]{2,1,0:T(8,128)(2,1)S(1)}, bf16[2,32,512]{2,1,0:T(8,128)(2,1)S(1)}, u32[]{:S(2)}, u32[]{:S(2)}) collective-permute-start(bf16[2,32,512]{2,1,0:T(8,128)(2,1)S(1)} %fusion.76), channel_id=1, source_target_pairs={{0,64},{32,96},{64,0},{96,32},{128,192},{160,224},{192,128},{224,1... | collective-permute-start | bytes 196616 | tf_op jit(solution)/shard_map/ppermute | solution.py:545
  187.8 16.4 %all-to-all-start.3 = ((bf16[32,32,128]{2,1,0:T(8,128)(2,1)}), bf16[32,32,128]{2,1,0:T(8,128)(2,1)S(1)}, u32[]{:S(2)}, u32[]{:S(2)}) async-start(bf16[32,32,128]{2,1,0:T(8,128)(2,1)} %shard_map.200), calls=%async_computation.3 | async-start | bytes 524288 | tf_op jit(solution)/shard_map/all_to_all | solution.py:43
  194.8 12.8 %collective-permute-start.23 = (bf16[1,32,512]{2,1,0:T(8,128)(2,1)S(1)}, bf16[1,32,512]{2,1,0:T(8,128)(2,1)S(1)}, u32[]{:S(2)}, u32[]{:S(2)}) collective-permute-start(bf16[1,32,512]{2,1,0:T(8,128)(2,1)S(1)} %fusion.78), channel_id=1, source_target_pairs={{0,128},{32,160},{64,192},{96,224},{128,0},{160,32},{192,64},{224,... | collective-permute-start | bytes 98312 | tf_op jit(solution)/shard_map/ppermute | solution.py:545
  207.5 1.6 collective-permute-start.25
  (44 other events, 158.6 us)

commit v3 on v2

--- a/solution.py
+++ b/solution.py
@@ -114,33 +114,6 @@
 
 GROUP = 4
 ROWS = 24
-
-
-def split_kernel(got_ref, x_ref, c_ref):
-    slots = x_ref.shape[0]
-    part = x_ref.shape[0] // (got_ref.shape[0] // ROWS // GROUP)
-    out_row = lax.broadcasted_iota(jnp.int32, (2 * part, 2 * part), 0)
-    in_row = lax.broadcasted_iota(jnp.int32, (2 * part, 2 * part), 1)
-    kind = (out_row >= part).astype(jnp.int32)
-    slot = out_row - kind * part
-    rows = part // GROUP
-    chip = sum((slot >= k * rows).astype(jnp.int32) for k in range(1, GROUP))
-    perm = jnp.where(slot + chip * rows + kind * rows == in_row, 1.0, 0.0).astype(bf16)
-
-    def block(i, carry):
-        start = pl.multiple_of(i * 2 * part, 2 * part)
-        made = dot(perm, got_ref[pl.ds(start, 2 * part), :]).astype(bf16)
-        place = pl.multiple_of(i * part, part)
-        x_ref[pl.ds(place, part), :] = made[:part]
-        c_ref[pl.ds(place, part), :] = made[part:]
-        return carry
-
-    lax.fori_loop(0, slots // part, block, 0)
-
-
-def split(got):
-    shape = jax.ShapeDtypeStruct((got.shape[0] // 2, got.shape[1]), bf16)
-    return pl.pallas_call(split_kernel, out_shape=(shape, shape))(got)
 
 
 def spread_kernel(own_ref, low_ref, up_ref, far_ref, sent_ref):
@@ -394,8 +367,12 @@
     side_other = swap(side)
     slots = chips * rows
     slots = chips * rows
-    side_other, small, small_other, back = lax.optimization_barrier(
-        (side_other, small, small_other, back)
+    out_row = lax.broadcasted_iota(jnp.int32, (slots, 2 * slots), 0)
+    in_row = lax.broadcasted_iota(jnp.int32, (slots, 2 * slots), 1)
+    origin = out_row + out_row // rows * rows
+    sort_rows = [(origin + j * rows == in_row).astype(bf16) for j in range(2)]
+    side_other, small, small_other, back, sort_rows = lax.optimization_barrier(
+        (side_other, small, small_other, back, sort_rows)
     )
     value = ordered(value_mine, side_other[:, :half])
     gated_all = jnp.concatenate([gated, side_other[:, half + 2 * STATE :]], axis=0)
@@ -458,7 +435,7 @@
     proj = rolled(proj_weight)
     hid = gate_weight.shape[2]
     received = exchange(sent.reshape(chips, 2 * rows, width)).reshape(2 * slots, width)
-    input_own, cotangent_own = split(received)
+    input_own, cotangent_own = (dot(a, received).astype(bf16) for a in sort_rows)
     input_low = ring(input_own, 1)
     cotangent_up = ring(cotangent_own, -1)
     input_up = ring(input_own, -1)
@@ -536,16 +513,24 @@
     scanned = scan_chunks(states_got)
     states_back = exchange(scanned)
     depth = lax.axis_index(SP[0])
-    gap = 1
-    while gap < deep:
-        upper = (depth & gap) != 0
-        pairs = proj_sum.reshape(-1, 2, block, width)
-        below, above = pairs[:, 0], pairs[:, 1]
-        away = jnp.where(upper, below, above).astype(bf16)
-        got = lax.ppermute(away, SP[0], [(i, i ^ gap) for i in range(deep)])
-        proj_sum = jnp.where(upper, above, below) + got.astype(f32)
-        gap *= 2
-    proj_grad = proj_sum[0]
+    upper = (depth & 1) != 0
+    pairs = proj_sum.reshape(deep // 2, 2, block, width)
+    away = jnp.where(upper, pairs[:, 0], pairs[:, 1]).astype(bf16)
+    got = lax.ppermute(away, SP[0], [(i, i ^ 1) for i in range(deep)])
+    proj_sum = jnp.where(upper, pairs[:, 1], pairs[:, 0]) + got.astype(f32)
+    level = depth >> 1
+    count = deep // 2
+
+    def level_part(i):
+        return lax.dynamic_index_in_dim(proj_sum, (level + i) & (count - 1), 0, keepdims=False)
+
+    others = [
+        lax.ppermute(
+            level_part(k).astype(bf16), SP[0], [(i, (i + 2 * k) % deep) for i in range(deep)]
+        )
+        for k in range(1, count)
+    ]
+    proj_grad = level_part(0) + sum(a.astype(f32) for a in others)
 
     base = mix_chunk(delta, value, write, read, cumul_wide, cumul_row)
     outs_mine, outs_send = tail(

time: 215 us -> 204 us (0.949)
  waiting for transfers between devices: 71 us -> 58.6 us
  other arithmetic: 18.3 us -> 24.1 us
  Pallas kernels: 19.3 us -> 15.9 us
    ppermute x15, waiting for transfers between devices: 46 us -> 38.4 us  [ring(): return lax.ppermute(x, axis, [(i, (i + shift) % n) for i in range(n)])]
    all_to_all x4, waiting for transfers between devices: 22 us -> 18 us  [exchange(): return lax.all_to_all(x, CHIPS, split_axis=0, concat_axis=0, tiled=True)]
    pallas_call x1 -> x0, Pallas kernels: 3.28 us -> none  [split(): return pl.pallas_call(split_kernel, out_shape=(shape, shape))(got)]
    unnamed x124 -> x112, local copies, waits for them, and re-layouts: 7.49 us -> 6.43 us
    dot_general x31 -> x33, matrix products: 23.4 us -> 22.5 us  [dot(): lax.dot_general(a, b, (((ca,), (cb,)), ((), ())), preferred_element_type=...]
    ppermute x3 -> x4, starting transfers between devices: 8.45 us -> 8.64 us  [the longest x3 8.48 us: on_device(): lax.ppermute(level_part(k).astype(bf16), SP[0], [(i, (i + 2 * k) % deep)...]
  transfers between devices with their start and end apart: 30 -> 31, of which waited for: 17 -> 16; matrix products, arithmetic and copies ran while one was open for 17% -> 19% of each run, Pallas kernels for 3% -> 4%
where the time goes in v3:
time: 204 us; the launch traced here: 200 us
  starting transfers between devices  64 us (31%)
  waiting for transfers between devices  58.6 us (29%)
  other arithmetic  24.1 us (12%)
  matrix products  22.8 us (11%)
  Pallas kernels  15.9 us (8%)
  local copies, waits for them, and re-layouts  13 us (6%)
    ppermute x15, waiting for transfers between devices, ring(): return lax.ppermute(x, axis, [(i, (i + shift) % n) for i in range(n)])  38.4 us
    all_to_all x4, starting transfers between devices, exchange(): return lax.all_to_all(x, CHIPS, split_axis=0, concat_axis=0, tiled=True)  32 us
    dot_general x33, matrix products, dot(): lax.dot_general(a, b, (((ca,), (cb,)), ((), ())), preferred_element_type=...  22.5 us
    ppermute x15, starting transfers between devices, ring(): return lax.ppermute(x, axis, [(i, (i + shift) % n) for i in range(n)])  21.5 us
    all_to_all x4, waiting for transfers between devices, exchange(): return lax.all_to_all(x, CHIPS, split_axis=0, concat_axis=0, tiled=True)  18 us
    ppermute x3, starting transfers between devices, on_device(): lax.ppermute(level_part(k).astype(bf16), SP[0], [(i, (i + 2 * k) % deep)...  8.48 us
    unnamed x112, local copies, waits for them, and re-layouts  6.43 us
  transfers between devices with their start and end apart: 31, of which 16 were waited for; matrix products, arithmetic and copies ran while one was open for 19% of the time, Pallas kernels for 4%

profile of v3, /device:TPU:4, one launch (start us, length us, event | category | flops | bytes accessed | tf_op | source)
XLA Modules:
  0.0 200.2 jit_solution(5254752001138960617)
XLA Ops:
  2.9 1.4 fusion.4
  6.8 3.4 %shard_map.197 = (bf16[768,512]{1,0:T(8,128)(2,1)}, s32[8,256]{1,0:T(8,128)}) custom-call(s32[1]{0:T(128)} %bitcast.core_ref, f32[12,128]{1,0:T(8,128)} %copy-done.47, f32[12,128]{1,0:T(8,128)} %copy-done.49, bf16[128,512]{1,0:T(8,128)(2,1)} %x_ref.1, bf16[128,512]{1,0:T(8,128)(2,1)} %copy-done.42, bf16[128,512]{1,0:T(8,128)(2,1)} %c_ref.1, ...), custom_call_target="tpu_custom_call" | custom-call | tf_op jit(solution)/shard_map/pallas_call | solution.py:105
  11.3 1.5 pad_maximum_fusion.20
  14.1 11.6 %all-to-all-start = ((bf16[32,24,512]{2,1,0:T(8,128)(2,1)}), bf16[32,24,512]{2,1,0:T(8,128)(2,1)}, u32[]{:S(2)}, u32[]{:S(2)}) async-start(bf16[32,24,512]{2,1,0:T(8,128)(2,1)} %bitcast.253), calls=%async_computation | async-start | bytes 1572864 | tf_op jit(solution)/shard_map/all_to_all | solution.py:43
  25.8 2.5 %dynamic-slice_bitcast_fusion.10 = (bf16[512,256]{1,0:T(8,128)(2,1)}, bf16[512,256]{1,0:T(8,128)(2,1)}, bf16[512,256]{1,0:T(8,128)(2,1)}, bf16[512,256]{1,0:T(8,...) fusion(bf16[4,512,256]{2,1,0:T(8,128)(2,1)S(1)} %bitcast.249, ...), kind=kLoop, calls=%fused_computation.156 | loop fusion | bytes 4194320 | tf_op jit(solution)/shard_map/jit(dynamic_index_in_dim)/squeeze | solution.py:417
  29.1 1.6 add_convert_fusion
  31.5 1.2 reduce-window.6
  40.1 8.3 %all-to-all-done = bf16[32,24,512]{2,1,0:T(8,128)(2,1)} async-done(((bf16[32,24,512]{2,1,0:T(8,128)(2,1)}), bf16[32,24,512]{2,1,0:T(8,128)(2,1)}, u32[]{:S(2)}, u32[]{:S(2)}) %all-to-all-start) | async-done | bytes 786464 | tf_op jit(solution)/shard_map/all_to_all | solution.py:43
  48.5 1.9 convolution_convert_fusion.9
  50.4 3.1 %collective-permute-start.7 = (bf16[384,512]{1,0:T(8,128)(2,1)S(1)}, bf16[384,512]{1,0:T(8,128)(2,1)S(1)}, u32[]{:S(2)}, u32[]{:S(2)}) collective-permute-start(bf16[384,512]{1,0:T(8,128)(2,1)S(1)} %convolution_convert_fusion.9), channel_id=1, source_target_pairs={{0,3},{1,0},{2,1},{3,2},{4,7},{5,4},{6,5},{7,6},{8,11},{9,8},{10,9... | collective-permute-start | bytes 1179656 | tf_op jit(solution)/shard_map/ppermute | solution.py:31
  53.5 1.6 convolution_convert_fusion.10
  55.1 3.3 %collective-permute-start.4 = (bf16[384,512]{1,0:T(8,128)(2,1)S(1)}, bf16[384,512]{1,0:T(8,128)(2,1)S(1)}, u32[]{:S(2)}, u32[]{:S(2)}) collective-permute-start(bf16[384,512]{1,0:T(8,128)(2,1)S(1)} %convolution_convert_fusion.10), channel_id=1, source_target_pairs={{0,3},{1,0},{2,1},{3,2},{4,7},{5,4},{6,5},{7,6},{8,11},{9,8},{10,9... | collective-permute-start | bytes 1179656 | tf_op jit(solution)/shard_map/ppermute | solution.py:31
  59.3 7.4 %collective-permute-done.8 = bf16[384,512]{1,0:T(8,128)(2,1)S(1)} collective-permute-done((bf16[384,512]{1,0:T(8,128)(2,1)S(1)}, bf16[384,512]{1,0:T(8,128)(2,1)S(1)}, u32[]{:S(2)}, u32[]{:S(2)}) %collective-permute-start.8) | collective-permute-done | bytes 393248 | tf_op jit(solution)/shard_map/ppermute | solution.py:31
  66.7 2.2 %collective-permute-done.4 = bf16[384,512]{1,0:T(8,128)(2,1)S(1)} collective-permute-done((bf16[384,512]{1,0:T(8,128)(2,1)S(1)}, bf16[384,512]{1,0:T(8,128)(2,1)S(1)}, u32[]{:S(2)}, u32[]{:S(2)}) %collective-permute-start.4) | collective-permute-done | bytes 393248 | tf_op jit(solution)/shard_map/ppermute | solution.py:31
  68.9 3.7 %collective-permute-start.6 = (bf16[384,512]{1,0:T(8,128)(2,1)S(1)}, bf16[384,512]{1,0:T(8,128)(2,1)S(1)}, u32[]{:S(2)}, u32[]{:S(2)}) collective-permute-start(bf16[384,512]{1,0:T(8,128)(2,1)S(1)} %collective-permute-done.4), channel_id=1, source_target_pairs={{0,3},{1,0},{2,1},{3,2},{4,7},{5,4},{6,5},{7,6},{8,11},{9,8},{10,9... | collective-permute-start | bytes 1179656 | tf_op jit(solution)/shard_map/ppermute | solution.py:31
  74.0 1.1 collective-permute-done.5
  75.5 5.3 %collective-permute-done.9 = bf16[384,512]{1,0:T(8,128)(2,1)S(1)} collective-permute-done((bf16[384,512]{1,0:T(8,128)(2,1)S(1)}, bf16[384,512]{1,0:T(8,128)(2,1)S(1)}, u32[]{:S(2)}, u32[]{:S(2)}) %collective-permute-start.9) | collective-permute-done | bytes 393248 | tf_op jit(solution)/shard_map/ppermute | solution.py:31
  82.7 1.2 convolution_convert_fusion.7
  83.8 1.2 convolution_convert_fusion.6
  85.0 1.2 convolution_convert_fusion.5
  86.2 3.2 %collective-permute-start.11 = (bf16[384,512]{1,0:T(8,128)(2,1)}, bf16[384,512]{1,0:T(8,128)(2,1)}, u32[]{:S(2)}, u32[]{:S(2)}) collective-permute-start(bf16[384,512]{1,0:T(8,128)(2,1)} %convolution_convert_fusion.6), channel_id=1, source_target_pairs={{0,3},{1,0},{2,1},{3,2},{4,7},{5,4},{6,5},{7,6},{8,11},{9,8},{10,9... | collective-permute-start | bytes 1179656 | tf_op jit(solution)/shard_map/ppermute | solution.py:31
  89.4 2.2 %convolution_convert_fusion.8.own_ref = bf16[384,512]{1,0:T(8,128)(2,1)} fusion(bf16[384,512]{0,1:T(8,128)(2,1)S(1)} %pad_maximum_fusion.9, bf16[512,256]{1,0:T(8,128)(2,1)} %get-tuple-element.132, bf16[512,256]{1,0:T(8,128)(2,1)} %get-tuple-element.176), kind=kOutput, calls=%fused_computation.12 | convolution fusion | flops 202571776 | bytes 1310720 | tf_op jit(solution)/shard_map/dot_general | solution.py:22
  91.6 12.7 %collective-permute-done.10.low_ref = bf16[384,512]{1,0:T(8,128)(2,1)S(1)} collective-permute-done((bf16[384,512]{1,0:T(8,128)(2,1)}, bf16[384,512]{1,0:T(8,128)(2,1)S(1)}, u32[]{:S(2)}, u32[]{:S(2)}) %collective-permute-start.10) | collective-permute-done | bytes 393248 | tf_op jit(solution)/shard_map/ppermute | solution.py:31
  105.1 3.6 %shard_map.198 = bf16[768,256]{1,0:T(8,128)(2,1)} custom-call(bf16[384,512]{1,0:T(8,128)(2,1)} %convolution_convert_fusion.8.own_ref, bf16[384,512]{1,0:T(8,128)(2,1)} %copy-done.38, bf16[384,512]{1,0:T(8,128)(2,1)} %collective-permute-done.11.up_ref, bf16[384,512]{1,0:T(8,128)(2,1)} %collective-permute-done.12.far_ref), custom_call_target="tpu_custom_call" | custom-call | tf_op jit(solution)/shard_map/pallas_call | solution.py:147
  108.7 6.7 %all-to-all-start.1 = ((bf16[32,24,256]{2,1,0:T(8,128)(2,1)}), bf16[32,24,256]{2,1,0:T(8,128)(2,1)S(1)}, u32[]{:S(2)}, u32[]{:S(2)}) async-start(bf16[32,24,256]{2,1,0:T(8,128)(2,1)} %bitcast.248), calls=%async_computation.1 | async-start | bytes 786432 | tf_op jit(solution)/shard_map/all_to_all | solution.py:43
  115.4 1.6 fusion
  123.4 1.1 maximum_bitcast_fusion.2
  124.5 2.1 %all-to-all-done.1 = bf16[32,24,256]{2,1,0:T(8,128)(2,1)S(1)} async-done(((bf16[32,24,256]{2,1,0:T(8,128)(2,1)}), bf16[32,24,256]{2,1,0:T(8,128)(2,1)S(1)}, u32[]{:S(2)}, u32[]{:S(2)}) %all-to-all-start.1) | async-done | bytes 393248 | tf_op jit(solution)/shard_map/all_to_all | solution.py:43
  126.6 1.3 fusion.109
  130.8 2.4 %collective-permute-start.16 = (bf16[128,512]{0,1:T(8,128)(2,1)S(1)}, bf16[128,512]{0,1:T(8,128)(2,1)S(1)}, u32[]{:S(2)}, u32[]{:S(2)}) collective-permute-start(bf16[128,512]{0,1:T(8,128)(2,1)S(1)} %fusion.61), channel_id=1, source_target_pairs={{0,1},{1,2},{2,3},{3,0},{4,5},{5,6},{6,7},{7,4},{8,9},{9,10},{10,1... | collective-permute-start | bytes 393224 | tf_op jit(solution)/shard_map/ppermute | solution.py:31
  134.0 3.7 %collective-permute-done.15 = bf16[128,512]{0,1:T(8,128)(2,1)S(1)} collective-permute-done((bf16[128,512]{0,1:T(8,128)(2,1)S(1)}, bf16[128,512]{0,1:T(8,128)(2,1)S(1)}, u32[]{:S(2)}, u32[]{:S(2)}) %collective-permute-start.15) | collective-permute-done | bytes 131104 | tf_op jit(solution)/shard_map/ppermute | solution.py:31
  138.0 1.8 collective-permute-done.16
  140.3 1.9 fusion.48
  146.7 1.8 collective-permute-start.20
  149.3 1.2 collective-permute-start.18
  151.3 8.3 %all-to-all-start.2 = ((bf16[32,40,128]{2,1,0:T(8,128)(2,1)}), bf16[32,40,128]{2,1,0:T(8,128)(2,1)S(1)}, u32[]{:S(2)}, u32[]{:S(2)}) async-start(bf16[32,40,128]{2,1,0:T(8,128)(2,1)} %pad_maximum_fusion.18), calls=%async_computation.2 | async-start | bytes 655360 | tf_op jit(solution)/shard_map/all_to_all | solution.py:43
  159.7 2.4 %collective-permute-done.19 = bf16[8,32,512]{2,1,0:T(8,128)(2,1)} collective-permute-done((bf16[8,32,512]{2,1,0:T(8,128)(2,1)S(1)}, bf16[8,32,512]{2,1,0:T(8,128)(2,1)}, u32[]{:S(2)}, u32[]{:S(2)}) %collective-permute-start.19) | collective-permute-done | bytes 262176 | tf_op jit(solution)/shard_map/ppermute | solution.py:31
  162.1 1.8 collective-permute-done.18
  163.8 1.2 fusion.32
  165.3 7.6 %all-to-all-done.2.msg_ref = bf16[32,40,128]{2,1,0:T(8,128)(2,1)S(1)} async-done(((bf16[32,40,128]{2,1,0:T(8,128)(2,1)}), bf16[32,40,128]{2,1,0:T(8,128)(2,1)S(1)}, u32[]{:S(2)}, u32[]{:S(2)}) %all-to-all-start.2) | async-done | bytes 327712 | tf_op jit(solution)/shard_map/all_to_all | solution.py:43
  173.7 1.8 shard_map.199
  175.5 5.4 %all-to-all-start.3 = ((bf16[32,32,128]{2,1,0:T(8,128)(2,1)}), bf16[32,32,128]{2,1,0:T(8,128)(2,1)S(1)}, u32[]{:S(2)}, u32[]{:S(2)}) async-start(bf16[32,32,128]{2,1,0:T(8,128)(2,1)} %shard_map.199), calls=%async_computation.3 | async-start | bytes 524288 | tf_op jit(solution)/shard_map/all_to_all | solution.py:43
  181.0 3.8 %collective-permute-start.24 = (bf16[32,512]{1,0:T(8,128)(2,1)S(1)}, bf16[32,512]{1,0:T(8,128)(2,1)S(1)}, u32[]{:S(2)}, u32[]{:S(2)}) collective-permute-start(bf16[32,512]{1,0:T(8,128)(2,1)S(1)} %get-tuple-element.152), channel_id=1, source_target_pairs={{0,192},{32,224},{64,0},{96,32},{128,64},{160,96},{192,128},{224,1... | collective-permute-start | bytes 98312 | tf_op jit(solution)/shard_map/ppermute | solution.py:528
  184.8 2.3 %collective-permute-start.23 = (bf16[32,512]{1,0:T(8,128)(2,1)S(1)}, bf16[32,512]{1,0:T(8,128)(2,1)S(1)}, u32[]{:S(2)}, u32[]{:S(2)}) collective-permute-start(bf16[32,512]{1,0:T(8,128)(2,1)S(1)} %get-tuple-element.153), channel_id=1, source_target_pairs={{0,128},{32,160},{64,192},{96,224},{128,0},{160,32},{192,64},{224,... | collective-permute-start | bytes 98312 | tf_op jit(solution)/shard_map/ppermute | solution.py:528
  187.1 2.4 %collective-permute-start.22 = (bf16[32,512]{1,0:T(8,128)(2,1)S(1)}, bf16[32,512]{1,0:T(8,128)(2,1)S(1)}, u32[]{:S(2)}, u32[]{:S(2)}) collective-permute-start(bf16[32,512]{1,0:T(8,128)(2,1)S(1)} %get-tuple-element.151), channel_id=1, source_target_pairs={{0,64},{32,96},{64,128},{96,160},{128,192},{160,224},{192,0},{224,... | collective-permute-start | bytes 98312 | tf_op jit(solution)/shard_map/ppermute | solution.py:528
  190.2 2.9 %shard_map.200.base_ref = f32[256,512]{1,0:T(8,128)} custom-call(bf16[256,256]{1,0:T(8,128)(2,1)} %pad_maximum_fusion.24.delta_ref, bf16[256,256]{1,0:T(8,128)(2,1)} %pad_maximum_fusion.22.value_ref, bf16[256,128]{1,0:T(8,128)(2,1)} %pad_maximum_fusion.26.write_ref, bf16[256,128]{1,0:T(8,128)(2,1)} %copy-done.21, f32[256,256]{1,0:T(8,128)} %copy-done.1, ...), custom_call_target="tpu_custom_call" | custom-call | tf_op jit(solution)/shard_map/pallas_call | solution.py:173
  193.7 2.6 %shard_map.201 = (f32[128,512]{1,0:T(8,128)}, bf16[128,512]{1,0:T(8,128)(2,1)}) custom-call(s32[1]{0:T(128)} %bitcast.core_ref, bf16[32,32,128]{2,1,0:T(8,128)(2,1)} %copy-done.22, bf16[256,128]{1,0:T(8,128)(2,1)} %pad_maximum_fusion.26.write_ref, bf16[256,256]{1,0:T(8,128)(2,1)} %copy-done.20, bf16[256,256]{1,0:T(8,128)(2,1)} %copy-done.19, ...), custom_call_target="tpu_custom_call" | custom-call | tf_op jit(solution)/shard_map/pallas_call | solution.py:274
  198.6 1.7 shard_map.202
  (241 shorter events, 42.3 us)
Async XLA Ops:
  0.6 137.1 %copy-start = (bf16[2048,512]{1,0:T(8,128)(2,1)S(1)}, bf16[2048,512]{1,0:T(8,128)(2,1)}, u32[]{:S(2)}) copy-start(bf16[2048,512]{1,0:T(8,128)(2,1)} %param.24) | copy-start | bytes 6291460
  0.6 10.7 %copy-start.34 = (bf16[128,512]{1,0:T(8,128)(2,1)S(1)}, bf16[128,512]{1,0:T(8,128)(2,1)}, u32[]{:S(2)}) copy-start(bf16[128,512]{1,0:T(8,128)(2,1)} %param.21) | copy-start | bytes 393220
  2.2 3.9 %collective-permute-start = (f32[12,128]{1,0:T(8,128)S(1)}, f32[12,128]{1,0:T(8,128)S(1)}, u32[]{:S(2)}, u32[]{:S(2)}) collective-permute-start(f32[12,128]{1,0:T(8,128)S(1)} %pad_maximum_fusion.28.mine_ref), channel_id=1, source_target_pairs={{0,4},{4,0},{1,5},{5,1},{2,6},{6,2},{3,7},{7,3},{8,12},{12,8},{9,1... | collective-permute-start | bytes 18440 | tf_op jit(solution)/shard_map/ppermute | solution.py:26
  2.3 3.8 %collective-permute-start.1 = (bf16[128,512]{1,0:T(8,128)(2,1)}, bf16[128,512]{1,0:T(8,128)(2,1)S(1)}, u32[]{:S(2)}, u32[]{:S(2)}) collective-permute-start(bf16[128,512]{1,0:T(8,128)(2,1)} %x_ref.1), channel_id=1, source_target_pairs={{0,4},{4,0},{1,5},{5,1},{2,6},{6,2},{3,7},{7,3},{8,12},{12,8},{9,1... | collective-permute-start | bytes 393224 | tf_op jit(solution)/shard_map/ppermute | solution.py:26
  2.8 3.3 %collective-permute-start.2 = (bf16[128,512]{1,0:T(8,128)(2,1)}, bf16[128,512]{1,0:T(8,128)(2,1)S(1)}, u32[]{:S(2)}, u32[]{:S(2)}) collective-permute-start(bf16[128,512]{1,0:T(8,128)(2,1)} %c_ref.1), channel_id=1, source_target_pairs={{0,4},{4,0},{1,5},{5,1},{2,6},{6,2},{3,7},{7,3},{8,12},{12,8},{9,1... | collective-permute-start | bytes 393224 | tf_op jit(solution)/shard_map/ppermute | solution.py:26
  2.9 22.8 %copy-start.23 = (bf16[1,2048,256]{2,1,0:T(8,128)(2,1)S(1)}, bf16[1,2048,256]{2,1,0:T(8,128)(2,1)}, u32[]{:S(2)}) copy-start(bf16[1,2048,256]{2,1,0:T(8,128)(2,1)} %param.19) | copy-start | bytes 3145732
  12.9 17.8 %collective-permute-start.3 = (bf16[128,1024]{1,0:T(8,128)(2,1)}, bf16[128,1024]{1,0:T(8,128)(2,1)}, u32[]{:S(2)}, u32[]{:S(2)}) collective-permute-start(bf16[128,1024]{1,0:T(8,128)(2,1)} %pad_maximum_fusion.20), channel_id=1, source_target_pairs={{0,4},{4,0},{1,5},{5,1},{2,6},{6,2},{3,7},{7,3},{8,12},{12,8},{9,1... | collective-permute-start | bytes 786440 | tf_op jit(solution)/shard_map/ppermute | solution.py:26
  14.1 34.4 %all-to-all-start = ((bf16[32,24,512]{2,1,0:T(8,128)(2,1)}), bf16[32,24,512]{2,1,0:T(8,128)(2,1)}, u32[]{:S(2)}, u32[]{:S(2)}) async-start(bf16[32,24,512]{2,1,0:T(8,128)(2,1)} %bitcast.253), calls=%async_computation | async-start | bytes 1572864 | tf_op jit(solution)/shard_map/all_to_all | solution.py:43
  33.5 16.9 %copy-start.1 = (f32[256,256]{1,0:T(8,128)}, f32[256,256]{1,0:T(8,128)S(1)}, u32[]{:S(2)}) copy-start(f32[256,256]{1,0:T(8,128)S(1)} %fusion.86.wide_ref) | copy-start | bytes 786436
  36.9 16.6 %copy-start.32 = (bf16[384,768]{1,0:T(8,128)(2,1)S(1)}, bf16[384,768]{1,0:T(8,128)(2,1)}, u32[]{:S(2)}) copy-start(bf16[384,768]{1,0:T(8,128)(2,1)} %get-tuple-element.63) | copy-start | bytes 1769476
  37.9 106.0 %copy-start.21 = (bf16[256,128]{1,0:T(8,128)(2,1)}, bf16[256,128]{1,0:T(8,128)(2,1)S(1)}, u32[]{:S(2)}) copy-start(bf16[256,128]{1,0:T(8,128)(2,1)S(1)} %pad_maximum_fusion.27.read_ref) | copy-start | bytes 196612
  48.5 10.0 %copy-start.33 = (bf16[1,256,2048]{2,1,0:T(8,128)(2,1)S(1)}, bf16[1,256,2048]{2,1,0:T(8,128)(2,1)}, u32[]{:S(2)}) copy-start(bf16[1,256,2048]{2,1,0:T(8,128)(2,1)} %param.20) | copy-start | bytes 3145732
  48.5 10.3 %copy-start.30 = (bf16[512,256]{1,0:T(8,128)(2,1)S(1)}, bf16[512,256]{1,0:T(8,128)(2,1)}, u32[]{:S(2)}) copy-start(bf16[512,256]{1,0:T(8,128)(2,1)} %get-tuple-element.132) | copy-start | bytes 786436
  48.5 10.3 %copy-start.31 = (bf16[512,256]{1,0:T(8,128)(2,1)S(1)}, bf16[512,256]{1,0:T(8,128)(2,1)}, u32[]{:S(2)}) copy-start(bf16[512,256]{1,0:T(8,128)(2,1)} %get-tuple-element.176) | copy-start | bytes 786436
  50.4 8.9 %copy-start.15 = (bf16[384,512]{1,0:T(8,128)(2,1)}, bf16[384,512]{1,0:T(8,128)(2,1)S(1)}, u32[]{:S(2)}) copy-start(bf16[384,512]{1,0:T(8,128)(2,1)S(1)} %convolution_convert_fusion.9) | copy-start | bytes 1179652
  50.4 22.2 %copy-start.28 = (bf16[512,256]{1,0:T(8,128)(2,1)S(1)}, bf16[512,256]{1,0:T(8,128)(2,1)}, u32[]{:S(2)}) copy-start(bf16[512,256]{1,0:T(8,128)(2,1)} %get-tuple-element.131) | copy-start | bytes 786436
  50.4 22.2 %copy-start.29 = (bf16[512,256]{1,0:T(8,128)(2,1)S(1)}, bf16[512,256]{1,0:T(8,128)(2,1)}, u32[]{:S(2)}) copy-start(bf16[512,256]{1,0:T(8,128)(2,1)} %get-tuple-element.177) | copy-start | bytes 786436
  50.4 22.2 %collective-permute-start.7 = (bf16[384,512]{1,0:T(8,128)(2,1)S(1)}, bf16[384,512]{1,0:T(8,128)(2,1)S(1)}, u32[]{:S(2)}, u32[]{:S(2)}) collective-permute-start(bf16[384,512]{1,0:T(8,128)(2,1)S(1)} %convolution_convert_fusion.9), channel_id=1, source_target_pairs={{0,3},{1,0},{2,1},{3,2},{4,7},{5,4},{6,5},{7,6},{8,11},{9,8},{10,9... | collective-permute-start | bytes 1179656 | tf_op jit(solution)/shard_map/ppermute | solution.py:31
  53.5 13.2 %collective-permute-start.8 = (bf16[384,512]{1,0:T(8,128)(2,1)S(1)}, bf16[384,512]{1,0:T(8,128)(2,1)S(1)}, u32[]{:S(2)}, u32[]{:S(2)}) collective-permute-start(bf16[384,512]{1,0:T(8,128)(2,1)S(1)} %convolution_convert_fusion.9), channel_id=1, source_target_pairs={{0,1},{1,2},{2,3},{3,0},{4,5},{5,6},{6,7},{7,4},{8,9},{9,10},{10,1... | collective-permute-start | bytes 1179656 | tf_op jit(solution)/shard_map/ppermute | solution.py:31
  55.1 18.0 %copy-start.9 = (bf16[384,512]{1,0:T(8,128)(2,1)}, bf16[384,512]{1,0:T(8,128)(2,1)S(1)}, u32[]{:S(2)}) copy-start(bf16[384,512]{1,0:T(8,128)(2,1)S(1)} %convolution_convert_fusion.10) | copy-start | bytes 1179652
  55.1 13.8 %collective-permute-start.4 = (bf16[384,512]{1,0:T(8,128)(2,1)S(1)}, bf16[384,512]{1,0:T(8,128)(2,1)S(1)}, u32[]{:S(2)}, u32[]{:S(2)}) collective-permute-start(bf16[384,512]{1,0:T(8,128)(2,1)S(1)} %convolution_convert_fusion.10), channel_id=1, source_target_pairs={{0,3},{1,0},{2,1},{3,2},{4,7},{5,4},{6,5},{7,6},{8,11},{9,8},{10,9... | collective-permute-start | bytes 1179656 | tf_op jit(solution)/shard_map/ppermute | solution.py:31
  58.4 16.7 %collective-permute-start.5 = (bf16[384,512]{1,0:T(8,128)(2,1)S(1)}, bf16[384,512]{1,0:T(8,128)(2,1)S(1)}, u32[]{:S(2)}, u32[]{:S(2)}) collective-permute-start(bf16[384,512]{1,0:T(8,128)(2,1)S(1)} %convolution_convert_fusion.10), channel_id=1, source_target_pairs={{0,1},{1,2},{2,3},{3,0},{4,5},{5,6},{6,7},{7,4},{8,9},{9,10},{10,1... | collective-permute-start | bytes 1179656 | tf_op jit(solution)/shard_map/ppermute | solution.py:31
  58.8 14.3 %copy-start.26 = (bf16[512,256]{1,0:T(8,128)(2,1)S(1)}, bf16[512,256]{1,0:T(8,128)(2,1)}, u32[]{:S(2)}) copy-start(bf16[512,256]{1,0:T(8,128)(2,1)} %get-tuple-element.130) | copy-start | bytes 786436
  58.8 14.3 %copy-start.27 = (bf16[512,256]{1,0:T(8,128)(2,1)S(1)}, bf16[512,256]{1,0:T(8,128)(2,1)}, u32[]{:S(2)}) copy-start(bf16[512,256]{1,0:T(8,128)(2,1)} %get-tuple-element.178) | copy-start | bytes 786436
  66.7 14.0 %collective-permute-start.9 = (bf16[384,512]{1,0:T(8,128)(2,1)S(1)}, bf16[384,512]{1,0:T(8,128)(2,1)S(1)}, u32[]{:S(2)}, u32[]{:S(2)}) collective-permute-start(bf16[384,512]{1,0:T(8,128)(2,1)S(1)} %collective-permute-done.8), channel_id=1, source_target_pairs={{0,1},{1,2},{2,3},{3,0},{4,5},{5,6},{6,7},{7,4},{8,9},{9,10},{10,1... | collective-permute-start | bytes 1179656 | tf_op jit(solution)/shard_map/ppermute | solution.py:31
  68.9 12.3 %collective-permute-start.6 = (bf16[384,512]{1,0:T(8,128)(2,1)S(1)}, bf16[384,512]{1,0:T(8,128)(2,1)S(1)}, u32[]{:S(2)}, u32[]{:S(2)}) collective-permute-start(bf16[384,512]{1,0:T(8,128)(2,1)S(1)} %collective-permute-done.4), channel_id=1, source_target_pairs={{0,3},{1,0},{2,1},{3,2},{4,7},{5,4},{6,5},{7,6},{8,11},{9,8},{10,9... | collective-permute-start | bytes 1179656 | tf_op jit(solution)/shard_map/ppermute | solution.py:31
  73.1 7.6 %copy-start.24 = (bf16[512,256]{1,0:T(8,128)(2,1)S(1)}, bf16[512,256]{1,0:T(8,128)(2,1)}, u32[]{:S(2)}) copy-start(bf16[512,256]{1,0:T(8,128)(2,1)} %get-tuple-element.129) | copy-start | bytes 786436
  86.2 18.2 %collective-permute-start.10 = (bf16[384,512]{1,0:T(8,128)(2,1)}, bf16[384,512]{1,0:T(8,128)(2,1)S(1)}, u32[]{:S(2)}, u32[]{:S(2)}) collective-permute-start(bf16[384,512]{1,0:T(8,128)(2,1)} %convolution_convert_fusion.7), channel_id=1, source_target_pairs={{0,1},{1,2},{2,3},{3,0},{4,5},{5,6},{6,7},{7,4},{8,9},{9,10},{10,1... | collective-permute-start | bytes 1179656 | tf_op jit(solution)/shard_map/ppermute | solution.py:31
  86.2 18.2 %collective-permute-start.11 = (bf16[384,512]{1,0:T(8,128)(2,1)}, bf16[384,512]{1,0:T(8,128)(2,1)}, u32[]{:S(2)}, u32[]{:S(2)}) collective-permute-start(bf16[384,512]{1,0:T(8,128)(2,1)} %convolution_convert_fusion.6), channel_id=1, source_target_pairs={{0,3},{1,0},{2,1},{3,2},{4,7},{5,4},{6,5},{7,6},{8,11},{9,8},{10,9... | collective-permute-start | bytes 1179656 | tf_op jit(solution)/shard_map/ppermute | solution.py:31
  89.4 14.9 %collective-permute-start.12 = (bf16[384,512]{1,0:T(8,128)(2,1)}, bf16[384,512]{1,0:T(8,128)(2,1)}, u32[]{:S(2)}, u32[]{:S(2)}) collective-permute-start(bf16[384,512]{1,0:T(8,128)(2,1)} %convolution_convert_fusion.5), channel_id=1, source_target_pairs={{0,2},{1,3},{2,0},{3,1},{4,6},{5,7},{6,4},{7,5},{8,10},{9,11},{10,... | collective-permute-start | bytes 1179656 | tf_op jit(solution)/shard_map/ppermute | solution.py:31
  108.7 17.9 %all-to-all-start.1 = ((bf16[32,24,256]{2,1,0:T(8,128)(2,1)}), bf16[32,24,256]{2,1,0:T(8,128)(2,1)S(1)}, u32[]{:S(2)}, u32[]{:S(2)}) async-start(bf16[32,24,256]{2,1,0:T(8,128)(2,1)} %bitcast.248), calls=%async_computation.1 | async-start | bytes 786432 | tf_op jit(solution)/shard_map/all_to_all | solution.py:43
  128.2 12.0 %copy-start.41 = (bf16[128,512]{1,0:T(8,128)(2,1)S(1)}, bf16[128,512]{1,0:T(8,128)(2,1)}, u32[]{:S(2)}) copy-start(bf16[128,512]{1,0:T(8,128)(2,1)} %param.23) | copy-start | bytes 393220
  128.3 1.4 collective-permute-start.13
  129.7 8.0 %collective-permute-start.15 = (bf16[128,512]{0,1:T(8,128)(2,1)S(1)}, bf16[128,512]{0,1:T(8,128)(2,1)S(1)}, u32[]{:S(2)}, u32[]{:S(2)}) collective-permute-start(bf16[128,512]{0,1:T(8,128)(2,1)S(1)} %fusion.61), channel_id=1, source_target_pairs={{0,2},{1,3},{2,0},{3,1},{4,6},{5,7},{6,4},{7,5},{8,10},{9,11},{10,... | collective-permute-start | bytes 393224 | tf_op jit(solution)/shard_map/ppermute | solution.py:31
  130.8 8.9 %collective-permute-start.16 = (bf16[128,512]{0,1:T(8,128)(2,1)S(1)}, bf16[128,512]{0,1:T(8,128)(2,1)S(1)}, u32[]{:S(2)}, u32[]{:S(2)}) collective-permute-start(bf16[128,512]{0,1:T(8,128)(2,1)S(1)} %fusion.61), channel_id=1, source_target_pairs={{0,1},{1,2},{2,3},{3,0},{4,5},{5,6},{6,7},{7,4},{8,9},{9,10},{10,1... | collective-permute-start | bytes 393224 | tf_op jit(solution)/shard_map/ppermute | solution.py:31
  133.2 6.8 %collective-permute-start.14 = (bf16[128,512]{0,1:T(8,128)(2,1)S(1)}, bf16[128,512]{0,1:T(8,128)(2,1)S(1)}, u32[]{:S(2)}, u32[]{:S(2)}) collective-permute-start(bf16[128,512]{0,1:T(8,128)(2,1)S(1)} %fusion.61), channel_id=1, source_target_pairs={{0,3},{1,0},{2,1},{3,2},{4,7},{5,4},{6,5},{7,6},{8,11},{9,8},{10,9... | collective-permute-start | bytes 393224 | tf_op jit(solution)/shard_map/ppermute | solution.py:31
  142.3 1.3 collective-permute-start.25
  142.4 2.1 %collective-permute-start.17 = (bf16[128,2048]{0,1:T(8,128)(2,1)S(1)}, bf16[128,2048]{0,1:T(8,128)(2,1)S(1)}, u32[]{:S(2)}, u32[]{:S(2)}) collective-permute-start(bf16[128,2048]{0,1:T(8,128)(2,1)S(1)} %pad_maximum_fusion.8), channel_id=1, source_target_pairs={{0,4},{4,0},{1,5},{5,1},{2,6},{6,2},{3,7},{7,3},{8,12},{12,8},{9,1... | collective-permute-start | bytes 1572872 | tf_op jit(solution)/shard_map/ppermute | solution.py:26
  146.7 13.0 %collective-permute-start.20 = (bf16[8,32,512]{2,1,0:T(8,128)(2,1)}, bf16[8,32,512]{2,1,0:T(8,128)(2,1)}, u32[]{:S(2)}, u32[]{:S(2)}) collective-permute-start(bf16[8,32,512]{2,1,0:T(8,128)(2,1)} %bitcast.70), channel_id=1, source_target_pairs={{0,16},{8,24},{16,0},{24,8},{1,17},{9,25},{17,1},{25,9},{2,18},{10... | collective-permute-start | bytes 786440 | tf_op jit(solution)/shard_map/ppermute | solution.py:31
  148.5 13.6 %collective-permute-start.19 = (bf16[8,32,512]{2,1,0:T(8,128)(2,1)S(1)}, bf16[8,32,512]{2,1,0:T(8,128)(2,1)}, u32[]{:S(2)}, u32[]{:S(2)}) collective-permute-start(bf16[8,32,512]{2,1,0:T(8,128)(2,1)S(1)} %bitcast.257), channel_id=1, source_target_pairs={{0,24},{8,0},{16,8},{24,16},{1,25},{9,1},{17,9},{25,17},{2,26},{10... | collective-permute-start | bytes 786440 | tf_op jit(solution)/shard_map/ppermute | solution.py:31
  149.3 14.5 %collective-permute-start.18 = (bf16[8,32,512]{2,1,0:T(8,128)(2,1)S(1)}, bf16[8,32,512]{2,1,0:T(8,128)(2,1)}, u32[]{:S(2)}, u32[]{:S(2)}) collective-permute-start(bf16[8,32,512]{2,1,0:T(8,128)(2,1)S(1)} %bitcast.256), channel_id=1, source_target_pairs={{0,8},{8,16},{16,24},{24,0},{1,9},{9,17},{17,25},{25,1},{2,10},{10... | collective-permute-start | bytes 786440 | tf_op jit(solution)/shard_map/ppermute | solution.py:31
  151.3 21.6 %all-to-all-start.2 = ((bf16[32,40,128]{2,1,0:T(8,128)(2,1)}), bf16[32,40,128]{2,1,0:T(8,128)(2,1)S(1)}, u32[]{:S(2)}, u32[]{:S(2)}) async-start(bf16[32,40,128]{2,1,0:T(8,128)(2,1)} %pad_maximum_fusion.18), calls=%async_computation.2 | async-start | bytes 655360 | tf_op jit(solution)/shard_map/all_to_all | solution.py:43
  165.1 15.8 %collective-permute-start.21 = (bf16[4,32,512]{2,1,0:T(8,128)(2,1)S(1)}, bf16[4,32,512]{2,1,0:T(8,128)(2,1)S(1)}, u32[]{:S(2)}, u32[]{:S(2)}) collective-permute-start(bf16[4,32,512]{2,1,0:T(8,128)(2,1)S(1)} %fusion.74), channel_id=1, source_target_pairs={{0,32},{32,0},{64,96},{96,64},{128,160},{160,128},{192,224},{224,1... | collective-permute-start | bytes 393224 | tf_op jit(solution)/shard_map/ppermute | solution.py:519
  175.5 17.6 %all-to-all-start.3 = ((bf16[32,32,128]{2,1,0:T(8,128)(2,1)}), bf16[32,32,128]{2,1,0:T(8,128)(2,1)S(1)}, u32[]{:S(2)}, u32[]{:S(2)}) async-start(bf16[32,32,128]{2,1,0:T(8,128)(2,1)} %shard_map.199), calls=%async_computation.3 | async-start | bytes 524288 | tf_op jit(solution)/shard_map/all_to_all | solution.py:43
  181.0 15.3 %collective-permute-start.24 = (bf16[32,512]{1,0:T(8,128)(2,1)S(1)}, bf16[32,512]{1,0:T(8,128)(2,1)S(1)}, u32[]{:S(2)}, u32[]{:S(2)}) collective-permute-start(bf16[32,512]{1,0:T(8,128)(2,1)S(1)} %get-tuple-element.152), channel_id=1, source_target_pairs={{0,192},{32,224},{64,0},{96,32},{128,64},{160,96},{192,128},{224,1... | collective-permute-start | bytes 98312 | tf_op jit(solution)/shard_map/ppermute | solution.py:528
  184.8 11.5 %collective-permute-start.23 = (bf16[32,512]{1,0:T(8,128)(2,1)S(1)}, bf16[32,512]{1,0:T(8,128)(2,1)S(1)}, u32[]{:S(2)}, u32[]{:S(2)}) collective-permute-start(bf16[32,512]{1,0:T(8,128)(2,1)S(1)} %get-tuple-element.153), channel_id=1, source_target_pairs={{0,128},{32,160},{64,192},{96,224},{128,0},{160,32},{192,64},{224,... | collective-permute-start | bytes 98312 | tf_op jit(solution)/shard_map/ppermute | solution.py:528
  187.1 9.3 %collective-permute-start.22 = (bf16[32,512]{1,0:T(8,128)(2,1)S(1)}, bf16[32,512]{1,0:T(8,128)(2,1)S(1)}, u32[]{:S(2)}, u32[]{:S(2)}) collective-permute-start(bf16[32,512]{1,0:T(8,128)(2,1)S(1)} %get-tuple-element.151), channel_id=1, source_target_pairs={{0,64},{32,96},{64,128},{96,160},{128,192},{160,224},{192,0},{224,... | collective-permute-start | bytes 98312 | tf_op jit(solution)/shard_map/ppermute | solution.py:528
  196.3 1.6 collective-permute-start.26
  (38 other events, 123.8 us)

commit v4 on v3

--- a/solution.py
+++ b/solution.py
@@ -383,10 +383,9 @@
         axis=1,
     )
     cumul_row = jnp.cumsum(rates, axis=1)
-    spread_heads = (
-        lax.broadcasted_iota(jnp.int32, (half_heads, half), 1) // HEAD_DIM
-        == lax.broadcasted_iota(jnp.int32, (half_heads, half), 0)
-    ).astype(f32)
+    head_of = lax.broadcasted_iota(jnp.int32, (half_heads, half), 0) * HEAD_DIM
+    lane = lax.broadcasted_iota(jnp.int32, (half_heads, half), 1)
+    spread_heads = ((lane >= head_of) & (lane < head_of + HEAD_DIM)).astype(f32)
     cumul_wide = lax.dot_general(
         cumul_row,
         spread_heads,
@@ -402,13 +401,12 @@
     value_start = (value_f * fade_start).astype(bf16)
     write_states = to_message(dot(write, value_end, 0, 0), dot(write, value_start, 0, 0))
     total_high = lax.reduce_precision(total_wide, 8, 7)
-    total_rows = jnp.concatenate(
-        [total_high, total_wide - total_high, jnp.zeros((6, half), f32)], axis=0
-    ).astype(bf16)
-    total_rows = jnp.broadcast_to(
-        total_rows.reshape(8, half // 128, 1, 128).transpose(1, 2, 0, 3),
-        (half // 128, STATE // 8, 8, 128),
-    ).reshape(-1, 8, 128)
+    row = lax.broadcasted_iota(jnp.int32, (8, half), 0)
+    total_low = total_wide - total_high
+    total_rows = jnp.where(row == 0, total_high, jnp.where(row == 1, total_low, 0.0)).astype(bf16)
+    total_rows = total_rows.reshape(8, half // 128, 1, 128).transpose(1, 2, 0, 3)
+    total_rows = jnp.broadcast_to(total_rows, (half // 128, STATE // 8, 8, 128))
+    total_rows = total_rows.reshape(-1, 8, 128)
     quarter = width
 
     def rolled(a):
@@ -435,6 +433,11 @@
     proj = rolled(proj_weight)
     hid = gate_weight.shape[2]
     received = exchange(sent.reshape(chips, 2 * rows, width)).reshape(2 * slots, width)
+    ready = (write, read, value, gated_all, fade_end, fade_start, value_end, value_start)
+    ready += (write_states, total_rows, cumul_wide, cumul_row)
+    received, ready = lax.optimization_barrier((received, ready))
+    write, read, value, gated_all, fade_end, fade_start, value_end, value_start = ready[:8]
+    write_states, total_rows, cumul_wide, cumul_row = ready[8:]
     input_own, cotangent_own = (dot(a, received).astype(bf16) for a in sort_rows)
     input_low = ring(input_own, 1)
     cotangent_up = ring(cotangent_own, -1)
@@ -453,14 +456,8 @@
     deltas = jnp.concatenate(
         [(hidden_grad * pre_up * slope).astype(bf16), (hidden_grad * active).astype(bf16)], axis=1
     )
-    ready = (write, read, value, gated_all, fade_end, fade_start, value_end, value_start)
-    ready += (write_states, total_rows, cumul_wide, cumul_row)
-    deltas, ready = lax.optimization_barrier((deltas, ready))
-    write, read, value, gated_all, fade_end, fade_start, value_end, value_start = ready[:8]
-    write_states, total_rows, cumul_wide, cumul_row = ready[8:]
-    partial = [dot(deltas, gate_up[i], 1, 1).astype(bf16) for i in range(n_tp)]
-    own, right, far, left = partial
-    opposite = ring(far, 2)
+    opposite = ring(dot(deltas, gate_up[2], 1, 1).astype(bf16), 2)
+    right, left, own = (dot(deltas, gate_up[i], 1, 1).astype(bf16) for i in (1, 3, 0))
     returned = spread(own, ring(right, 1), ring(left, -1), opposite)
     returned, deltas, hidden = lax.optimization_barrier((returned, deltas, hidden))
     cut = width // 2

time: 204 us -> 216 us (1.059)
  matrix products: 22.8 us -> 29 us
  waiting for transfers between devices: 58.6 us -> 63.3 us
    dot_general x33, matrix products: 22.5 us -> 28.7 us  [dot(): lax.dot_general(a, b, (((ca,), (cb,)), ((), ())), preferred_element_type=...]
    all_to_all x4, waiting for transfers between devices: 18 us -> 22.1 us  [exchange(): return lax.all_to_all(x, CHIPS, split_axis=0, concat_axis=0, tiled=True)]
    slice x4, local copies, waits for them, and re-layouts: 0.15 us -> 3.3 us  [on_device(): up_grad = jnp.concatenate([a[:, hid:] for a in both_grad], axis=0)[None]]
    unnamed x112 -> x132, local copies, waits for them, and re-layouts: 6.43 us -> 4.72 us
  transfers between devices with their start and end apart: 31 -> 31, of which waited for: 16 -> 16; matrix products, arithmetic and copies ran while one was open for 19% -> 18% of each run, Pallas kernels for 4% -> 3%
where the time goes in v4:
time: 216 us; the launch traced here: 214 us
  starting transfers between devices  64.7 us (30%)
  waiting for transfers between devices  63.3 us (29%)
  matrix products  29 us (13%)
  other arithmetic  24.9 us (12%)
  Pallas kernels  16 us (7%)
  local copies, waits for them, and re-layouts  13.8 us (6%)
    ppermute x15, waiting for transfers between devices, ring(): return lax.ppermute(x, axis, [(i, (i + shift) % n) for i in range(n)])  39 us
    all_to_all x4, starting transfers between devices, exchange(): return lax.all_to_all(x, CHIPS, split_axis=0, concat_axis=0, tiled=True)  31.3 us
    dot_general x33, matrix products, dot(): lax.dot_general(a, b, (((ca,), (cb,)), ((), ())), preferred_element_type=...  28.7 us
    all_to_all x4, waiting for transfers between devices, exchange(): return lax.all_to_all(x, CHIPS, split_axis=0, concat_axis=0, tiled=True)  22.1 us
    ppermute x15, starting transfers between devices, ring(): return lax.ppermute(x, axis, [(i, (i + shift) % n) for i in range(n)])  20.7 us
    ppermute x3, starting transfers between devices, on_device(): lax.ppermute(level_part(k).astype(bf16), SP[0], [(i, (i + 2 * k) % deep)...  9.69 us
    unnamed x132, local copies, waits for them, and re-layouts  4.72 us
  transfers between devices with their start and end apart: 31, of which 16 were waited for; matrix products, arithmetic and copies ran while one was open for 18% of the time, Pallas kernels for 3%

profile of v4, /device:TPU:4, one launch (start us, length us, event | category | flops | bytes accessed | tf_op | source)
XLA Modules:
  0.0 213.7 jit_solution(11079346134981629910)
XLA Ops:
  2.9 1.4 fusion.4
  6.2 3.4 %shard_map.197 = (bf16[768,512]{1,0:T(8,128)(2,1)}, s32[8,256]{1,0:T(8,128)}) custom-call(s32[1]{0:T(128)} %bitcast.core_ref, f32[12,128]{1,0:T(8,128)} %copy-done.57, f32[12,128]{1,0:T(8,128)} %copy-done.59, bf16[128,512]{1,0:T(8,128)(2,1)} %x_ref.1, bf16[128,512]{1,0:T(8,128)(2,1)} %copy-done.52, bf16[128,512]{1,0:T(8,128)(2,1)} %c_ref.1, ...), custom_call_target="tpu_custom_call" | custom-call | tf_op jit(solution)/shard_map/pallas_call | solution.py:105
  10.7 1.5 pad_maximum_fusion.20
  13.4 11.6 %all-to-all-start = ((bf16[32,24,512]{2,1,0:T(8,128)(2,1)}), bf16[32,24,512]{2,1,0:T(8,128)(2,1)}, u32[]{:S(2)}, u32[]{:S(2)}) async-start(bf16[32,24,512]{2,1,0:T(8,128)(2,1)} %bitcast.247), calls=%async_computation | async-start | bytes 1572864 | tf_op jit(solution)/shard_map/all_to_all | solution.py:43
  25.2 2.6 %dynamic-slice_bitcast_fusion.10 = (bf16[512,256]{1,0:T(8,128)(2,1)}, bf16[512,256]{1,0:T(8,128)(2,1)}, bf16[512,256]{1,0:T(8,128)(2,1)}, bf16[512,256]{1,0:T(8,...) fusion(bf16[4,512,256]{2,1,0:T(8,128)(2,1)S(1)} %bitcast.243, ...), kind=kLoop, calls=%fused_computation.154 | loop fusion | bytes 4194320 | tf_op jit(solution)/shard_map/jit(dynamic_index_in_dim)/squeeze | solution.py:415
  28.5 1.6 add_convert_fusion
  39.4 8.4 %all-to-all-done = bf16[32,24,512]{2,1,0:T(8,128)(2,1)} async-done(((bf16[32,24,512]{2,1,0:T(8,128)(2,1)}), bf16[32,24,512]{2,1,0:T(8,128)(2,1)}, u32[]{:S(2)}, u32[]{:S(2)}) %all-to-all-start) | async-done | bytes 786464 | tf_op jit(solution)/shard_map/all_to_all | solution.py:43
  48.5 1.8 convolution_convert_fusion.10
  50.4 3.1 %collective-permute-start.4 = (bf16[384,512]{1,0:T(8,128)(2,1)S(1)}, bf16[384,512]{1,0:T(8,128)(2,1)S(1)}, u32[]{:S(2)}, u32[]{:S(2)}) collective-permute-start(bf16[384,512]{1,0:T(8,128)(2,1)S(1)} %convolution_convert_fusion.10), channel_id=1, source_target_pairs={{0,3},{1,0},{2,1},{3,2},{4,7},{5,4},{6,5},{7,6},{8,11},{9,8},{10,9... | collective-permute-start | bytes 1179656 | tf_op jit(solution)/shard_map/ppermute | solution.py:31
  53.5 1.8 convolution_convert_fusion.9
  55.3 3.3 %collective-permute-start.7 = (bf16[384,512]{1,0:T(8,128)(2,1)S(1)}, bf16[384,512]{1,0:T(8,128)(2,1)S(1)}, u32[]{:S(2)}, u32[]{:S(2)}) collective-permute-start(bf16[384,512]{1,0:T(8,128)(2,1)S(1)} %convolution_convert_fusion.9), channel_id=1, source_target_pairs={{0,3},{1,0},{2,1},{3,2},{4,7},{5,4},{6,5},{7,6},{8,11},{9,8},{10,9... | collective-permute-start | bytes 1179656 | tf_op jit(solution)/shard_map/ppermute | solution.py:31
  59.4 3.5 %collective-permute-done.4 = bf16[384,512]{1,0:T(8,128)(2,1)S(1)} collective-permute-done((bf16[384,512]{1,0:T(8,128)(2,1)S(1)}, bf16[384,512]{1,0:T(8,128)(2,1)S(1)}, u32[]{:S(2)}, u32[]{:S(2)}) %collective-permute-start.4) | collective-permute-done | bytes 393248 | tf_op jit(solution)/shard_map/ppermute | solution.py:31
  63.0 3.7 %collective-permute-start.6 = (bf16[384,512]{1,0:T(8,128)(2,1)S(1)}, bf16[384,512]{1,0:T(8,128)(2,1)S(1)}, u32[]{:S(2)}, u32[]{:S(2)}) collective-permute-start(bf16[384,512]{1,0:T(8,128)(2,1)S(1)} %collective-permute-done.4), channel_id=1, source_target_pairs={{0,3},{1,0},{2,1},{3,2},{4,7},{5,4},{6,5},{7,6},{8,11},{9,8},{10,9... | collective-permute-start | bytes 1179656 | tf_op jit(solution)/shard_map/ppermute | solution.py:31
  66.7 5.6 %collective-permute-done.8 = bf16[384,512]{1,0:T(8,128)(2,1)S(1)} collective-permute-done((bf16[384,512]{1,0:T(8,128)(2,1)S(1)}, bf16[384,512]{1,0:T(8,128)(2,1)S(1)}, u32[]{:S(2)}, u32[]{:S(2)}) %collective-permute-start.8) | collective-permute-done | bytes 393248 | tf_op jit(solution)/shard_map/ppermute | solution.py:31
  74.1 7.7 %collective-permute-done.9 = bf16[384,512]{1,0:T(8,128)(2,1)S(1)} collective-permute-done((bf16[384,512]{1,0:T(8,128)(2,1)S(1)}, bf16[384,512]{1,0:T(8,128)(2,1)S(1)}, u32[]{:S(2)}, u32[]{:S(2)}) %collective-permute-start.9) | collective-permute-done | bytes 393248 | tf_op jit(solution)/shard_map/ppermute | solution.py:31
  86.4 1.7 collective-permute-start.11
  89.6 2.3 %convolution_convert_fusion.8.own_ref = bf16[384,512]{1,0:T(8,128)(2,1)} fusion(bf16[512,256]{1,0:T(8,128)(2,1)S(1)} %copy-done.37, bf16[512,256]{1,0:T(8,128)(2,1)} %get-tuple-element.174, bf16[384,256]{0,1:T(8,128)(2,1)} %copy-done.51, bf16[384,256]{0,1:T(8,128)(2,1)} %copy-done.50), kind=kOutput, calls=%fused_computation.12 | convolution fusion | flops 203358208 | bytes 1310720 | tf_op jit(solution)/shard_map/dot_general | solution.py:22
  91.9 8.0 %collective-permute-done.12.far_ref = bf16[384,512]{1,0:T(8,128)(2,1)} collective-permute-done((bf16[384,512]{1,0:T(8,128)(2,1)}, bf16[384,512]{1,0:T(8,128)(2,1)}, u32[]{:S(2)}, u32[]{:S(2)}) %collective-permute-start.12) | collective-permute-done | bytes 393248 | tf_op jit(solution)/shard_map/ppermute | solution.py:31
  99.9 1.3 collective-permute-done.11.up_ref
  101.3 2.8 %collective-permute-done.10.low_ref = bf16[384,512]{1,0:T(8,128)(2,1)} collective-permute-done((bf16[384,512]{1,0:T(8,128)(2,1)}, bf16[384,512]{1,0:T(8,128)(2,1)}, u32[]{:S(2)}, u32[]{:S(2)}) %collective-permute-start.10) | collective-permute-done | bytes 393248 | tf_op jit(solution)/shard_map/ppermute | solution.py:31
  104.1 3.6 %shard_map.198 = bf16[768,256]{1,0:T(8,128)(2,1)} custom-call(bf16[384,512]{1,0:T(8,128)(2,1)} %convolution_convert_fusion.8.own_ref, bf16[384,512]{1,0:T(8,128)(2,1)} %collective-permute-done.10.low_ref, bf16[384,512]{1,0:T(8,128)(2,1)} %collective-permute-done.11.up_ref, bf16[384,512]{1,0:T(8,128)(2,1)} %collective-permute-done.12.far_ref), custom_call_target="tpu_custom_call" | custom-call | tf_op jit(solution)/shard_map/pallas_call | solution.py:147
  107.7 1.4 fusion.6
  109.1 1.5 fusion
  115.8 8.0 %all-to-all-start.1 = ((bf16[32,24,256]{2,1,0:T(8,128)(2,1)}), bf16[32,24,256]{2,1,0:T(8,128)(2,1)S(1)}, u32[]{:S(2)}, u32[]{:S(2)}) async-start(bf16[32,24,256]{2,1,0:T(8,128)(2,1)} %bitcast.242), calls=%async_computation.1 | async-start | bytes 786432 | tf_op jit(solution)/shard_map/all_to_all | solution.py:43
  123.9 1.3 fusion.7
  125.2 1.3 fusion.8
  126.5 1.3 fusion.9
  131.3 6.8 %all-to-all-done.1 = bf16[32,24,256]{2,1,0:T(8,128)(2,1)S(1)} async-done(((bf16[32,24,256]{2,1,0:T(8,128)(2,1)}), bf16[32,24,256]{2,1,0:T(8,128)(2,1)S(1)}, u32[]{:S(2)}, u32[]{:S(2)}) %all-to-all-start.1) | async-done | bytes 393248 | tf_op jit(solution)/shard_map/all_to_all | solution.py:43
  138.1 1.3 fusion.109
  139.4 1.3 fusion.108
  142.7 3.2 %collective-permute-start.14 = (bf16[128,512]{0,1:T(8,128)(2,1)S(1)}, bf16[128,512]{0,1:T(8,128)(2,1)S(1)}, u32[]{:S(2)}, u32[]{:S(2)}) collective-permute-start(bf16[128,512]{0,1:T(8,128)(2,1)S(1)} %fusion.61), channel_id=1, source_target_pairs={{0,3},{1,0},{2,1},{3,2},{4,7},{5,4},{6,5},{7,6},{8,11},{9,8},{10,9... | collective-permute-start | bytes 393224 | tf_op jit(solution)/shard_map/ppermute | solution.py:31
  145.9 4.4 %collective-permute-done.15 = bf16[128,512]{0,1:T(8,128)(2,1)S(1)} collective-permute-done((bf16[128,512]{0,1:T(8,128)(2,1)S(1)}, bf16[128,512]{0,1:T(8,128)(2,1)S(1)}, u32[]{:S(2)}, u32[]{:S(2)}) %collective-permute-start.15) | collective-permute-done | bytes 131104 | tf_op jit(solution)/shard_map/ppermute | solution.py:31
  150.5 1.7 collective-permute-done.16
  152.8 2.0 fusion.48
  157.0 1.6 convolution_convert_fusion
  162.2 2.7 %collective-permute-start.20 = (bf16[8,32,512]{2,1,0:T(8,128)(2,1)S(1)}, bf16[8,32,512]{2,1,0:T(8,128)(2,1)}, u32[]{:S(2)}, u32[]{:S(2)}) collective-permute-start(bf16[8,32,512]{2,1,0:T(8,128)(2,1)S(1)} %bitcast.250), channel_id=1, source_target_pairs={{0,16},{8,24},{16,0},{24,8},{1,17},{9,25},{17,1},{25,9},{2,18},{10... | collective-permute-start | bytes 786440 | tf_op jit(solution)/shard_map/ppermute | solution.py:31
  165.7 6.0 %all-to-all-start.2 = ((bf16[32,40,128]{2,1,0:T(8,128)(2,1)}), bf16[32,40,128]{2,1,0:T(8,128)(2,1)S(1)}, u32[]{:S(2)}, u32[]{:S(2)}) async-start(bf16[32,40,128]{2,1,0:T(8,128)(2,1)} %pad_maximum_fusion.18), calls=%async_computation.2 | async-start | bytes 655360 | tf_op jit(solution)/shard_map/all_to_all | solution.py:43
  171.8 3.8 %collective-permute-done.20 = bf16[8,32,512]{2,1,0:T(8,128)(2,1)} collective-permute-done((bf16[8,32,512]{2,1,0:T(8,128)(2,1)S(1)}, bf16[8,32,512]{2,1,0:T(8,128)(2,1)}, u32[]{:S(2)}, u32[]{:S(2)}) %collective-permute-start.20) | collective-permute-done | bytes 262176 | tf_op jit(solution)/shard_map/ppermute | solution.py:31
  175.5 1.3 fusion.32
  178.1 6.9 %all-to-all-done.2.msg_ref = bf16[32,40,128]{2,1,0:T(8,128)(2,1)S(1)} async-done(((bf16[32,40,128]{2,1,0:T(8,128)(2,1)}), bf16[32,40,128]{2,1,0:T(8,128)(2,1)S(1)}, u32[]{:S(2)}, u32[]{:S(2)}) %all-to-all-start.2) | async-done | bytes 327712 | tf_op jit(solution)/shard_map/all_to_all | solution.py:43
  185.7 1.8 shard_map.199
  187.5 5.5 %all-to-all-start.3 = ((bf16[32,32,128]{2,1,0:T(8,128)(2,1)}), bf16[32,32,128]{2,1,0:T(8,128)(2,1)S(1)}, u32[]{:S(2)}, u32[]{:S(2)}) async-start(bf16[32,32,128]{2,1,0:T(8,128)(2,1)} %shard_map.199), calls=%async_computation.3 | async-start | bytes 524288 | tf_op jit(solution)/shard_map/all_to_all | solution.py:43
  193.2 2.5 %collective-permute-start.22 = (bf16[32,512]{1,0:T(8,128)(2,1)S(1)}, bf16[32,512]{1,0:T(8,128)(2,1)S(1)}, u32[]{:S(2)}, u32[]{:S(2)}) collective-permute-start(bf16[32,512]{1,0:T(8,128)(2,1)S(1)} %get-tuple-element.151), channel_id=1, source_target_pairs={{0,64},{32,96},{64,128},{96,160},{128,192},{160,224},{192,0},{224,... | collective-permute-start | bytes 98312 | tf_op jit(solution)/shard_map/ppermute | solution.py:525
  195.7 3.7 %collective-permute-start.23 = (bf16[32,512]{1,0:T(8,128)(2,1)S(1)}, bf16[32,512]{1,0:T(8,128)(2,1)S(1)}, u32[]{:S(2)}, u32[]{:S(2)}) collective-permute-start(bf16[32,512]{1,0:T(8,128)(2,1)S(1)} %get-tuple-element.153), channel_id=1, source_target_pairs={{0,128},{32,160},{64,192},{96,224},{128,0},{160,32},{192,64},{224,... | collective-permute-start | bytes 98312 | tf_op jit(solution)/shard_map/ppermute | solution.py:525
  199.4 3.5 %collective-permute-start.24 = (bf16[32,512]{1,0:T(8,128)(2,1)S(1)}, bf16[32,512]{1,0:T(8,128)(2,1)S(1)}, u32[]{:S(2)}, u32[]{:S(2)}) collective-permute-start(bf16[32,512]{1,0:T(8,128)(2,1)S(1)} %get-tuple-element.152), channel_id=1, source_target_pairs={{0,192},{32,224},{64,0},{96,32},{128,64},{160,96},{192,128},{224,1... | collective-permute-start | bytes 98312 | tf_op jit(solution)/shard_map/ppermute | solution.py:525
  203.6 2.9 %shard_map.200.base_ref = f32[256,512]{1,0:T(8,128)} custom-call(bf16[256,256]{1,0:T(8,128)(2,1)} %pad_maximum_fusion.24.delta_ref, bf16[256,256]{1,0:T(8,128)(2,1)} %pad_maximum_fusion.22.value_ref, bf16[256,128]{1,0:T(8,128)(2,1)} %pad_maximum_fusion.26.write_ref, bf16[256,128]{1,0:T(8,128)(2,1)} %pad_maximum_fusion.27.read_ref, f32[256,256]{1,0:T(8,128)} %copy-done.1, ...), custom_call_target="tpu_custom_call" | custom-call | tf_op jit(solution)/shard_map/pallas_call | solution.py:173
  207.1 2.6 %shard_map.201 = (f32[128,512]{1,0:T(8,128)}, bf16[128,512]{1,0:T(8,128)(2,1)}) custom-call(s32[1]{0:T(128)} %bitcast.core_ref, bf16[32,32,128]{2,1,0:T(8,128)(2,1)} %copy-done.20, bf16[256,128]{1,0:T(8,128)(2,1)} %pad_maximum_fusion.26.write_ref, bf16[256,256]{1,0:T(8,128)(2,1)} %copy-done.18, bf16[256,256]{1,0:T(8,128)(2,1)} %copy-done.17, ...), custom_call_target="tpu_custom_call" | custom-call | tf_op jit(solution)/shard_map/pallas_call | solution.py:274
  212.0 1.7 shard_map.202
  (259 shorter events, 48.8 us)
Async XLA Ops:
  0.6 149.6 %copy-start = (bf16[2048,512]{1,0:T(8,128)(2,1)S(1)}, bf16[2048,512]{1,0:T(8,128)(2,1)}, u32[]{:S(2)}) copy-start(bf16[2048,512]{1,0:T(8,128)(2,1)} %param.24) | copy-start | bytes 6291460
  2.2 3.3 %collective-permute-start = (f32[12,128]{1,0:T(8,128)S(1)}, f32[12,128]{1,0:T(8,128)S(1)}, u32[]{:S(2)}, u32[]{:S(2)}) collective-permute-start(f32[12,128]{1,0:T(8,128)S(1)} %pad_maximum_fusion.28.mine_ref), channel_id=1, source_target_pairs={{0,4},{4,0},{1,5},{5,1},{2,6},{6,2},{3,7},{7,3},{8,12},{12,8},{9,1... | collective-permute-start | bytes 18440 | tf_op jit(solution)/shard_map/ppermute | solution.py:26
  2.3 3.2 %collective-permute-start.1 = (bf16[128,512]{1,0:T(8,128)(2,1)}, bf16[128,512]{1,0:T(8,128)(2,1)S(1)}, u32[]{:S(2)}, u32[]{:S(2)}) collective-permute-start(bf16[128,512]{1,0:T(8,128)(2,1)} %x_ref.1), channel_id=1, source_target_pairs={{0,4},{4,0},{1,5},{5,1},{2,6},{6,2},{3,7},{7,3},{8,12},{12,8},{9,1... | collective-permute-start | bytes 393224 | tf_op jit(solution)/shard_map/ppermute | solution.py:26
  2.8 2.7 %collective-permute-start.2 = (bf16[128,512]{1,0:T(8,128)(2,1)}, bf16[128,512]{1,0:T(8,128)(2,1)S(1)}, u32[]{:S(2)}, u32[]{:S(2)}) collective-permute-start(bf16[128,512]{1,0:T(8,128)(2,1)} %c_ref.1), channel_id=1, source_target_pairs={{0,4},{4,0},{1,5},{5,1},{2,6},{6,2},{3,7},{7,3},{8,12},{12,8},{9,1... | collective-permute-start | bytes 393224 | tf_op jit(solution)/shard_map/ppermute | solution.py:26
  2.9 22.1 %copy-start.21 = (bf16[1,2048,256]{2,1,0:T(8,128)(2,1)S(1)}, bf16[1,2048,256]{2,1,0:T(8,128)(2,1)}, u32[]{:S(2)}) copy-start(bf16[1,2048,256]{2,1,0:T(8,128)(2,1)} %param.19) | copy-start | bytes 3145732
  12.2 17.9 %collective-permute-start.3 = (bf16[128,1024]{1,0:T(8,128)(2,1)}, bf16[128,1024]{1,0:T(8,128)(2,1)}, u32[]{:S(2)}, u32[]{:S(2)}) collective-permute-start(bf16[128,1024]{1,0:T(8,128)(2,1)} %pad_maximum_fusion.20), channel_id=1, source_target_pairs={{0,4},{4,0},{1,5},{5,1},{2,6},{6,2},{3,7},{7,3},{8,12},{12,8},{9,1... | collective-permute-start | bytes 786440 | tf_op jit(solution)/shard_map/ppermute | solution.py:26
  13.4 34.4 %all-to-all-start = ((bf16[32,24,512]{2,1,0:T(8,128)(2,1)}), bf16[32,24,512]{2,1,0:T(8,128)(2,1)}, u32[]{:S(2)}, u32[]{:S(2)}) async-start(bf16[32,24,512]{2,1,0:T(8,128)(2,1)} %bitcast.247), calls=%async_computation | async-start | bytes 1572864 | tf_op jit(solution)/shard_map/all_to_all | solution.py:43
  32.9 17.4 %copy-start.1 = (f32[256,256]{1,0:T(8,128)}, f32[256,256]{1,0:T(8,128)S(1)}, u32[]{:S(2)}) copy-start(f32[256,256]{1,0:T(8,128)S(1)} %fusion.88.wide_ref) | copy-start | bytes 786436
  35.5 18.0 %copy-start.17 = (bf16[256,256]{1,0:T(8,128)(2,1)}, bf16[256,256]{1,0:T(8,128)(2,1)S(1)}, u32[]{:S(2)}) copy-start(bf16[256,256]{1,0:T(8,128)(2,1)S(1)} %get-tuple-element.91.value_end_ref) | copy-start | bytes 393220
  35.5 18.0 %copy-start.18 = (bf16[256,256]{1,0:T(8,128)(2,1)}, bf16[256,256]{1,0:T(8,128)(2,1)S(1)}, u32[]{:S(2)}) copy-start(bf16[256,256]{1,0:T(8,128)(2,1)S(1)} %get-tuple-element.90.value_start_ref) | copy-start | bytes 393220
  35.5 120.6 %copy-start.2 = (f32[256,256]{1,0:T(8,128)}, f32[256,256]{1,0:T(8,128)S(1)}, u32[]{:S(2)}) copy-start(f32[256,256]{1,0:T(8,128)S(1)} %get-tuple-element.85.fade_end_ref) | copy-start | bytes 786436
  35.5 120.6 %copy-start.3 = (f32[256,256]{1,0:T(8,128)}, f32[256,256]{1,0:T(8,128)S(1)}, u32[]{:S(2)}) copy-start(f32[256,256]{1,0:T(8,128)S(1)} %get-tuple-element.86.fade_start_ref) | copy-start | bytes 786436
  50.3 22.0 %copy-start.30 = (bf16[512,256]{1,0:T(8,128)(2,1)S(1)}, bf16[512,256]{1,0:T(8,128)(2,1)}, u32[]{:S(2)}) copy-start(bf16[512,256]{1,0:T(8,128)(2,1)} %get-tuple-element.131) | copy-start | bytes 786436
  50.4 22.0 %copy-start.31 = (bf16[512,256]{1,0:T(8,128)(2,1)S(1)}, bf16[512,256]{1,0:T(8,128)(2,1)}, u32[]{:S(2)}) copy-start(bf16[512,256]{1,0:T(8,128)(2,1)} %get-tuple-element.175) | copy-start | bytes 786436
  50.4 12.6 %collective-permute-start.4 = (bf16[384,512]{1,0:T(8,128)(2,1)S(1)}, bf16[384,512]{1,0:T(8,128)(2,1)S(1)}, u32[]{:S(2)}, u32[]{:S(2)}) collective-permute-start(bf16[384,512]{1,0:T(8,128)(2,1)S(1)} %convolution_convert_fusion.10), channel_id=1, source_target_pairs={{0,3},{1,0},{2,1},{3,2},{4,7},{5,4},{6,5},{7,6},{8,11},{9,8},{10,9... | collective-permute-start | bytes 1179656 | tf_op jit(solution)/shard_map/ppermute | solution.py:31
  53.5 20.3 %collective-permute-start.5 = (bf16[384,512]{1,0:T(8,128)(2,1)S(1)}, bf16[384,512]{1,0:T(8,128)(2,1)S(1)}, u32[]{:S(2)}, u32[]{:S(2)}) collective-permute-start(bf16[384,512]{1,0:T(8,128)(2,1)S(1)} %convolution_convert_fusion.10), channel_id=1, source_target_pairs={{0,1},{1,2},{2,3},{3,0},{4,5},{5,6},{6,7},{7,4},{8,9},{9,10},{10,1... | collective-permute-start | bytes 1179656 | tf_op jit(solution)/shard_map/ppermute | solution.py:31
  55.3 17.0 %copy-start.13 = (bf16[384,512]{1,0:T(8,128)(2,1)}, bf16[384,512]{1,0:T(8,128)(2,1)S(1)}, u32[]{:S(2)}) copy-start(bf16[384,512]{1,0:T(8,128)(2,1)S(1)} %convolution_convert_fusion.9) | copy-start | bytes 1179652
  55.3 17.0 %collective-permute-start.7 = (bf16[384,512]{1,0:T(8,128)(2,1)S(1)}, bf16[384,512]{1,0:T(8,128)(2,1)S(1)}, u32[]{:S(2)}, u32[]{:S(2)}) collective-permute-start(bf16[384,512]{1,0:T(8,128)(2,1)S(1)} %convolution_convert_fusion.9), channel_id=1, source_target_pairs={{0,3},{1,0},{2,1},{3,2},{4,7},{5,4},{6,5},{7,6},{8,11},{9,8},{10,9... | collective-permute-start | bytes 1179656 | tf_op jit(solution)/shard_map/ppermute | solution.py:31
  58.6 13.7 %collective-permute-start.8 = (bf16[384,512]{1,0:T(8,128)(2,1)S(1)}, bf16[384,512]{1,0:T(8,128)(2,1)S(1)}, u32[]{:S(2)}, u32[]{:S(2)}) collective-permute-start(bf16[384,512]{1,0:T(8,128)(2,1)S(1)} %convolution_convert_fusion.9), channel_id=1, source_target_pairs={{0,1},{1,2},{2,3},{3,0},{4,5},{5,6},{6,7},{7,4},{8,9},{9,10},{10,1... | collective-permute-start | bytes 1179656 | tf_op jit(solution)/shard_map/ppermute | solution.py:31
  58.9 13.9 %copy-start.32 = (bf16[512,256]{1,0:T(8,128)(2,1)S(1)}, bf16[512,256]{1,0:T(8,128)(2,1)}, u32[]{:S(2)}) copy-start(bf16[512,256]{1,0:T(8,128)(2,1)} %get-tuple-element.130) | copy-start | bytes 786436
  58.9 13.9 %copy-start.33 = (bf16[512,256]{1,0:T(8,128)(2,1)S(1)}, bf16[512,256]{1,0:T(8,128)(2,1)}, u32[]{:S(2)}) copy-start(bf16[512,256]{1,0:T(8,128)(2,1)} %get-tuple-element.176) | copy-start | bytes 786436
  63.0 19.8 %copy-start.10 = (bf16[384,512]{1,0:T(8,128)(2,1)}, bf16[384,512]{1,0:T(8,128)(2,1)S(1)}, u32[]{:S(2)}) copy-start(bf16[384,512]{1,0:T(8,128)(2,1)S(1)} %collective-permute-done.4) | copy-start | bytes 1179652
  63.0 19.3 %collective-permute-start.6 = (bf16[384,512]{1,0:T(8,128)(2,1)S(1)}, bf16[384,512]{1,0:T(8,128)(2,1)S(1)}, u32[]{:S(2)}, u32[]{:S(2)}) collective-permute-start(bf16[384,512]{1,0:T(8,128)(2,1)S(1)} %collective-permute-done.4), channel_id=1, source_target_pairs={{0,3},{1,0},{2,1},{3,2},{4,7},{5,4},{6,5},{7,6},{8,11},{9,8},{10,9... | collective-permute-start | bytes 1179656 | tf_op jit(solution)/shard_map/ppermute | solution.py:31
  72.3 9.5 %collective-permute-start.9 = (bf16[384,512]{1,0:T(8,128)(2,1)S(1)}, bf16[384,512]{1,0:T(8,128)(2,1)S(1)}, u32[]{:S(2)}, u32[]{:S(2)}) collective-permute-start(bf16[384,512]{1,0:T(8,128)(2,1)S(1)} %collective-permute-done.8), channel_id=1, source_target_pairs={{0,1},{1,2},{2,3},{3,0},{4,5},{5,6},{6,7},{7,4},{8,9},{9,10},{10,1... | collective-permute-start | bytes 1179656 | tf_op jit(solution)/shard_map/ppermute | solution.py:31
  73.7 12.6 %copy-start.11 = (bf16[384,512]{1,0:T(8,128)(2,1)}, bf16[384,512]{1,0:T(8,128)(2,1)S(1)}, u32[]{:S(2)}) copy-start(bf16[384,512]{1,0:T(8,128)(2,1)S(1)} %collective-permute-done.5) | copy-start | bytes 1179652
  86.3 13.6 %collective-permute-start.12 = (bf16[384,512]{1,0:T(8,128)(2,1)}, bf16[384,512]{1,0:T(8,128)(2,1)}, u32[]{:S(2)}, u32[]{:S(2)}) collective-permute-start(bf16[384,512]{1,0:T(8,128)(2,1)} %convolution_convert_fusion.5), channel_id=1, source_target_pairs={{0,2},{1,3},{2,0},{3,1},{4,6},{5,7},{6,4},{7,5},{8,10},{9,11},{10,... | collective-permute-start | bytes 1179656 | tf_op jit(solution)/shard_map/ppermute | solution.py:31
  86.4 14.9 %collective-permute-start.11 = (bf16[384,512]{1,0:T(8,128)(2,1)}, bf16[384,512]{1,0:T(8,128)(2,1)}, u32[]{:S(2)}, u32[]{:S(2)}) collective-permute-start(bf16[384,512]{1,0:T(8,128)(2,1)} %convolution_convert_fusion.6), channel_id=1, source_target_pairs={{0,3},{1,0},{2,1},{3,2},{4,7},{5,4},{6,5},{7,6},{8,11},{9,8},{10,9... | collective-permute-start | bytes 1179656 | tf_op jit(solution)/shard_map/ppermute | solution.py:31
  88.1 16.0 %collective-permute-start.10 = (bf16[384,512]{1,0:T(8,128)(2,1)}, bf16[384,512]{1,0:T(8,128)(2,1)}, u32[]{:S(2)}, u32[]{:S(2)}) collective-permute-start(bf16[384,512]{1,0:T(8,128)(2,1)} %convolution_convert_fusion.7), channel_id=1, source_target_pairs={{0,1},{1,2},{2,3},{3,0},{4,5},{5,6},{6,7},{7,4},{8,9},{9,10},{10,1... | collective-permute-start | bytes 1179656 | tf_op jit(solution)/shard_map/ppermute | solution.py:31
  115.8 22.2 %all-to-all-start.1 = ((bf16[32,24,256]{2,1,0:T(8,128)(2,1)}), bf16[32,24,256]{2,1,0:T(8,128)(2,1)S(1)}, u32[]{:S(2)}, u32[]{:S(2)}) async-start(bf16[32,24,256]{2,1,0:T(8,128)(2,1)} %bitcast.242), calls=%async_computation.1 | async-start | bytes 786432 | tf_op jit(solution)/shard_map/all_to_all | solution.py:43
  140.7 1.4 collective-permute-start.13
  142.2 12.7 %copy-start.46 = (bf16[128,512]{0,1:T(8,128)(2,1)}, bf16[128,512]{0,1:T(8,128)(2,1)S(1)}, u32[]{:S(2)}) copy-start(bf16[128,512]{0,1:T(8,128)(2,1)S(1)} %fusion.61) | copy-start | bytes 393220
  142.2 8.0 %collective-permute-start.15 = (bf16[128,512]{0,1:T(8,128)(2,1)S(1)}, bf16[128,512]{0,1:T(8,128)(2,1)S(1)}, u32[]{:S(2)}, u32[]{:S(2)}) collective-permute-start(bf16[128,512]{0,1:T(8,128)(2,1)S(1)} %fusion.61), channel_id=1, source_target_pairs={{0,2},{1,3},{2,0},{3,1},{4,6},{5,7},{6,4},{7,5},{8,10},{9,11},{10,... | collective-permute-start | bytes 393224 | tf_op jit(solution)/shard_map/ppermute | solution.py:31
  142.6 9.6 %collective-permute-start.16 = (bf16[128,512]{0,1:T(8,128)(2,1)S(1)}, bf16[128,512]{0,1:T(8,128)(2,1)S(1)}, u32[]{:S(2)}, u32[]{:S(2)}) collective-permute-start(bf16[128,512]{0,1:T(8,128)(2,1)S(1)} %fusion.61), channel_id=1, source_target_pairs={{0,1},{1,2},{2,3},{3,0},{4,5},{5,6},{6,7},{7,4},{8,9},{9,10},{10,1... | collective-permute-start | bytes 393224 | tf_op jit(solution)/shard_map/ppermute | solution.py:31
  142.7 9.8 %collective-permute-start.14 = (bf16[128,512]{0,1:T(8,128)(2,1)S(1)}, bf16[128,512]{0,1:T(8,128)(2,1)S(1)}, u32[]{:S(2)}, u32[]{:S(2)}) collective-permute-start(bf16[128,512]{0,1:T(8,128)(2,1)S(1)} %fusion.61), channel_id=1, source_target_pairs={{0,3},{1,0},{2,1},{3,2},{4,7},{5,4},{6,5},{7,6},{8,11},{9,8},{10,9... | collective-permute-start | bytes 393224 | tf_op jit(solution)/shard_map/ppermute | solution.py:31
  154.8 1.3 collective-permute-start.25
  154.9 2.1 collective-permute-start.17
  160.1 11.6 %collective-permute-start.18 = (bf16[8,32,512]{2,1,0:T(8,128)(2,1)}, bf16[8,32,512]{2,1,0:T(8,128)(2,1)}, u32[]{:S(2)}, u32[]{:S(2)}) collective-permute-start(bf16[8,32,512]{2,1,0:T(8,128)(2,1)} %bitcast.68), channel_id=1, source_target_pairs={{0,8},{8,16},{16,24},{24,0},{1,9},{9,17},{17,25},{25,1},{2,10},{10... | collective-permute-start | bytes 786440 | tf_op jit(solution)/shard_map/ppermute | solution.py:31
  161.3 10.4 %collective-permute-start.19 = (bf16[8,32,512]{2,1,0:T(8,128)(2,1)S(1)}, bf16[8,32,512]{2,1,0:T(8,128)(2,1)}, u32[]{:S(2)}, u32[]{:S(2)}) collective-permute-start(bf16[8,32,512]{2,1,0:T(8,128)(2,1)S(1)} %bitcast.251), channel_id=1, source_target_pairs={{0,24},{8,0},{16,8},{24,16},{1,25},{9,1},{17,9},{25,17},{2,26},{10... | collective-permute-start | bytes 786440 | tf_op jit(solution)/shard_map/ppermute | solution.py:31
  162.2 13.4 %collective-permute-start.20 = (bf16[8,32,512]{2,1,0:T(8,128)(2,1)S(1)}, bf16[8,32,512]{2,1,0:T(8,128)(2,1)}, u32[]{:S(2)}, u32[]{:S(2)}) collective-permute-start(bf16[8,32,512]{2,1,0:T(8,128)(2,1)S(1)} %bitcast.250), channel_id=1, source_target_pairs={{0,16},{8,24},{16,0},{24,8},{1,17},{9,25},{17,1},{25,9},{2,18},{10... | collective-permute-start | bytes 786440 | tf_op jit(solution)/shard_map/ppermute | solution.py:31
  165.7 19.3 %all-to-all-start.2 = ((bf16[32,40,128]{2,1,0:T(8,128)(2,1)}), bf16[32,40,128]{2,1,0:T(8,128)(2,1)S(1)}, u32[]{:S(2)}, u32[]{:S(2)}) async-start(bf16[32,40,128]{2,1,0:T(8,128)(2,1)} %pad_maximum_fusion.18), calls=%async_computation.2 | async-start | bytes 655360 | tf_op jit(solution)/shard_map/all_to_all | solution.py:43
  175.5 27.4 %copy-start.40 = (bf16[128,256]{1,0:T(8,128)(2,1)S(1)}, bf16[128,256]{1,0:T(8,128)(2,1)}, u32[]{:S(2)}) copy-start(bf16[128,256]{1,0:T(8,128)(2,1)} %copy-done.39) | copy-start | bytes 196612
  175.5 27.4 %copy-start.42 = (bf16[128,256]{1,0:T(8,128)(2,1)S(1)}, bf16[128,256]{1,0:T(8,128)(2,1)}, u32[]{:S(2)}) copy-start(bf16[128,256]{1,0:T(8,128)(2,1)} %copy-done.41) | copy-start | bytes 196612
  176.8 16.3 %collective-permute-start.21 = (bf16[4,32,512]{2,1,0:T(8,128)(2,1)S(1)}, bf16[4,32,512]{2,1,0:T(8,128)(2,1)S(1)}, u32[]{:S(2)}, u32[]{:S(2)}) collective-permute-start(bf16[4,32,512]{2,1,0:T(8,128)(2,1)S(1)} %fusion.74), channel_id=1, source_target_pairs={{0,32},{32,0},{64,96},{96,64},{128,160},{160,128},{192,224},{224,1... | collective-permute-start | bytes 393224 | tf_op jit(solution)/shard_map/ppermute | solution.py:516
  187.5 18.9 %all-to-all-start.3 = ((bf16[32,32,128]{2,1,0:T(8,128)(2,1)}), bf16[32,32,128]{2,1,0:T(8,128)(2,1)S(1)}, u32[]{:S(2)}, u32[]{:S(2)}) async-start(bf16[32,32,128]{2,1,0:T(8,128)(2,1)} %shard_map.199), calls=%async_computation.3 | async-start | bytes 524288 | tf_op jit(solution)/shard_map/all_to_all | solution.py:43
  193.2 16.6 %collective-permute-start.22 = (bf16[32,512]{1,0:T(8,128)(2,1)S(1)}, bf16[32,512]{1,0:T(8,128)(2,1)S(1)}, u32[]{:S(2)}, u32[]{:S(2)}) collective-permute-start(bf16[32,512]{1,0:T(8,128)(2,1)S(1)} %get-tuple-element.151), channel_id=1, source_target_pairs={{0,64},{32,96},{64,128},{96,160},{128,192},{160,224},{192,0},{224,... | collective-permute-start | bytes 98312 | tf_op jit(solution)/shard_map/ppermute | solution.py:525
  195.7 14.1 %collective-permute-start.23 = (bf16[32,512]{1,0:T(8,128)(2,1)S(1)}, bf16[32,512]{1,0:T(8,128)(2,1)S(1)}, u32[]{:S(2)}, u32[]{:S(2)}) collective-permute-start(bf16[32,512]{1,0:T(8,128)(2,1)S(1)} %get-tuple-element.153), channel_id=1, source_target_pairs={{0,128},{32,160},{64,192},{96,224},{128,0},{160,32},{192,64},{224,... | collective-permute-start | bytes 98312 | tf_op jit(solution)/shard_map/ppermute | solution.py:525
  199.4 10.4 %collective-permute-start.24 = (bf16[32,512]{1,0:T(8,128)(2,1)S(1)}, bf16[32,512]{1,0:T(8,128)(2,1)S(1)}, u32[]{:S(2)}, u32[]{:S(2)}) collective-permute-start(bf16[32,512]{1,0:T(8,128)(2,1)S(1)} %get-tuple-element.152), channel_id=1, source_target_pairs={{0,192},{32,224},{64,0},{96,32},{128,64},{160,96},{192,128},{224,1... | collective-permute-start | bytes 98312 | tf_op jit(solution)/shard_map/ppermute | solution.py:525
  209.8 1.6 collective-permute-start.26
  (48 other events, 195.3 us)

commit v5 on v4

--- a/solution.py
+++ b/solution.py
@@ -510,16 +510,12 @@
     scanned = scan_chunks(states_got)
     states_back = exchange(scanned)
     depth = lax.axis_index(SP[0])
-    upper = (depth & 1) != 0
-    pairs = proj_sum.reshape(deep // 2, 2, block, width)
-    away = jnp.where(upper, pairs[:, 0], pairs[:, 1]).astype(bf16)
-    got = lax.ppermute(away, SP[0], [(i, i ^ 1) for i in range(deep)])
-    proj_sum = jnp.where(upper, pairs[:, 1], pairs[:, 0]) + got.astype(f32)
     level = depth >> 1
     count = deep // 2
+    levels = proj_sum.reshape(count, 2, block, width)
 
     def level_part(i):
-        return lax.dynamic_index_in_dim(proj_sum, (level + i) & (count - 1), 0, keepdims=False)
+        return lax.dynamic_index_in_dim(levels, (level + i) & (count - 1), 0, keepdims=False)
 
     others = [
         lax.ppermute(
@@ -527,7 +523,11 @@
         )
         for k in range(1, count)
     ]
-    proj_grad = level_part(0) + sum(a.astype(f32) for a in others)
+    upper = (depth & 1) != 0
+    pair = level_part(0) + sum(a.astype(f32) for a in others)
+    away = jnp.where(upper, pair[0], pair[1]).astype(bf16)
+    got = lax.ppermute(away, SP[0], [(i, i ^ 1) for i in range(deep)])
+    proj_grad = jnp.where(upper, pair[1], pair[0]) + got.astype(f32)
 
     base = mix_chunk(delta, value, write, read, cumul_wide, cumul_row)
     outs_mine, outs_send = tail(

time: 216 us -> 218 us (level)
    all_to_all x4, starting transfers between devices: 31.3 us -> 35.4 us  [exchange(): return lax.all_to_all(x, CHIPS, split_axis=0, concat_axis=0, tiled=True)]
    ppermute x3, starting transfers between devices: 9.69 us -> 5.98 us  [on_device(): lax.ppermute(level_part(k).astype(bf16), SP[0], [(i, (i + 2 * k) % deep)...]
    unnamed x132 -> x134, local copies, waits for them, and re-layouts: 4.72 us -> 4.71 us
  transfers between devices with their start and end apart: 31 -> 31, of which waited for: 16 -> 17; matrix products, arithmetic and copies ran while one was open for 18% -> 18% of each run, Pallas kernels for 3% -> 3%
where the time goes in v5:
time: 218 us; the launch traced here: 214 us
  starting transfers between devices  65.5 us (30%)
  waiting for transfers between devices  63.6 us (29%)
  matrix products  28.2 us (13%)
  other arithmetic  24.8 us (11%)
  Pallas kernels  16 us (7%)
  local copies, waits for them, and re-layouts  13.9 us (6%)
    ppermute x15, waiting for transfers between devices, ring(): return lax.ppermute(x, axis, [(i, (i + shift) % n) for i in range(n)])  38.9 us
    all_to_all x4, starting transfers between devices, exchange(): return lax.all_to_all(x, CHIPS, split_axis=0, concat_axis=0, tiled=True)  35.4 us
    dot_general x33, matrix products, dot(): lax.dot_general(a, b, (((ca,), (cb,)), ((), ())), preferred_element_type=...  27.8 us
    all_to_all x4, waiting for transfers between devices, exchange(): return lax.all_to_all(x, CHIPS, split_axis=0, concat_axis=0, tiled=True)  22.6 us
    ppermute x15, starting transfers between devices, ring(): return lax.ppermute(x, axis, [(i, (i + shift) % n) for i in range(n)])  20.7 us
    ppermute x3, starting transfers between devices, on_device(): lax.ppermute(level_part(k).astype(bf16), SP[0], [(i, (i + 2 * k) % deep)...  5.98 us
    unnamed x134, local copies, waits for them, and re-layouts  4.71 us
  transfers between devices with their start and end apart: 31, of which 17 were waited for; matrix products, arithmetic and copies ran while one was open for 18% of the time, Pallas kernels for 3%

profile of v5, /device:TPU:4, one launch (start us, length us, event | category | flops | bytes accessed | tf_op | source)
XLA Modules:
  0.0 213.9 jit_solution(262948127737606164)
XLA Ops:
  2.9 1.4 fusion.4
  6.2 3.4 %shard_map.197 = (bf16[768,512]{1,0:T(8,128)(2,1)}, s32[8,256]{1,0:T(8,128)}) custom-call(s32[1]{0:T(128)} %bitcast.core_ref, f32[12,128]{1,0:T(8,128)} %copy-done.58, f32[12,128]{1,0:T(8,128)} %copy-done.60, bf16[128,512]{1,0:T(8,128)(2,1)} %x_ref.1, bf16[128,512]{1,0:T(8,128)(2,1)} %copy-done.53, bf16[128,512]{1,0:T(8,128)(2,1)} %c_ref.1, ...), custom_call_target="tpu_custom_call" | custom-call | tf_op jit(solution)/shard_map/pallas_call | solution.py:105
  10.7 1.5 pad_maximum_fusion.20
  13.4 11.6 %all-to-all-start = ((bf16[32,24,512]{2,1,0:T(8,128)(2,1)}), bf16[32,24,512]{2,1,0:T(8,128)(2,1)}, u32[]{:S(2)}, u32[]{:S(2)}) async-start(bf16[32,24,512]{2,1,0:T(8,128)(2,1)} %bitcast.231), calls=%async_computation | async-start | bytes 1572864 | tf_op jit(solution)/shard_map/all_to_all | solution.py:43
  25.1 2.6 %dynamic-slice_bitcast_fusion.10 = (bf16[512,256]{1,0:T(8,128)(2,1)}, bf16[512,256]{1,0:T(8,128)(2,1)}, bf16[512,256]{1,0:T(8,128)(2,1)}, bf16[512,256]{1,0:T(8,...) fusion(bf16[4,512,256]{2,1,0:T(8,128)(2,1)S(1)} %bitcast.227, ...), kind=kLoop, calls=%fused_computation.150 | loop fusion | bytes 4194320 | tf_op jit(solution)/shard_map/jit(dynamic_index_in_dim)/squeeze | solution.py:415
  28.5 1.6 add_convert_fusion
  39.4 8.4 %all-to-all-done = bf16[32,24,512]{2,1,0:T(8,128)(2,1)} async-done(((bf16[32,24,512]{2,1,0:T(8,128)(2,1)}), bf16[32,24,512]{2,1,0:T(8,128)(2,1)}, u32[]{:S(2)}, u32[]{:S(2)}) %all-to-all-start) | async-done | bytes 786464 | tf_op jit(solution)/shard_map/all_to_all | solution.py:43
  48.5 1.8 convolution_convert_fusion.10
  50.4 3.1 %collective-permute-start.4 = (bf16[384,512]{1,0:T(8,128)(2,1)S(1)}, bf16[384,512]{1,0:T(8,128)(2,1)S(1)}, u32[]{:S(2)}, u32[]{:S(2)}) collective-permute-start(bf16[384,512]{1,0:T(8,128)(2,1)S(1)} %convolution_convert_fusion.10), channel_id=1, source_target_pairs={{0,3},{1,0},{2,1},{3,2},{4,7},{5,4},{6,5},{7,6},{8,11},{9,8},{10,9... | collective-permute-start | bytes 1179656 | tf_op jit(solution)/shard_map/ppermute | solution.py:31
  53.5 1.8 convolution_convert_fusion.9
  55.3 3.3 %collective-permute-start.7 = (bf16[384,512]{1,0:T(8,128)(2,1)S(1)}, bf16[384,512]{1,0:T(8,128)(2,1)S(1)}, u32[]{:S(2)}, u32[]{:S(2)}) collective-permute-start(bf16[384,512]{1,0:T(8,128)(2,1)S(1)} %convolution_convert_fusion.9), channel_id=1, source_target_pairs={{0,3},{1,0},{2,1},{3,2},{4,7},{5,4},{6,5},{7,6},{8,11},{9,8},{10,9... | collective-permute-start | bytes 1179656 | tf_op jit(solution)/shard_map/ppermute | solution.py:31
  59.4 3.5 %collective-permute-done.4 = bf16[384,512]{1,0:T(8,128)(2,1)S(1)} collective-permute-done((bf16[384,512]{1,0:T(8,128)(2,1)S(1)}, bf16[384,512]{1,0:T(8,128)(2,1)S(1)}, u32[]{:S(2)}, u32[]{:S(2)}) %collective-permute-start.4) | collective-permute-done | bytes 393248 | tf_op jit(solution)/shard_map/ppermute | solution.py:31
  63.0 3.7 %collective-permute-start.6 = (bf16[384,512]{1,0:T(8,128)(2,1)S(1)}, bf16[384,512]{1,0:T(8,128)(2,1)S(1)}, u32[]{:S(2)}, u32[]{:S(2)}) collective-permute-start(bf16[384,512]{1,0:T(8,128)(2,1)S(1)} %collective-permute-done.4), channel_id=1, source_target_pairs={{0,3},{1,0},{2,1},{3,2},{4,7},{5,4},{6,5},{7,6},{8,11},{9,8},{10,9... | collective-permute-start | bytes 1179656 | tf_op jit(solution)/shard_map/ppermute | solution.py:31
  66.7 5.6 %collective-permute-done.8 = bf16[384,512]{1,0:T(8,128)(2,1)S(1)} collective-permute-done((bf16[384,512]{1,0:T(8,128)(2,1)S(1)}, bf16[384,512]{1,0:T(8,128)(2,1)S(1)}, u32[]{:S(2)}, u32[]{:S(2)}) %collective-permute-start.8) | collective-permute-done | bytes 393248 | tf_op jit(solution)/shard_map/ppermute | solution.py:31
  74.1 7.8 %collective-permute-done.9 = bf16[384,512]{1,0:T(8,128)(2,1)S(1)} collective-permute-done((bf16[384,512]{1,0:T(8,128)(2,1)S(1)}, bf16[384,512]{1,0:T(8,128)(2,1)S(1)}, u32[]{:S(2)}, u32[]{:S(2)}) %collective-permute-start.9) | collective-permute-done | bytes 393248 | tf_op jit(solution)/shard_map/ppermute | solution.py:31
  86.4 1.7 collective-permute-start.11
  89.6 2.3 %convolution_convert_fusion.8.own_ref = bf16[384,512]{1,0:T(8,128)(2,1)} fusion(bf16[512,256]{1,0:T(8,128)(2,1)S(1)} %copy-done.37, bf16[512,256]{1,0:T(8,128)(2,1)} %get-tuple-element.174, bf16[384,256]{0,1:T(8,128)(2,1)} %copy-done.52, bf16[384,256]{0,1:T(8,128)(2,1)} %copy-done.51), kind=kOutput, calls=%fused_computation.12 | convolution fusion | flops 203358208 | bytes 1310720 | tf_op jit(solution)/shard_map/dot_general | solution.py:22
  92.0 8.0 %collective-permute-done.12.far_ref = bf16[384,512]{1,0:T(8,128)(2,1)} collective-permute-done((bf16[384,512]{1,0:T(8,128)(2,1)}, bf16[384,512]{1,0:T(8,128)(2,1)}, u32[]{:S(2)}, u32[]{:S(2)}) %collective-permute-start.12) | collective-permute-done | bytes 393248 | tf_op jit(solution)/shard_map/ppermute | solution.py:31
  100.0 1.3 collective-permute-done.11.up_ref
  101.3 2.9 %collective-permute-done.10.low_ref = bf16[384,512]{1,0:T(8,128)(2,1)} collective-permute-done((bf16[384,512]{1,0:T(8,128)(2,1)}, bf16[384,512]{1,0:T(8,128)(2,1)}, u32[]{:S(2)}, u32[]{:S(2)}) %collective-permute-start.10) | collective-permute-done | bytes 393248 | tf_op jit(solution)/shard_map/ppermute | solution.py:31
  104.2 3.6 %shard_map.198 = bf16[768,256]{1,0:T(8,128)(2,1)} custom-call(bf16[384,512]{1,0:T(8,128)(2,1)} %convolution_convert_fusion.8.own_ref, bf16[384,512]{1,0:T(8,128)(2,1)} %collective-permute-done.10.low_ref, bf16[384,512]{1,0:T(8,128)(2,1)} %collective-permute-done.11.up_ref, bf16[384,512]{1,0:T(8,128)(2,1)} %collective-permute-done.12.far_ref), custom_call_target="tpu_custom_call" | custom-call | tf_op jit(solution)/shard_map/pallas_call | solution.py:147
  107.7 1.4 fusion.6
  109.1 1.5 fusion
  115.9 8.0 %all-to-all-start.1 = ((bf16[32,24,256]{2,1,0:T(8,128)(2,1)}), bf16[32,24,256]{2,1,0:T(8,128)(2,1)S(1)}, u32[]{:S(2)}, u32[]{:S(2)}) async-start(bf16[32,24,256]{2,1,0:T(8,128)(2,1)} %bitcast.224), calls=%async_computation.1 | async-start | bytes 786432 | tf_op jit(solution)/shard_map/all_to_all | solution.py:43
  123.8 1.3 fusion.7
  125.1 1.3 fusion.8
  126.4 1.3 fusion.9
  131.2 6.8 %all-to-all-done.1 = bf16[32,24,256]{2,1,0:T(8,128)(2,1)S(1)} async-done(((bf16[32,24,256]{2,1,0:T(8,128)(2,1)}), bf16[32,24,256]{2,1,0:T(8,128)(2,1)S(1)}, u32[]{:S(2)}, u32[]{:S(2)}) %all-to-all-start.1) | async-done | bytes 393248 | tf_op jit(solution)/shard_map/all_to_all | solution.py:43
  138.0 1.3 fusion.107
  139.3 1.3 fusion.106
  142.7 3.2 %collective-permute-start.14 = (bf16[128,512]{0,1:T(8,128)(2,1)S(1)}, bf16[128,512]{0,1:T(8,128)(2,1)S(1)}, u32[]{:S(2)}, u32[]{:S(2)}) collective-permute-start(bf16[128,512]{0,1:T(8,128)(2,1)S(1)} %fusion.61), channel_id=1, source_target_pairs={{0,3},{1,0},{2,1},{3,2},{4,7},{5,4},{6,5},{7,6},{8,11},{9,8},{10,9... | collective-permute-start | bytes 393224 | tf_op jit(solution)/shard_map/ppermute | solution.py:31
  145.8 4.4 %collective-permute-done.15 = bf16[128,512]{0,1:T(8,128)(2,1)S(1)} collective-permute-done((bf16[128,512]{0,1:T(8,128)(2,1)S(1)}, bf16[128,512]{0,1:T(8,128)(2,1)S(1)}, u32[]{:S(2)}, u32[]{:S(2)}) %collective-permute-start.15) | collective-permute-done | bytes 131104 | tf_op jit(solution)/shard_map/ppermute | solution.py:31
  150.4 1.7 collective-permute-done.16
  152.7 2.0 fusion.48
  161.3 2.7 %collective-permute-start.20 = (bf16[8,32,512]{2,1,0:T(8,128)(2,1)S(1)}, bf16[8,32,512]{2,1,0:T(8,128)(2,1)}, u32[]{:S(2)}, u32[]{:S(2)}) collective-permute-start(bf16[8,32,512]{2,1,0:T(8,128)(2,1)S(1)} %bitcast.234), channel_id=1, source_target_pairs={{0,16},{8,24},{16,0},{24,8},{1,17},{9,25},{17,1},{25,9},{2,18},{10... | collective-permute-start | bytes 786440 | tf_op jit(solution)/shard_map/ppermute | solution.py:31
  164.8 6.2 %all-to-all-start.2 = ((bf16[32,40,128]{2,1,0:T(8,128)(2,1)}), bf16[32,40,128]{2,1,0:T(8,128)(2,1)S(1)}, u32[]{:S(2)}, u32[]{:S(2)}) async-start(bf16[32,40,128]{2,1,0:T(8,128)(2,1)} %pad_maximum_fusion.18), calls=%async_computation.2 | async-start | bytes 655360 | tf_op jit(solution)/shard_map/all_to_all | solution.py:43
  171.0 3.6 %collective-permute-done.20 = bf16[8,32,512]{2,1,0:T(8,128)(2,1)} collective-permute-done((bf16[8,32,512]{2,1,0:T(8,128)(2,1)S(1)}, bf16[8,32,512]{2,1,0:T(8,128)(2,1)}, u32[]{:S(2)}, u32[]{:S(2)}) %collective-permute-start.20) | collective-permute-done | bytes 262176 | tf_op jit(solution)/shard_map/ppermute | solution.py:31
  175.9 1.3 collective-permute-start.21
  177.2 1.4 collective-permute-start.22
  178.6 3.3 %collective-permute-start.23 = (bf16[2,32,512]{2,1,0:T(8,128)(2,1)S(1)}, bf16[2,32,512]{2,1,0:T(8,128)(2,1)S(1)}, u32[]{:S(2)}, u32[]{:S(2)}) collective-permute-start(bf16[2,32,512]{2,1,0:T(8,128)(2,1)S(1)} %get-tuple-element.135), channel_id=1, source_target_pairs={{0,192},{32,224},{64,0},{96,32},{128,64},{160,96},{192,128},{224,1... | collective-permute-start | bytes 196616 | tf_op jit(solution)/shard_map/ppermute | solution.py:521
  181.9 2.8 %all-to-all-done.2.msg_ref = bf16[32,40,128]{2,1,0:T(8,128)(2,1)S(1)} async-done(((bf16[32,40,128]{2,1,0:T(8,128)(2,1)}), bf16[32,40,128]{2,1,0:T(8,128)(2,1)S(1)}, u32[]{:S(2)}, u32[]{:S(2)}) %all-to-all-start.2) | async-done | bytes 327712 | tf_op jit(solution)/shard_map/all_to_all | solution.py:43
  185.4 1.8 shard_map.199
  187.2 9.7 %all-to-all-start.3 = ((bf16[32,32,128]{2,1,0:T(8,128)(2,1)}), bf16[32,32,128]{2,1,0:T(8,128)(2,1)S(1)}, u32[]{:S(2)}, u32[]{:S(2)}) async-start(bf16[32,32,128]{2,1,0:T(8,128)(2,1)} %shard_map.199), calls=%async_computation.3 | async-start | bytes 524288 | tf_op jit(solution)/shard_map/all_to_all | solution.py:43
  197.0 1.6 collective-permute-start.24
  199.2 2.9 %shard_map.200.base_ref = f32[256,512]{1,0:T(8,128)} custom-call(bf16[256,256]{1,0:T(8,128)(2,1)} %pad_maximum_fusion.24.delta_ref, bf16[256,256]{1,0:T(8,128)(2,1)} %pad_maximum_fusion.22.value_ref, bf16[256,128]{1,0:T(8,128)(2,1)} %pad_maximum_fusion.26.write_ref, bf16[256,128]{1,0:T(8,128)(2,1)} %pad_maximum_fusion.27.read_ref, f32[256,256]{1,0:T(8,128)} %copy-done.1, ...), custom_call_target="tpu_custom_call" | custom-call | tf_op jit(solution)/shard_map/pallas_call | solution.py:173
  202.1 4.5 %all-to-all-done.3.back_ref = bf16[32,32,128]{2,1,0:T(8,128)(2,1)S(1)} async-done(((bf16[32,32,128]{2,1,0:T(8,128)(2,1)}), bf16[32,32,128]{2,1,0:T(8,128)(2,1)S(1)}, u32[]{:S(2)}, u32[]{:S(2)}) %all-to-all-start.3) | async-done | bytes 262176 | tf_op jit(solution)/shard_map/all_to_all | solution.py:43
  207.3 2.6 %shard_map.201 = (f32[128,512]{1,0:T(8,128)}, bf16[128,512]{1,0:T(8,128)(2,1)}) custom-call(s32[1]{0:T(128)} %bitcast.core_ref, bf16[32,32,128]{2,1,0:T(8,128)(2,1)} %copy-done.20, bf16[256,128]{1,0:T(8,128)(2,1)} %pad_maximum_fusion.26.write_ref, bf16[256,256]{1,0:T(8,128)(2,1)} %copy-done.18, bf16[256,256]{1,0:T(8,128)(2,1)} %copy-done.17, ...), custom_call_target="tpu_custom_call" | custom-call | tf_op jit(solution)/shard_map/pallas_call | solution.py:274
  212.2 1.7 shard_map.202
  (261 shorter events, 49.5 us)
Async XLA Ops:
  0.6 149.6 %copy-start = (bf16[2048,512]{1,0:T(8,128)(2,1)S(1)}, bf16[2048,512]{1,0:T(8,128)(2,1)}, u32[]{:S(2)}) copy-start(bf16[2048,512]{1,0:T(8,128)(2,1)} %param.24) | copy-start | bytes 6291460
  2.2 3.3 %collective-permute-start = (f32[12,128]{1,0:T(8,128)S(1)}, f32[12,128]{1,0:T(8,128)S(1)}, u32[]{:S(2)}, u32[]{:S(2)}) collective-permute-start(f32[12,128]{1,0:T(8,128)S(1)} %pad_maximum_fusion.28.mine_ref), channel_id=1, source_target_pairs={{0,4},{4,0},{1,5},{5,1},{2,6},{6,2},{3,7},{7,3},{8,12},{12,8},{9,1... | collective-permute-start | bytes 18440 | tf_op jit(solution)/shard_map/ppermute | solution.py:26
  2.3 3.2 %collective-permute-start.1 = (bf16[128,512]{1,0:T(8,128)(2,1)}, bf16[128,512]{1,0:T(8,128)(2,1)S(1)}, u32[]{:S(2)}, u32[]{:S(2)}) collective-permute-start(bf16[128,512]{1,0:T(8,128)(2,1)} %x_ref.1), channel_id=1, source_target_pairs={{0,4},{4,0},{1,5},{5,1},{2,6},{6,2},{3,7},{7,3},{8,12},{12,8},{9,1... | collective-permute-start | bytes 393224 | tf_op jit(solution)/shard_map/ppermute | solution.py:26
  2.8 2.7 %collective-permute-start.2 = (bf16[128,512]{1,0:T(8,128)(2,1)}, bf16[128,512]{1,0:T(8,128)(2,1)S(1)}, u32[]{:S(2)}, u32[]{:S(2)}) collective-permute-start(bf16[128,512]{1,0:T(8,128)(2,1)} %c_ref.1), channel_id=1, source_target_pairs={{0,4},{4,0},{1,5},{5,1},{2,6},{6,2},{3,7},{7,3},{8,12},{12,8},{9,1... | collective-permute-start | bytes 393224 | tf_op jit(solution)/shard_map/ppermute | solution.py:26
  2.9 22.1 %copy-start.21 = (bf16[1,2048,256]{2,1,0:T(8,128)(2,1)S(1)}, bf16[1,2048,256]{2,1,0:T(8,128)(2,1)}, u32[]{:S(2)}) copy-start(bf16[1,2048,256]{2,1,0:T(8,128)(2,1)} %param.19) | copy-start | bytes 3145732
  12.2 17.9 %collective-permute-start.3 = (bf16[128,1024]{1,0:T(8,128)(2,1)}, bf16[128,1024]{1,0:T(8,128)(2,1)}, u32[]{:S(2)}, u32[]{:S(2)}) collective-permute-start(bf16[128,1024]{1,0:T(8,128)(2,1)} %pad_maximum_fusion.20), channel_id=1, source_target_pairs={{0,4},{4,0},{1,5},{5,1},{2,6},{6,2},{3,7},{7,3},{8,12},{12,8},{9,1... | collective-permute-start | bytes 786440 | tf_op jit(solution)/shard_map/ppermute | solution.py:26
  13.4 34.4 %all-to-all-start = ((bf16[32,24,512]{2,1,0:T(8,128)(2,1)}), bf16[32,24,512]{2,1,0:T(8,128)(2,1)}, u32[]{:S(2)}, u32[]{:S(2)}) async-start(bf16[32,24,512]{2,1,0:T(8,128)(2,1)} %bitcast.231), calls=%async_computation | async-start | bytes 1572864 | tf_op jit(solution)/shard_map/all_to_all | solution.py:43
  32.9 17.4 %copy-start.1 = (f32[256,256]{1,0:T(8,128)}, f32[256,256]{1,0:T(8,128)S(1)}, u32[]{:S(2)}) copy-start(f32[256,256]{1,0:T(8,128)S(1)} %fusion.86.wide_ref) | copy-start | bytes 786436
  35.5 17.9 %copy-start.17 = (bf16[256,256]{1,0:T(8,128)(2,1)}, bf16[256,256]{1,0:T(8,128)(2,1)S(1)}, u32[]{:S(2)}) copy-start(bf16[256,256]{1,0:T(8,128)(2,1)S(1)} %get-tuple-element.91.value_end_ref) | copy-start | bytes 393220
  35.5 17.9 %copy-start.18 = (bf16[256,256]{1,0:T(8,128)(2,1)}, bf16[256,256]{1,0:T(8,128)(2,1)S(1)}, u32[]{:S(2)}) copy-start(bf16[256,256]{1,0:T(8,128)(2,1)S(1)} %get-tuple-element.90.value_start_ref) | copy-start | bytes 393220
  35.5 120.6 %copy-start.2 = (f32[256,256]{1,0:T(8,128)}, f32[256,256]{1,0:T(8,128)S(1)}, u32[]{:S(2)}) copy-start(f32[256,256]{1,0:T(8,128)S(1)} %get-tuple-element.85.fade_end_ref) | copy-start | bytes 786436
  35.5 120.6 %copy-start.3 = (f32[256,256]{1,0:T(8,128)}, f32[256,256]{1,0:T(8,128)S(1)}, u32[]{:S(2)}) copy-start(f32[256,256]{1,0:T(8,128)S(1)} %get-tuple-element.86.fade_start_ref) | copy-start | bytes 786436
  50.3 22.0 %copy-start.30 = (bf16[512,256]{1,0:T(8,128)(2,1)S(1)}, bf16[512,256]{1,0:T(8,128)(2,1)}, u32[]{:S(2)}) copy-start(bf16[512,256]{1,0:T(8,128)(2,1)} %get-tuple-element.131) | copy-start | bytes 786436
  50.3 22.0 %copy-start.31 = (bf16[512,256]{1,0:T(8,128)(2,1)S(1)}, bf16[512,256]{1,0:T(8,128)(2,1)}, u32[]{:S(2)}) copy-start(bf16[512,256]{1,0:T(8,128)(2,1)} %get-tuple-element.175) | copy-start | bytes 786436
  50.4 12.6 %collective-permute-start.4 = (bf16[384,512]{1,0:T(8,128)(2,1)S(1)}, bf16[384,512]{1,0:T(8,128)(2,1)S(1)}, u32[]{:S(2)}, u32[]{:S(2)}) collective-permute-start(bf16[384,512]{1,0:T(8,128)(2,1)S(1)} %convolution_convert_fusion.10), channel_id=1, source_target_pairs={{0,3},{1,0},{2,1},{3,2},{4,7},{5,4},{6,5},{7,6},{8,11},{9,8},{10,9... | collective-permute-start | bytes 1179656 | tf_op jit(solution)/shard_map/ppermute | solution.py:31
  53.5 20.3 %collective-permute-start.5 = (bf16[384,512]{1,0:T(8,128)(2,1)S(1)}, bf16[384,512]{1,0:T(8,128)(2,1)S(1)}, u32[]{:S(2)}, u32[]{:S(2)}) collective-permute-start(bf16[384,512]{1,0:T(8,128)(2,1)S(1)} %convolution_convert_fusion.10), channel_id=1, source_target_pairs={{0,1},{1,2},{2,3},{3,0},{4,5},{5,6},{6,7},{7,4},{8,9},{9,10},{10,1... | collective-permute-start | bytes 1179656 | tf_op jit(solution)/shard_map/ppermute | solution.py:31
  55.2 17.1 %copy-start.13 = (bf16[384,512]{1,0:T(8,128)(2,1)}, bf16[384,512]{1,0:T(8,128)(2,1)S(1)}, u32[]{:S(2)}) copy-start(bf16[384,512]{1,0:T(8,128)(2,1)S(1)} %convolution_convert_fusion.9) | copy-start | bytes 1179652
  55.3 17.0 %collective-permute-start.7 = (bf16[384,512]{1,0:T(8,128)(2,1)S(1)}, bf16[384,512]{1,0:T(8,128)(2,1)S(1)}, u32[]{:S(2)}, u32[]{:S(2)}) collective-permute-start(bf16[384,512]{1,0:T(8,128)(2,1)S(1)} %convolution_convert_fusion.9), channel_id=1, source_target_pairs={{0,3},{1,0},{2,1},{3,2},{4,7},{5,4},{6,5},{7,6},{8,11},{9,8},{10,9... | collective-permute-start | bytes 1179656 | tf_op jit(solution)/shard_map/ppermute | solution.py:31
  58.6 13.7 %collective-permute-start.8 = (bf16[384,512]{1,0:T(8,128)(2,1)S(1)}, bf16[384,512]{1,0:T(8,128)(2,1)S(1)}, u32[]{:S(2)}, u32[]{:S(2)}) collective-permute-start(bf16[384,512]{1,0:T(8,128)(2,1)S(1)} %convolution_convert_fusion.9), channel_id=1, source_target_pairs={{0,1},{1,2},{2,3},{3,0},{4,5},{5,6},{6,7},{7,4},{8,9},{9,10},{10,1... | collective-permute-start | bytes 1179656 | tf_op jit(solution)/shard_map/ppermute | solution.py:31
  58.9 13.9 %copy-start.32 = (bf16[512,256]{1,0:T(8,128)(2,1)S(1)}, bf16[512,256]{1,0:T(8,128)(2,1)}, u32[]{:S(2)}) copy-start(bf16[512,256]{1,0:T(8,128)(2,1)} %get-tuple-element.130) | copy-start | bytes 786436
  58.9 13.9 %copy-start.33 = (bf16[512,256]{1,0:T(8,128)(2,1)S(1)}, bf16[512,256]{1,0:T(8,128)(2,1)}, u32[]{:S(2)}) copy-start(bf16[512,256]{1,0:T(8,128)(2,1)} %get-tuple-element.176) | copy-start | bytes 786436
  63.0 19.8 %copy-start.10 = (bf16[384,512]{1,0:T(8,128)(2,1)}, bf16[384,512]{1,0:T(8,128)(2,1)S(1)}, u32[]{:S(2)}) copy-start(bf16[384,512]{1,0:T(8,128)(2,1)S(1)} %collective-permute-done.4) | copy-start | bytes 1179652
  63.0 19.4 %collective-permute-start.6 = (bf16[384,512]{1,0:T(8,128)(2,1)S(1)}, bf16[384,512]{1,0:T(8,128)(2,1)S(1)}, u32[]{:S(2)}, u32[]{:S(2)}) collective-permute-start(bf16[384,512]{1,0:T(8,128)(2,1)S(1)} %collective-permute-done.4), channel_id=1, source_target_pairs={{0,3},{1,0},{2,1},{3,2},{4,7},{5,4},{6,5},{7,6},{8,11},{9,8},{10,9... | collective-permute-start | bytes 1179656 | tf_op jit(solution)/shard_map/ppermute | solution.py:31
  72.3 9.6 %collective-permute-start.9 = (bf16[384,512]{1,0:T(8,128)(2,1)S(1)}, bf16[384,512]{1,0:T(8,128)(2,1)S(1)}, u32[]{:S(2)}, u32[]{:S(2)}) collective-permute-start(bf16[384,512]{1,0:T(8,128)(2,1)S(1)} %collective-permute-done.8), channel_id=1, source_target_pairs={{0,1},{1,2},{2,3},{3,0},{4,5},{5,6},{6,7},{7,4},{8,9},{9,10},{10,1... | collective-permute-start | bytes 1179656 | tf_op jit(solution)/shard_map/ppermute | solution.py:31
  73.7 12.6 %copy-start.11 = (bf16[384,512]{1,0:T(8,128)(2,1)}, bf16[384,512]{1,0:T(8,128)(2,1)S(1)}, u32[]{:S(2)}) copy-start(bf16[384,512]{1,0:T(8,128)(2,1)S(1)} %collective-permute-done.5) | copy-start | bytes 1179652
  86.3 13.6 %collective-permute-start.12 = (bf16[384,512]{1,0:T(8,128)(2,1)}, bf16[384,512]{1,0:T(8,128)(2,1)}, u32[]{:S(2)}, u32[]{:S(2)}) collective-permute-start(bf16[384,512]{1,0:T(8,128)(2,1)} %convolution_convert_fusion.5), channel_id=1, source_target_pairs={{0,2},{1,3},{2,0},{3,1},{4,6},{5,7},{6,4},{7,5},{8,10},{9,11},{10,... | collective-permute-start | bytes 1179656 | tf_op jit(solution)/shard_map/ppermute | solution.py:31
  86.4 14.8 %collective-permute-start.11 = (bf16[384,512]{1,0:T(8,128)(2,1)}, bf16[384,512]{1,0:T(8,128)(2,1)}, u32[]{:S(2)}, u32[]{:S(2)}) collective-permute-start(bf16[384,512]{1,0:T(8,128)(2,1)} %convolution_convert_fusion.6), channel_id=1, source_target_pairs={{0,3},{1,0},{2,1},{3,2},{4,7},{5,4},{6,5},{7,6},{8,11},{9,8},{10,9... | collective-permute-start | bytes 1179656 | tf_op jit(solution)/shard_map/ppermute | solution.py:31
  88.2 16.0 %collective-permute-start.10 = (bf16[384,512]{1,0:T(8,128)(2,1)}, bf16[384,512]{1,0:T(8,128)(2,1)}, u32[]{:S(2)}, u32[]{:S(2)}) collective-permute-start(bf16[384,512]{1,0:T(8,128)(2,1)} %convolution_convert_fusion.7), channel_id=1, source_target_pairs={{0,1},{1,2},{2,3},{3,0},{4,5},{5,6},{6,7},{7,4},{8,9},{9,10},{10,1... | collective-permute-start | bytes 1179656 | tf_op jit(solution)/shard_map/ppermute | solution.py:31
  115.9 22.2 %all-to-all-start.1 = ((bf16[32,24,256]{2,1,0:T(8,128)(2,1)}), bf16[32,24,256]{2,1,0:T(8,128)(2,1)S(1)}, u32[]{:S(2)}, u32[]{:S(2)}) async-start(bf16[32,24,256]{2,1,0:T(8,128)(2,1)} %bitcast.224), calls=%async_computation.1 | async-start | bytes 786432 | tf_op jit(solution)/shard_map/all_to_all | solution.py:43
  140.7 1.4 collective-permute-start.13
  142.2 12.7 %copy-start.46 = (bf16[128,512]{0,1:T(8,128)(2,1)}, bf16[128,512]{0,1:T(8,128)(2,1)S(1)}, u32[]{:S(2)}) copy-start(bf16[128,512]{0,1:T(8,128)(2,1)S(1)} %fusion.61) | copy-start | bytes 393220
  142.2 8.0 %collective-permute-start.15 = (bf16[128,512]{0,1:T(8,128)(2,1)S(1)}, bf16[128,512]{0,1:T(8,128)(2,1)S(1)}, u32[]{:S(2)}, u32[]{:S(2)}) collective-permute-start(bf16[128,512]{0,1:T(8,128)(2,1)S(1)} %fusion.61), channel_id=1, source_target_pairs={{0,2},{1,3},{2,0},{3,1},{4,6},{5,7},{6,4},{7,5},{8,10},{9,11},{10,... | collective-permute-start | bytes 393224 | tf_op jit(solution)/shard_map/ppermute | solution.py:31
  142.6 9.6 %collective-permute-start.16 = (bf16[128,512]{0,1:T(8,128)(2,1)S(1)}, bf16[128,512]{0,1:T(8,128)(2,1)S(1)}, u32[]{:S(2)}, u32[]{:S(2)}) collective-permute-start(bf16[128,512]{0,1:T(8,128)(2,1)S(1)} %fusion.61), channel_id=1, source_target_pairs={{0,1},{1,2},{2,3},{3,0},{4,5},{5,6},{6,7},{7,4},{8,9},{9,10},{10,1... | collective-permute-start | bytes 393224 | tf_op jit(solution)/shard_map/ppermute | solution.py:31
  142.7 9.8 %collective-permute-start.14 = (bf16[128,512]{0,1:T(8,128)(2,1)S(1)}, bf16[128,512]{0,1:T(8,128)(2,1)S(1)}, u32[]{:S(2)}, u32[]{:S(2)}) collective-permute-start(bf16[128,512]{0,1:T(8,128)(2,1)S(1)} %fusion.61), channel_id=1, source_target_pairs={{0,3},{1,0},{2,1},{3,2},{4,7},{5,4},{6,5},{7,6},{8,11},{9,8},{10,9... | collective-permute-start | bytes 393224 | tf_op jit(solution)/shard_map/ppermute | solution.py:31
  154.7 1.3 collective-permute-start.25
  154.9 2.1 collective-permute-start.17
  159.3 11.7 %collective-permute-start.18 = (bf16[8,32,512]{2,1,0:T(8,128)(2,1)}, bf16[8,32,512]{2,1,0:T(8,128)(2,1)}, u32[]{:S(2)}, u32[]{:S(2)}) collective-permute-start(bf16[8,32,512]{2,1,0:T(8,128)(2,1)} %bitcast.68), channel_id=1, source_target_pairs={{0,8},{8,16},{16,24},{24,0},{1,9},{9,17},{17,25},{25,1},{2,10},{10... | collective-permute-start | bytes 786440 | tf_op jit(solution)/shard_map/ppermute | solution.py:31
  160.5 10.5 %collective-permute-start.19 = (bf16[8,32,512]{2,1,0:T(8,128)(2,1)}, bf16[8,32,512]{2,1,0:T(8,128)(2,1)}, u32[]{:S(2)}, u32[]{:S(2)}) collective-permute-start(bf16[8,32,512]{2,1,0:T(8,128)(2,1)} %bitcast.69), channel_id=1, source_target_pairs={{0,24},{8,0},{16,8},{24,16},{1,25},{9,1},{17,9},{25,17},{2,26},{10... | collective-permute-start | bytes 786440 | tf_op jit(solution)/shard_map/ppermute | solution.py:31
  161.3 13.3 %collective-permute-start.20 = (bf16[8,32,512]{2,1,0:T(8,128)(2,1)S(1)}, bf16[8,32,512]{2,1,0:T(8,128)(2,1)}, u32[]{:S(2)}, u32[]{:S(2)}) collective-permute-start(bf16[8,32,512]{2,1,0:T(8,128)(2,1)S(1)} %bitcast.234), channel_id=1, source_target_pairs={{0,16},{8,24},{16,0},{24,8},{1,17},{9,25},{17,1},{25,9},{2,18},{10... | collective-permute-start | bytes 786440 | tf_op jit(solution)/shard_map/ppermute | solution.py:31
  164.8 33.8 %copy-start.40 = (bf16[128,256]{1,0:T(8,128)(2,1)S(1)}, bf16[128,256]{1,0:T(8,128)(2,1)}, u32[]{:S(2)}) copy-start(bf16[128,256]{1,0:T(8,128)(2,1)} %copy-done.39) | copy-start | bytes 196612
  164.8 33.8 %copy-start.42 = (bf16[128,256]{1,0:T(8,128)(2,1)S(1)}, bf16[128,256]{1,0:T(8,128)(2,1)}, u32[]{:S(2)}) copy-start(bf16[128,256]{1,0:T(8,128)(2,1)} %copy-done.41) | copy-start | bytes 196612
  164.8 19.9 %all-to-all-start.2 = ((bf16[32,40,128]{2,1,0:T(8,128)(2,1)}), bf16[32,40,128]{2,1,0:T(8,128)(2,1)S(1)}, u32[]{:S(2)}, u32[]{:S(2)}) async-start(bf16[32,40,128]{2,1,0:T(8,128)(2,1)} %pad_maximum_fusion.18), calls=%async_computation.2 | async-start | bytes 655360 | tf_op jit(solution)/shard_map/all_to_all | solution.py:43
  175.9 21.0 %collective-permute-start.21 = (bf16[2,32,512]{2,1,0:T(8,128)(2,1)S(1)}, bf16[2,32,512]{2,1,0:T(8,128)(2,1)S(1)}, u32[]{:S(2)}, u32[]{:S(2)}) collective-permute-start(bf16[2,32,512]{2,1,0:T(8,128)(2,1)S(1)} %get-tuple-element.134), channel_id=1, source_target_pairs={{0,64},{32,96},{64,128},{96,160},{128,192},{160,224},{192,0},{224,... | collective-permute-start | bytes 196616 | tf_op jit(solution)/shard_map/ppermute | solution.py:521
  177.2 19.7 %collective-permute-start.22 = (bf16[2,32,512]{2,1,0:T(8,128)(2,1)S(1)}, bf16[2,32,512]{2,1,0:T(8,128)(2,1)S(1)}, u32[]{:S(2)}, u32[]{:S(2)}) collective-permute-start(bf16[2,32,512]{2,1,0:T(8,128)(2,1)S(1)} %get-tuple-element.136), channel_id=1, source_target_pairs={{0,128},{32,160},{64,192},{96,224},{128,0},{160,32},{192,64},{224,... | collective-permute-start | bytes 196616 | tf_op jit(solution)/shard_map/ppermute | solution.py:521
  178.6 18.3 %collective-permute-start.23 = (bf16[2,32,512]{2,1,0:T(8,128)(2,1)S(1)}, bf16[2,32,512]{2,1,0:T(8,128)(2,1)S(1)}, u32[]{:S(2)}, u32[]{:S(2)}) collective-permute-start(bf16[2,32,512]{2,1,0:T(8,128)(2,1)S(1)} %get-tuple-element.135), channel_id=1, source_target_pairs={{0,192},{32,224},{64,0},{96,32},{128,64},{160,96},{192,128},{224,1... | collective-permute-start | bytes 196616 | tf_op jit(solution)/shard_map/ppermute | solution.py:521
  187.2 19.4 %all-to-all-start.3 = ((bf16[32,32,128]{2,1,0:T(8,128)(2,1)}), bf16[32,32,128]{2,1,0:T(8,128)(2,1)S(1)}, u32[]{:S(2)}, u32[]{:S(2)}) async-start(bf16[32,32,128]{2,1,0:T(8,128)(2,1)} %shard_map.199), calls=%async_computation.3 | async-start | bytes 524288 | tf_op jit(solution)/shard_map/all_to_all | solution.py:43
  197.0 13.0 %collective-permute-start.24 = (bf16[32,512]{1,0:T(8,128)(2,1)S(1)}, bf16[32,512]{1,0:T(8,128)(2,1)S(1)}, u32[]{:S(2)}, u32[]{:S(2)}) collective-permute-start(bf16[32,512]{1,0:T(8,128)(2,1)S(1)} %fusion.75), channel_id=1, source_target_pairs={{0,32},{32,0},{64,96},{96,64},{128,160},{160,128},{192,224},{224,1... | collective-permute-start | bytes 98312 | tf_op jit(solution)/shard_map/ppermute | solution.py:529
  210.0 1.6 collective-permute-start.26
  (49 other events, 194.0 us)
